TPU v7x, 128 devices: a whole 4x4x4 slice. The times are simulated.
128 devices in a mesh: st: 64 (over z, y, x), tp: 2 (over core).
Axes of the slice: x: 4, y: 4, z: 4, core: 2. Of those that a mesh axis runs over, the one named last changes fastest.
Arguments:
- hidden: bfloat16 [65536, 2048], P('st'), may hold values from -6 to 6
- norm_gain: float32 [2048], replicated, may hold values from 0.1 to 1.9
- store: bfloat16 [1536, 64, 2048], P('st'), may hold values from -6 to 6
- store_gain: float32 [2048], replicated, may hold values from 0.1 to 1.9
- passage_ids: int32 [512, 4], P('st'), may hold values from 0 to 1535, as said below
- w_pool: bfloat16 [2048, 1024], P(None, 'tp'), may hold values from -0.125 to 0.125
- pool_mix: bfloat16 [4, 256, 256], P('tp'), may hold values from -0.375 to 0.375
- w_branch: bfloat16 [1024, 2048], P('tp'), may hold values from -0.1875 to 0.1875
- w_query: bfloat16 [2048, 512], P(None, 'tp'), may hold values from -0.125 to 0.125
- w_key: bfloat16 [2048, 512], P(None, 'tp'), may hold values from -0.125 to 0.125
- w_value: bfloat16 [2048, 512], P(None, 'tp'), may hold values from -0.125 to 0.125
- sharpness: float32 [4], P('tp'), may hold values from 1 to 90
- w_out: bfloat16 [512, 2048], P('tp'), may hold values from -0.25 to 0.25
- w_gate: bfloat16 [2048, 2048], P(None, 'tp'), may hold values from -0.125 to 0.125
Outputs:
- mixed: bfloat16 [65536, 2048], P('st', 'tp')
Inputs may be any that keep to these rules, and one draw needn't show every extreme that they name: `passage_ids`: passage p lies on index p // 24 of st. The ids of one sequence's blocks (aligned rows of 32 ids) name passages of at most 1 reads on any one holder, counted with repeats, and some sequence reaches 1 at some holder in every draw.
All inputs are finite; a program needn't handle non-finite values.
Results may differ from a plain program's by a relative error of at most 0.0095.
The roundings to bfloat16 on the way count: a program that leaves them out, or rounds other values in their place, can miss the bound.
Values may be sent and summed in bfloat16 or wider, within the bound.
No kernel may reach another device: no remote copies, remote signals or barrier semaphores. Data moves between devices by JAX's collectives and lax.ppermute only.
A program may use at most 128 MiB of HBM per device.

v0:
```python
import math

import jax
import jax.numpy as jnp
from jax import lax
from jax.sharding import PartitionSpec as P

GROUPS = 4


def sent_together(arrays, axis, split_dim, concat_dim, along):
    both = jnp.concatenate(arrays, axis=along)
    filled, at, finished = (
        lax.all_to_all(both, axis, split_axis=split_dim, concat_axis=concat_dim, tiled=True),
        0,
        [],
    )
    for a in arrays:
        finished.append(lax.slice_in_dim(filled, at, at + a.shape[along], axis=along))
        at += a.shape[along]
    return tuple(finished)


def cut_along(shard, dim, count):
    shape = shard.shape
    pieces = shard.reshape(*shape[:dim], count, shape[dim] // count, *shape[dim + 1 :])
    return jnp.moveaxis(pieces, dim, 0)


def sum_at_owner(shard, axis, dim):
    pieces = cut_along(shard, dim, lax.axis_size(axis))
    arrived = lax.all_to_all(pieces, axis, split_axis=0, concat_axis=0, tiled=True)
    return arrived.astype(jnp.float32).sum(axis=0)


def sent_together_2(arrays, axis, dim, along):
    both = jnp.concatenate(arrays, axis=along)
    filled, at, finished = (sum_at_owner(both, axis, dim), 0, [])
    for a in arrays:
        finished.append(lax.slice_in_dim(filled, at, at + a.shape[along], axis=along))
        at += a.shape[along]
    return tuple(finished)


def rms_norm(values, gain):
    wide = values.astype(jnp.float32)
    scale = lax.rsqrt(jnp.mean(wide * wide, axis=-1, keepdims=True) + 1e-05)
    return wide * scale * gain


def project_rows(rows, store_gain, w_key, w_value):
    count, length, width = rows.shape
    passage_normed = rms_norm(rows, store_gain).astype(jnp.bfloat16).reshape(count * length, width)
    keys = jnp.dot(passage_normed, w_key, preferred_element_type=jnp.float32).astype(jnp.bfloat16)
    values = jnp.dot(passage_normed, w_value, preferred_element_type=jnp.float32).astype(
        jnp.bfloat16
    )
    return (keys.reshape(count, length, -1), values.reshape(count, length, -1))


def body(
    hidden,
    norm_gain,
    store,
    store_gain,
    passage_ids,
    w_pool,
    pool_mix,
    w_branch,
    w_query,
    w_key,
    w_value,
    sharpness,
    w_out,
    w_gate,
):
    tokens = hidden.shape[0]
    normed = rms_norm(hidden, norm_gain).astype(jnp.bfloat16)
    local_groups = pool_mix.shape[0]
    group_dim = pool_mix.shape[1]
    pool_in = jnp.dot(normed, w_pool, preferred_element_type=jnp.float32).astype(jnp.bfloat16)
    grouped = pool_in.astype(jnp.float32).reshape(tokens, local_groups, group_dim)
    group_index = lax.axis_index("tp") * local_groups + jnp.arange(local_groups, dtype=jnp.int32)
    window = jnp.power(2, group_index + 1)
    total = jnp.zeros_like(grouped)
    for shift in range(2**GROUPS):
        shifted = jnp.pad(grouped, ((shift, 0), (0, 0), (0, 0)))[:tokens]
        total = total + jnp.where(shift < window, 1.0, 0.0)[None, :, None] * shifted
    position = jnp.arange(tokens, dtype=jnp.int32)[:, None]
    count = jnp.minimum(position + 1, window[None, :]).astype(jnp.float32)
    pooled = (total / count[:, :, None] - grouped).astype(jnp.bfloat16)
    pool_out = jnp.einsum("tgc,gcd->tgd", pooled, pool_mix, preferred_element_type=jnp.float32)
    pool_out = pool_out.astype(jnp.bfloat16).reshape(tokens, local_groups * group_dim)
    pool_term = jnp.dot(pool_out, w_branch, preferred_element_type=jnp.float32)
    gate = jax.nn.sigmoid(jnp.dot(normed, w_gate, preferred_element_type=jnp.float32))
    holders = lax.axis_size("st")
    flat_ids = passage_ids.reshape(-1)
    reads = flat_ids.shape[0]
    pass_dev = store.shape[0]
    owner = flat_ids // pass_dev
    local = flat_ids % pass_dev
    order = jnp.arange(reads, dtype=jnp.int32)
    earlier = (owner[None, :] == owner[:, None]) & (order[None, :] < order[:, None])
    rank = jnp.sum(earlier.astype(jnp.int32), axis=1)
    most = max(1, 2 * reads // holders)
    slot = owner * most + rank
    hits = slot[None, :] == jnp.arange(holders * most, dtype=jnp.int32)[:, None]
    request = jnp.sum(jnp.where(hits, local[None, :], 0), axis=1).reshape(holders, most)
    incoming = lax.all_to_all(request, "st", split_axis=0, concat_axis=0, tiled=True)
    rows = store[incoming.reshape(-1)]
    own_keys, own_values = project_rows(rows, store_gain, w_key, w_value)
    keys, values = sent_together((own_keys, own_values), "st", 0, 0, 1)
    local_heads = sharpness.shape[0]
    local_width = w_query.shape[1]
    head_dim = local_width // local_heads
    blocks_dev, per_block = passage_ids.shape
    block_len = tokens // blocks_dev
    query = jnp.dot(normed, w_query, preferred_element_type=jnp.float32).astype(jnp.bfloat16)
    query_blocks = query.reshape(blocks_dev, block_len, local_heads, head_dim)
    block_slot = slot.reshape(blocks_dev, per_block)
    block_keys = keys[block_slot].reshape(blocks_dev, -1, local_heads, head_dim)
    block_values = values[block_slot].reshape(blocks_dev, -1, local_heads, head_dim)
    scores = jnp.einsum(
        "bqhd,bkhd->bhqk", query_blocks, block_keys, preferred_element_type=jnp.float32
    )
    scores = scores * (sharpness / math.sqrt(head_dim))[None, :, None, None]
    weights = jax.nn.softmax(scores, axis=-1).astype(jnp.bfloat16)
    read = jnp.einsum("bhqk,bkhd->bqhd", weights, block_values, preferred_element_type=jnp.float32)
    read = read.astype(jnp.bfloat16).reshape(tokens, local_width)
    read_term = jnp.dot(read, w_out, preferred_element_type=jnp.float32)
    branch_pool, branch_read = sent_together_2(
        (pool_term.astype(jnp.bfloat16), read_term.astype(jnp.bfloat16)), "tp", 1, 0
    )
    return (branch_pool + gate * branch_read).astype(jnp.bfloat16)


def solution(mesh):
    placed = (
        P("st", None),
        P(),
        P("st", None, None),
        P(),
        P("st", None),
        P(None, "tp"),
        P("tp", None, None),
        P("tp", None),
        P(None, "tp"),
        P(None, "tp"),
        P(None, "tp"),
        P("tp"),
        P("tp", None),
        P(None, "tp"),
    )
    return jax.shard_map(body, mesh=mesh, in_specs=placed, out_specs=P("st", "tp"), check_vma=False)
```

profile of v0, /device:TPU:1, one launch (start us, length us, event | category | flops | bytes accessed | tf_op | source)
XLA Modules:
  0.0 203.5 jit_solution(14691474276485838262)
XLA Ops:
  0.0 0.9 copy.134
  0.9 0.1 div.60
  1.0 0.1 rem.34
  1.1 0.1 ne.405
  1.2 0.2 convert_reduce_fusion.1
  1.4 0.1 select_reduce_fusion
  1.5 0.7 copy.137
  2.2 12.0 %all-to-all-start = ((s32[64,1,1]{2,1,0:T(1,128)}), s32[64,1,1]{2,1,0:T(1,128)S(1)}, u32[]{:S(2)}, u32[]{:S(2)}) async-start(s32[64,1,1]{2,1,0:T(1,128)} %copy.137), calls=%async_computation | async-start | bytes 65536 | tf_op jit(solution)/shard_map/all_to_all | solution.py:109
  14.2 3.2 %fusion.3 = f32[1024]{0:T(1024)S(1)} fusion(bf16[1024,2048]{1,0:T(8,128)(2,1)} %param.14), kind=kLoop, calls=%fused_computation.11 | loop fusion | flops 6290432 | bytes 4198400 | tf_op jit(solution)/shard_map/reduce_sum | solution.py:47
  17.4 0.2 copy-done.2
  17.6 2.5 %convolution_convert_fusion.7 = bf16[1024,256]{1,0:T(8,128)(2,1)S(1)} fusion(bf16[2048,256]{1,0:T(8,128)(2,1)} %param.22, bf16[1024,2048]{1,0:T(8,128)(2,1)S(1)} %copy-done.2, f32[2048]{0:T(1024)S(1)} %copy-done.9, f32[1024]{0:T(1024)S(1)} %add_rsqrt_fusion.1), kind=kOutput, calls=%fused_computation.77 | convolution fusion | flops 1082392576 | bytes 5779456 | tf_op jit(solution)/shard_map/dot_general | solution.py:118
  20.2 0.1 reduce_sum.60
  20.2 2.3 %all-to-all-done = s32[64,1,1]{2,1,0:T(1,128)S(1)} async-done(((s32[64,1,1]{2,1,0:T(1,128)}), s32[64,1,1]{2,1,0:T(1,128)S(1)}, u32[]{:S(2)}, u32[]{:S(2)}) %all-to-all-start) | async-done | bytes 288 | tf_op jit(solution)/shard_map/all_to_all | solution.py:109
  22.5 1.2 reduce
  23.8 10.3 %gather_fusion = bf16[64,64,2048]{2,1,0:T(8,128)(2,1)} fusion(bf16[24,64,2048]{2,1,0:T(8,128)(2,1)} %param.16, s32[1024]{0:T(1024)S(1)} %pad_clamp_fusion.1), kind=kCustom, calls=%fused_computation | custom fusion | bytes 33554688 | tf_op jit(solution)/shard_map/gather | solution.py:110
  34.0 7.2 %multiply_reduce_fusion = f32[64,64]{1,0:T(8,128)S(1)} fusion(bf16[64,64,2048]{2,1,0:T(8,128)(2,1)} %gather_fusion), kind=kLoop, calls=%fused_computation.7 | loop fusion | flops 25161728 | bytes 16793600 | tf_op jit(solution)/shard_map/reduce_sum | solution.py:47
  41.2 0.1 rsqrt.21
  41.3 10.1 %fusion.2 = bf16[4096,2048]{1,0:T(8,128)(2,1)S(1)} fusion(f32[2048]{0:T(1024)S(1)} %copy-done.5, f32[4096]{0:T(1024)S(1)} %rsqrt.21, bf16[64,64,2048]{2,1,0:T(8,128)(2,1)} %gather_fusion), kind=kLoop, calls=%fused_computation.6 | loop fusion | flops 33554432 | bytes 33579008 | tf_op jit(solution)/shard_map/convert_element_type | solution.py:53
  51.5 0.0 copy-start.7
  51.5 4.7 %convolution_convert_fusion.1 = bf16[4096,256]{1,0:T(8,128)(2,1)S(1)} fusion(bf16[4096,2048]{1,0:T(8,128)(2,1)S(1)} %fusion.2, bf16[2048,256]{1,0:T(8,128)(2,1)S(1)} %copy-done.6), kind=kOutput, calls=%fused_computation.17 | convolution fusion | flops 4296015872 | bytes 19922944 | tf_op jit(solution)/shard_map/dot_general | solution.py:54
  56.2 4.7 %convolution_convert_fusion = bf16[4096,256]{1,0:T(8,128)(2,1)S(1)} fusion(bf16[4096,2048]{1,0:T(8,128)(2,1)S(1)} %fusion.2, bf16[2048,256]{1,0:T(8,128)(2,1)S(1)} %copy-done.7), kind=kOutput, calls=%fused_computation.16 | convolution fusion | flops 4296015872 | bytes 19922944 | tf_op jit(solution)/shard_map/dot_general | solution.py:55
  61.0 2.5 %pad_maximum_fusion.1 = bf16[64,128,256]{2,1,0:T(8,128)(2,1)} fusion(bf16[64,64,256]{2,1,0:T(8,128)(2,1)S(1)} %bitcast.49, bf16[64,64,256]{2,1,0:T(8,128)(2,1)S(1)} %bitcast.48), kind=kLoop, calls=%fused_computation.21 | loop fusion | flops 8388608 | bytes 8388608 | tf_op jit(solution)/shard_map/concatenate | solution.py:12
  63.4 7.6 %all-to-all-start.1 = ((bf16[64,128,256]{2,1,0:T(8,128)(2,1)}), bf16[64,128,256]{2,1,0:T(8,128)(2,1)}, u32[]{:S(2)}, u32[]{:S(2)}) async-start(bf16[64,128,256]{2,1,0:T(8,128)(2,1)} %pad_maximum_fusion.1), calls=%async_computation.1 | async-start | bytes 8388608 | tf_op jit(solution)/shard_map/all_to_all | solution.py:14
  71.1 0.1 reshape.340
  71.2 0.9 reshape.323
  72.1 5.4 %convolution_convert_fusion.5 = bf16[1024,512]{0,1:T(8,128)(2,1)S(1)} fusion(bf16[2048,512]{1,0:T(8,128)(2,1)} %param.19, bf16[1024,2048]{1,0:T(8,128)(2,1)} %param.14, f32[2048]{0:T(1024)S(1)} %copy-done.9, f32[1024]{0:T(1024)S(1)} %add_rsqrt_fusion.1), kind=kOutput, calls=%fused_computation.75 | convolution fusion | flops 2156396544 | bytes 7352320 | tf_op jit(solution)/shard_map/dot_general | solution.py:81
  77.5 0.0 copy-start.8
  77.5 1.6 copy.116
  79.4 0.1 minimum_convert_fusion
  79.4 17.1 %convolution_convert_fusion.4 = bf16[2,1024,256]{1,2,0:T(8,128)(2,1)S(1)} fusion(bf16[2,256,256]{2,1,0:T(8,128)(2,1)S(1)} %copy-done.8, f32[1024,2,256]{2,0,1:T(8,128)} %copy.116, f32[1024,2]{0,1:T(2,128)S(1)} %minimum_convert_fusion, f32[2]{0:T(128)S(1)} %get-tuple-element.11, f32[2]{0:T(128)S(1)} %get-tuple-element.12, f32[2]{0:T(128)S(1)} %get-tuple-element.13, ...), kind=kOutput, calls=%fused_computation.74 | convolution fusion | flops 286785536 | bytes 3416192 | tf_op jit(solution)/shard_map/tgc,gcd->tgd/dot_general | solution.py:92
  96.5 4.4 %convolution_convert_fusion.3 = bf16[1024,2048]{1,0:T(8,128)(2,1)} fusion(bf16[1024,512]{0,1:T(8,128)(2,1)S(1)} %bitcast.52, bf16[512,2048]{1,0:T(8,128)(2,1)S(1)} %copy-done), kind=kOutput, calls=%fused_computation.23 | convolution fusion | flops 2149580800 | bytes 7340032 | tf_op jit(solution)/shard_map/dot_general | solution.py:94
  100.9 21.1 %all-to-all-done.1 = bf16[64,128,256]{2,1,0:T(8,128)(2,1)} async-done(((bf16[64,128,256]{2,1,0:T(8,128)(2,1)}), bf16[64,128,256]{2,1,0:T(8,128)(2,1)}, u32[]{:S(2)}, u32[]{:S(2)}) %all-to-all-start.1) | async-done | bytes 4194336 | tf_op jit(solution)/shard_map/all_to_all | solution.py:14
  122.0 4.1 %fusion.67 = (bf16[64,64,256]{2,1,0:T(8,128)(2,1)}, bf16[64,64,256]{2,1,0:T(8,128)(2,1)S(1)}) fusion(bf16[64,128,256]{2,1,0:T(8,128)(2,1)} %all-to-all-done.1), kind=kLoop, calls=%fused_computation.132 | loop fusion | bytes 8388608 | tf_op jit(solution)/shard_map/slice | solution.py:19
  126.1 3.2 %gather_fusion.2 = bf16[32,64,256]{2,1,0:T(8,128)(2,1)} fusion(bf16[64,64,256]{2,1,0:T(8,128)(2,1)} %get-tuple-element.5, s32[1024]{0:T(1024)S(1)} %pad_clamp_fusion), kind=kCustom, calls=%fused_computation.2 | custom fusion | bytes 2097280 | tf_op jit(solution)/shard_map/gather | solution.py:121
  129.3 1.3 reshape.324
  130.7 2.8 %fusion.41 = f32[8,2,128,256]{3,2,1,0:T(8,128)} fusion(bf16[8,256,2,128]{3,2,1,0:T(2,128)(2,1)S(1)} %reshape.324, bf16[8,128,2,128]{3,2,1,0:T(2,128)(2,1)} %reshape.323), kind=kOutput, calls=%fused_computation.80 | convolution fusion | flops 134217728 | bytes 3670016 | tf_op jit(solution)/shard_map/bqhd,bkhd->bhqk/dot_general | solution.py:123
  133.5 2.0 fusion.68
  135.5 0.6 gather_fusion.1
  136.1 0.5 reshape.322
  136.6 0.0 copy-start.4
  136.7 5.7 %fusion.39 = bf16[8,128,2,128]{1,3,2,0:T(8,128)(2,1)S(1)} fusion(bf16[8,256,2,128]{3,2,1,0:T(2,128)(2,1)S(1)} %reshape.322, f32[8,2,128]{2,1,0:T(2,128)S(1)} %fusion.68, f32[8,2,128,256]{3,2,1,0:T(8,128)} %fusion.41, f32[2]{0:T(128)S(1)} %broadcast_multiply_fusion), kind=kOutput, calls=%fused_computation.78 | convolution fusion | flops 136579328 | bytes 3678216 | tf_op jit(solution)/shard_map/bhqk,bkhd->bqhd/dot_general | solution.py:128
  142.4 0.3 copy.141
  142.7 3.3 %convolution_convert_fusion.2 = bf16[1024,2048]{1,0:T(8,128)(2,1)} fusion(bf16[256,2048]{1,0:T(8,128)(2,1)S(1)} %copy-done.4, bf16[32,8,8,128]{3,2,1,0:T(8,128)(2,1)S(1)} %bitcast.47), kind=kOutput, calls=%fused_computation.22 | convolution fusion | flops 1075838976 | bytes 5767168 | tf_op jit(solution)/shard_map/dot_general | solution.py:130
  146.0 8.4 %pad_maximum_fusion = bf16[2048,2048]{1,0:T(8,128)(2,1)} fusion(bf16[1024,2048]{1,0:T(8,128)(2,1)} %convolution_convert_fusion.2, bf16[1024,2048]{1,0:T(8,128)(2,1)} %convolution_convert_fusion.3), kind=kLoop, calls=%fused_computation.15 | loop fusion | flops 16777216 | bytes 16777216 | tf_op jit(solution)/shard_map/concatenate | solution.py:37
  154.3 7.8 %copy.169 = bf16[256,2,8,1024]{3,2,0,1:T(8,128)(2,1)} copy(bf16[256,2,8,1024]{3,2,1,0:T(8,128)(2,1)} %bitcast.45) | data formatting | bytes 16777216 | tf_op jit(solution)/shard_map/reshape | solution.py:26
  162.1 21.2 %all_to_all.22 = bf16[2,2048,1024]{2,1,0:T(8,128)(2,1)} all-to-all(bf16[2,2048,1024]{2,1,0:T(8,128)(2,1)} %bitcast.46), channel_id=1, replica_groups=mesh['st'=64,'tp'=2] {'tp'}, dimensions={0} | all-to-all | bytes 16777216 | tf_op jit(solution)/shard_map/all_to_all | solution.py:32
  183.3 10.1 %convert_reduce_fusion = f32[2048,1024]{1,0:T(8,128)} fusion(bf16[2,2048,1024]{2,1,0:T(8,128)(2,1)} %all_to_all.22), kind=kLoop, calls=%fused_computation.8 | loop fusion | flops 6291456 | bytes 16777216 | tf_op jit(solution)/shard_map/reduce_sum | solution.py:33
  193.4 10.1 %fusion.7 = bf16[1024,1024]{1,0:T(8,128)(2,1)} fusion(f32[2048,1024]{1,0:T(8,128)} %convert_reduce_fusion, bf16[2048,1024]{1,0:T(8,128)(2,1)} %param.27, bf16[1024,2048]{1,0:T(8,128)(2,1)S(1)} %copy-done.3, f32[2048]{0:T(1024)S(1)} %copy-done.9, f32[1024]{0:T(1024)S(1)} %add_rsqrt_fusion.1), kind=kOutput, calls=%fused_computation.20 | convolution fusion | flops 4309647360 | bytes 18886656 | tf_op jit(solution)/shard_map/dot_general | solution.py:95
  (39 shorter events, 0.3 us)
Async XLA Ops:
  0.0 96.5 %copy-start = (bf16[512,2048]{1,0:T(8,128)(2,1)S(1)}, bf16[512,2048]{1,0:T(8,128)(2,1)}, u32[]{:S(2)}) copy-start(bf16[512,2048]{1,0:T(8,128)(2,1)} %param.21) | copy-start | bytes 6291460
  2.2 20.3 %all-to-all-start = ((s32[64,1,1]{2,1,0:T(1,128)}), s32[64,1,1]{2,1,0:T(1,128)S(1)}, u32[]{:S(2)}, u32[]{:S(2)}) async-start(s32[64,1,1]{2,1,0:T(1,128)} %copy.137), calls=%async_computation | async-start | bytes 65536 | tf_op jit(solution)/shard_map/all_to_all | solution.py:109
  14.2 3.5 %copy-start.2 = (bf16[1024,2048]{1,0:T(8,128)(2,1)S(1)}, bf16[1024,2048]{1,0:T(8,128)(2,1)}, u32[]{:S(2)}) copy-start(bf16[1024,2048]{1,0:T(8,128)(2,1)} %param.14) | copy-start | bytes 12582916
  14.2 3.4 %copy-start.9 = (f32[2048]{0:T(1024)S(1)}, f32[2048]{0:T(1024)}, u32[]{:S(2)}) copy-start(f32[2048]{0:T(1024)} %param.15) | copy-start | bytes 24580
  34.0 7.3 %copy-start.5 = (f32[2048]{0:T(1024)S(1)}, f32[2048]{0:T(1024)}, u32[]{:S(2)}) copy-start(f32[2048]{0:T(1024)} %param.17) | copy-start | bytes 24580
  41.3 10.1 %copy-start.6 = (bf16[2048,256]{1,0:T(8,128)(2,1)S(1)}, bf16[2048,256]{1,0:T(8,128)(2,1)}, u32[]{:S(2)}) copy-start(bf16[2048,256]{1,0:T(8,128)(2,1)} %param.23) | copy-start | bytes 3145732
  51.5 4.8 %copy-start.7 = (bf16[2048,256]{1,0:T(8,128)(2,1)S(1)}, bf16[2048,256]{1,0:T(8,128)(2,1)}, u32[]{:S(2)}) copy-start(bf16[2048,256]{1,0:T(8,128)(2,1)} %param.24) | copy-start | bytes 3145732
  63.4 58.6 %all-to-all-start.1 = ((bf16[64,128,256]{2,1,0:T(8,128)(2,1)}), bf16[64,128,256]{2,1,0:T(8,128)(2,1)}, u32[]{:S(2)}, u32[]{:S(2)}) async-start(bf16[64,128,256]{2,1,0:T(8,128)(2,1)} %pad_maximum_fusion.1), calls=%async_computation.1 | async-start | bytes 8388608 | tf_op jit(solution)/shard_map/all_to_all | solution.py:14
  77.5 1.8 copy-start.10
  77.5 1.9 copy-start.8
  136.6 6.1 %copy-start.4 = (bf16[256,2048]{1,0:T(8,128)(2,1)S(1)}, bf16[256,2048]{1,0:T(8,128)(2,1)}, u32[]{:S(2)}) copy-start(bf16[256,2048]{1,0:T(8,128)(2,1)} %param.26) | copy-start | bytes 3145732
  183.3 10.1 %copy-start.3 = (bf16[1024,2048]{1,0:T(8,128)(2,1)S(1)}, bf16[1024,2048]{1,0:T(8,128)(2,1)}, u32[]{:S(2)}) copy-start(bf16[1024,2048]{1,0:T(8,128)(2,1)} %param.14) | copy-start | bytes 12582916
  193.4 10.1 %copy-start.1 = (bf16[512,2048]{1,0:T(8,128)(2,1)S(1)}, bf16[512,2048]{1,0:T(8,128)(2,1)}, u32[]{:S(2)}) copy-start(bf16[512,2048]{1,0:T(8,128)(2,1)} %param.21) | copy-start | bytes 6291460
where the time goes:
time: 204 us
  matrix products  62.7 us (31%)
  other arithmetic  43.3 us (21%)
  local copies, waits for them, and re-layouts  33.1 us (16%)
  waiting for transfers between devices  23.3 us (11%)
  blocking collectives  21.2 us (10%)
  starting transfers between devices  19.6 us (10%)
    all_to_all x1, blocking collectives, sum_at_owner(): lax.all_to_all(pieces, axis, split_axis=0, concat_axis=0, tiled=True)  21.2 us
    all_to_all x1, waiting for transfers between devices, sent_together(): lax.all_to_all(both, axis, split_axis=split_dim, concat_axis=concat_dim,...  21.1 us
    dot_general x1, matrix products, body(): jnp.einsum('tgc,gcd->tgd', pooled, pool_mix, preferred_element_type=jnp.f...  17.1 us
    all_to_all x1, starting transfers between devices, body(): lax.all_to_all(request, 'st', split_axis=0, concat_axis=0, tiled=True)  12 us
    reduce_sum x2, other arithmetic, rms_norm(): scale = lax.rsqrt(jnp.mean(wide * wide, axis=-1, keepdims=True) + 1e-05)  10.4 us
    gather x1, local copies, waits for them, and re-layouts, body(): rows = store[incoming.reshape(-1)]  10.3 us
    convert_element_type x1, other arithmetic, project_rows(): rms_norm(rows, store_gain).astype(jnp.bfloat16)  10.1 us
    reduce_sum x1, other arithmetic, sum_at_owner(): return arrived.astype(jnp.float32).sum(axis=0)  10.1 us
  transfers between devices with their start and end apart: 2, of which 2 were waited for; matrix products, arithmetic and copies ran while one was open for 17% of the time, Pallas kernels for 0%

commit v1 on v0

v1 whole, which is shorter than its diff:
```python
import functools
import math

import jax
import jax.numpy as jnp
from jax import lax
from jax.experimental import pallas as pl
from jax.experimental.pallas import tpu as pltpu
from jax.sharding import PartitionSpec as P

F32, BF16 = jnp.float32, jnp.bfloat16
EPS = 1e-05
CARRY = 16
SWAP = [(0, 1), (1, 0)]


def rms_norm(wide, gain):
    scale = lax.rsqrt(jnp.mean(wide * wide, axis=-1, keepdims=True) + EPS)
    return (wide * scale * gain).astype(BF16)


def dot(a, b):
    return jnp.dot(a, b, preferred_element_type=F32)


def cost(flops, bytes_accessed, transcendentals=0):
    return pl.CostEstimate(
        flops=flops, bytes_accessed=bytes_accessed, transcendentals=transcendentals
    )


def params(mib, **kw):
    return pltpu.CompilerParams(vmem_limit_bytes=mib << 20, **kw)


def project_kernel(rows_ref, gain_ref, key_ref, value_ref, out_ref):
    normed = rms_norm(rows_ref[...].astype(F32), gain_ref[...])
    width = key_ref.shape[1]
    out_ref[:, :width] = dot(normed, key_ref[...]).astype(BF16)
    out_ref[:, width:] = dot(normed, value_ref[...]).astype(BF16)


def project(store, gain, w_key, w_value):
    count, length, width = store.shape
    rows = count * length
    tile = 256
    kv = w_key.shape[1] + w_value.shape[1]
    return pl.pallas_call(
        project_kernel,
        grid=(rows // tile,),
        in_specs=[
            pl.BlockSpec((tile, width), lambda i: (i, 0)),
            pl.BlockSpec((1, width), lambda i: (0, 0)),
            pl.BlockSpec(w_key.shape, lambda i: (0, 0)),
            pl.BlockSpec(w_value.shape, lambda i: (0, 0)),
        ],
        out_specs=pl.BlockSpec((tile, kv), lambda i: (i, 0)),
        out_shape=jax.ShapeDtypeStruct((rows, kv), BF16),
        compiler_params=params(24),
        cost_estimate=cost(2 * rows * width * kv, rows * (width + kv) * 2 + width * kv * 2),
        name="project",
    )(store.reshape(rows, width), gain.reshape(1, width), w_key, w_value)


def place_kernel(request_ref, kv_ref, out_ref, sems):
    readers = out_ref.shape[0]

    def copy(r):
        which = jnp.maximum(request_ref[r] - 1, 0)
        return pltpu.make_async_copy(kv_ref.at[which], out_ref.at[r], sems.at[r])

    def start(r, _):
        @pl.when(request_ref[r] > 0)
        def _():
            copy(r).start()

        return 0

    def finish(r, _):
        @pl.when(request_ref[r] > 0)
        def _():
            copy(r).wait()

        return 0

    lax.fori_loop(0, readers, start, 0)
    lax.fori_loop(0, readers, finish, 0)


def place(request, kv):
    readers = request.shape[0]
    return pl.pallas_call(
        place_kernel,
        in_specs=[
            pl.BlockSpec(memory_space=pltpu.SMEM),
            pl.BlockSpec(memory_space=pltpu.VMEM),
        ],
        out_specs=pl.BlockSpec(memory_space=pl.ANY),
        out_shape=jax.ShapeDtypeStruct((readers,) + kv.shape[1:], BF16),
        scratch_shapes=[pltpu.SemaphoreType.DMA((readers,))],
        compiler_params=params(8),
        cost_estimate=cost(0, 6 << 20),
        name="place",
    )(request, kv)


def front_kernel(
    half_ref, hidden_ref, gain_ref, pool_ref, query_ref, gate_ref, mix_ref,
    pool_out_ref, query_out_ref, gate_out_ref, carry,
):
    step = pl.program_id(0)
    tile = hidden_ref.shape[0]
    groups, dim = mix_ref.shape[0], mix_ref.shape[1]

    @pl.when(step == 0)
    def _():
        carry[...] = jnp.zeros_like(carry)

    normed = rms_norm(hidden_ref[...].astype(F32), gain_ref[...])
    pool_in = dot(normed, pool_ref[...]).astype(BF16)
    query_out_ref[...] = dot(normed, query_ref[...]).astype(BF16)
    gate_out_ref[...] = jax.nn.sigmoid(dot(normed, gate_ref[...]))
    recent = jnp.concatenate([carry[...], pool_in], axis=0)
    carry[...] = pool_in[tile - CARRY :]
    shape = (tile, tile + CARRY)
    back = (
        lax.broadcasted_iota(jnp.int32, shape, 0)
        + CARRY
        - lax.broadcasted_iota(jnp.int32, shape, 1)
    )
    position = step * tile + lax.broadcasted_iota(jnp.int32, (tile, 1), 0)
    for g in range(groups):
        window = jnp.left_shift(2, half_ref[0] * groups + g)
        band = jnp.where((back >= 0) & (back < window), 1.0, 0.0).astype(BF16)
        columns = slice(g * dim, (g + 1) * dim)
        total = dot(band, recent[:, columns])
        count = jnp.minimum(position + 1, window).astype(F32)
        pooled = (total / count - pool_in[:, columns].astype(F32)).astype(BF16)
        pool_out_ref[:, columns] = dot(pooled, mix_ref[g]).astype(BF16)


def front(half, hidden, gain, w_pool, w_query, w_gate, pool_mix):
    tokens, width = hidden.shape
    tile = 256
    fixed = lambda a: pl.BlockSpec(a.shape, lambda i: (0,) * a.ndim)
    rowed = lambda n: pl.BlockSpec((tile, n), lambda i: (i, 0))
    gain = gain.reshape(1, width)
    outs = (w_pool.shape[1], w_query.shape[1], w_gate.shape[1])
    return pl.pallas_call(
        front_kernel,
        grid=(tokens // tile,),
        in_specs=[
            pl.BlockSpec(memory_space=pltpu.SMEM),
            rowed(width),
            fixed(gain),
            fixed(w_pool),
            fixed(w_query),
            fixed(w_gate),
            fixed(pool_mix),
        ],
        out_specs=[rowed(n) for n in outs],
        out_shape=[
            jax.ShapeDtypeStruct((tokens, outs[0]), BF16),
            jax.ShapeDtypeStruct((tokens, outs[1]), BF16),
            jax.ShapeDtypeStruct((tokens, outs[2]), F32),
        ],
        scratch_shapes=[pltpu.VMEM((CARRY, outs[0]), BF16)],
        compiler_params=params(40),
        cost_estimate=cost(2 * tokens * width * sum(outs), 24 << 20, tokens * outs[2]),
        name="front",
    )(half, hidden, gain, w_pool, w_query, w_gate, pool_mix)


def branch_kernel(own_ref, other_ref, w_own_ref, w_other_ref, out_ref):
    own = dot(own_ref[...], w_own_ref[...]).astype(BF16).astype(F32)
    out_ref[...] = own + dot(other_ref[...], w_other_ref[...]).astype(BF16).astype(F32)


def branch(own, other, w_own, w_other):
    tokens, depth = own.shape
    width = w_own.shape[1]
    tile = 256
    return pl.pallas_call(
        branch_kernel,
        grid=(tokens // tile,),
        in_specs=[
            pl.BlockSpec((tile, depth), lambda i: (i, 0)),
            pl.BlockSpec((tile, depth), lambda i: (i, 0)),
            pl.BlockSpec((depth, width), lambda i: (0, 0)),
            pl.BlockSpec((depth, width), lambda i: (0, 0)),
        ],
        out_specs=pl.BlockSpec((tile, width), lambda i: (i, 0)),
        out_shape=jax.ShapeDtypeStruct((tokens, width), F32),
        compiler_params=params(24),
        cost_estimate=cost(4 * tokens * depth * width, 8 << 20),
        name="branch",
    )(own, other, w_own, w_other)


def attend_kernel(slot_ref, sharp_ref, query_ref, kv_ref, out_ref, held, sems, *, reads):
    count, length, width = held.shape[0], held.shape[1], held.shape[2]
    heads = sharp_ref.shape[0]
    half = width // 2
    dim = half // heads
    blocks = count // reads
    block = query_ref.shape[0] // blocks

    def copy(r):
        return pltpu.make_async_copy(kv_ref.at[slot_ref[r]], held.at[r], sems.at[r])

    for r in range(count):
        copy(r).start()

    def one_block(b, _):
        for j in range(reads):
            copy(b * reads + j).wait()
        rows = pl.ds(pl.multiple_of(b * block, block), block)
        memory = held[pl.ds(b * reads, reads)].reshape(reads * length, width)
        query = query_ref[rows, :]
        for h in range(heads):
            keys = memory[:, h * dim : (h + 1) * dim]
            values = memory[:, half + h * dim : half + (h + 1) * dim]
            scores = lax.dot_general(
                query[:, h * dim : (h + 1) * dim], keys, (((1,), (1,)), ((), ())),
                preferred_element_type=F32,
            )
            scores = scores * (sharp_ref[h] / math.sqrt(dim))
            scores = jnp.exp(scores - jnp.max(scores, axis=-1, keepdims=True))
            weights = (scores / jnp.sum(scores, axis=-1, keepdims=True)).astype(BF16)
            out_ref[rows, h * dim : (h + 1) * dim] = dot(weights, values).astype(BF16)
        return 0

    lax.fori_loop(0, blocks, one_block, 0)


def attend(slots, sharpness, query, kv, reads):
    count = slots.shape[0]
    return pl.pallas_call(
        functools.partial(attend_kernel, reads=reads),
        in_specs=[
            pl.BlockSpec(memory_space=pltpu.SMEM),
            pl.BlockSpec(memory_space=pltpu.SMEM),
            pl.BlockSpec(memory_space=pltpu.VMEM),
            pl.BlockSpec(memory_space=pl.ANY),
        ],
        out_specs=pl.BlockSpec(memory_space=pltpu.VMEM),
        out_shape=jax.ShapeDtypeStruct(query.shape, BF16),
        scratch_shapes=[
            pltpu.VMEM((count,) + kv.shape[1:], BF16),
            pltpu.SemaphoreType.DMA((count,)),
        ],
        compiler_params=params(16),
        cost_estimate=cost(1 << 30, 3 << 20, 1 << 19),
        name="attend",
    )(slots, sharpness, query, kv)


def mixed_kernel(own_ref, other_ref, w_own_ref, w_other_ref, pool_ref, gate_ref, out_ref):
    own = dot(own_ref[...], w_own_ref[...]).astype(BF16).astype(F32)
    read = own + dot(other_ref[...], w_other_ref[...]).astype(BF16).astype(F32)
    out_ref[...] = (pool_ref[...] + gate_ref[...] * read).astype(BF16)


def mix(own, other, w_own, w_other, pool, gate):
    tokens, depth = own.shape
    width = w_own.shape[1]
    tile = 256
    rowed = lambda n: pl.BlockSpec((tile, n), lambda i: (i, 0))
    fixed = pl.BlockSpec((depth, width), lambda i: (0, 0))
    return pl.pallas_call(
        mixed_kernel,
        grid=(tokens // tile,),
        in_specs=[rowed(depth), rowed(depth), fixed, fixed, rowed(width), rowed(width)],
        out_specs=rowed(width),
        out_shape=jax.ShapeDtypeStruct((tokens, width), BF16),
        compiler_params=params(24),
        cost_estimate=cost(4 * tokens * depth * width, 12 << 20),
        name="mixed",
    )(own, other, w_own, w_other, pool, gate)


def body(
    hidden, norm_gain, store, store_gain, passage_ids, w_pool, pool_mix, w_branch,
    w_query, w_key, w_value, sharpness, w_out, w_gate,
):
    half = lax.axis_index("tp")
    holders = lax.axis_size("st")
    count, length, _ = store.shape
    reads = passage_ids.shape[1]
    flat = passage_ids.reshape(-1)
    owner, local = flat // count, flat % count
    hits = owner[None, :] == jnp.arange(holders, dtype=jnp.int32)[:, None]
    request = jnp.sum(jnp.where(hits, local[None, :] + 1, 0), axis=1).reshape(holders, 1, 1)
    incoming = lax.all_to_all(request, "st", split_axis=0, concat_axis=0, tiled=True)
    kv = project(store, store_gain, w_key, w_value).reshape(count, length, -1)
    sent = place(incoming.reshape(-1), kv)
    arrived = lax.all_to_all(sent, "st", split_axis=0, concat_axis=0, tiled=True)

    columns = w_branch.shape[1] // 2

    def weights(w):
        mine = lax.dynamic_slice_in_dim(w, half * columns, columns, axis=1)
        theirs = lax.dynamic_slice_in_dim(w, (1 - half) * columns, columns, axis=1)
        return mine, lax.ppermute(theirs, "tp", SWAP)

    branch_own, branch_other = weights(w_branch)
    out_own, out_other = weights(w_out)
    pool_out, query, gate = front(
        half.reshape(1), hidden, norm_gain, w_pool, w_query, w_gate, pool_mix
    )
    pool = branch(pool_out, lax.ppermute(pool_out, "tp", SWAP), branch_own, branch_other)
    read = attend(owner, sharpness, query, arrived, reads)
    return mix(read, lax.ppermute(read, "tp", SWAP), out_own, out_other, pool, gate)


def solution(mesh):
    placed = (
        P("st", None), P(), P("st", None, None), P(), P("st", None), P(None, "tp"),
        P("tp", None, None), P("tp", None), P(None, "tp"), P(None, "tp"), P(None, "tp"),
        P("tp"), P("tp", None), P(None, "tp"),
    )
    return jax.shard_map(body, mesh=mesh, in_specs=placed, out_specs=P("st", "tp"), check_vma=False)
```

time: 204 us -> 117 us (0.57)
  matrix products: 62.7 us -> 0 us
  Pallas kernels: 0 us -> 41.1 us
  other arithmetic: 43.3 us -> 2.7 us
  blocking collectives: 21.2 us -> 0 us
  local copies, waits for them, and re-layouts: 33.1 us -> 17.1 us
  starting transfers between devices: 19.6 us -> 28 us
  waiting for transfers between devices: 23.3 us -> 27.2 us
    dot_general x10 -> x0, matrix products: 60.7 us -> none  [the longest x1 17.1 us: body(): jnp.einsum('tgc,gcd->tgd', pooled, pool_mix, preferred_element_type=jnp.f...]
    pallas_call x0 -> x6, Pallas kernels: none -> 41.1 us  [the longest x1 13.8 us: front(): pl.pallas_call(front_kernel, grid=(tokens // tile,), in_specs=[pl.BlockSp...]
    all_to_all x1 -> x0, blocking collectives: 21.2 us -> none  [sum_at_owner(): lax.all_to_all(pieces, axis, split_axis=0, concat_axis=0, tiled=True)]
    reduce_sum x5 -> x1, other arithmetic: 20.8 us -> 0.09 us  [body(): jnp.sum(jnp.where(hits, local[None, :] + 1, 0), axis=1)]
    gather x3 -> x0, local copies, waits for them, and re-layouts: 14.1 us -> none  [the longest x1 10.3 us: body(): rows = store[incoming.reshape(-1)]]
    unnamed x23 -> x34, local copies, waits for them, and re-layouts: 1.15 us -> 13.8 us
    reshape x5 -> x1, local copies, waits for them, and re-layouts: 12.2 us -> 0.72 us  [body(): jnp.sum(jnp.where(hits, local[None, :] + 1, 0), axis=1)]
    concatenate x2 -> x0, other arithmetic: 10.8 us -> none  [the longest x1 8.35 us: sent_together_2(): both = jnp.concatenate(arrays, axis=along)]
  transfers between devices with their start and end apart: 2 -> 6, of which waited for: 2 -> 1; matrix products, arithmetic and copies ran while one was open for 17% -> 2% of each run, Pallas kernels for 0% -> 28%
where the time goes in v1:
time: 117 us; the launch traced here: 116 us
  Pallas kernels  41.1 us (35%)
  starting transfers between devices  28 us (24%)
  waiting for transfers between devices  27.2 us (23%)
  local copies, waits for them, and re-layouts  17.1 us (15%)
  other arithmetic  2.7 us (2%)
    all_to_all x1, waiting for transfers between devices, body(): lax.all_to_all(sent, 'st', split_axis=0, concat_axis=0, tiled=True)  27.2 us
    unnamed x34, local copies, waits for them, and re-layouts  13.8 us
    pallas_call x1, Pallas kernels, front(): pl.pallas_call(front_kernel, grid=(tokens // tile,), in_specs=[pl.BlockSp...  13.8 us
    all_to_all x1, starting transfers between devices, body(): lax.all_to_all(request, 'st', split_axis=0, concat_axis=0, tiled=True)  12 us
    all_to_all x1, starting transfers between devices, body(): lax.all_to_all(sent, 'st', split_axis=0, concat_axis=0, tiled=True)  9.97 us
    pallas_call x1, Pallas kernels, attend(): pl.pallas_call(functools.partial(attend_kernel, reads=reads), in_specs=[p...  8.16 us
    pallas_call x1, Pallas kernels, place(): pl.pallas_call(place_kernel, in_specs=[pl.BlockSpec(memory_space=pltpu.SM...  5.81 us
    pallas_call x1, Pallas kernels, project(): pl.pallas_call(project_kernel, grid=(rows // tile,), in_specs=[pl.BlockSp...  5.66 us
  transfers between devices with their start and end apart: 6, of which 1 were waited for; matrix products, arithmetic and copies ran while one was open for 2% of the time, Pallas kernels for 28%

profile of v1, /device:TPU:1, one launch (start us, length us, event | category | flops | bytes accessed | tf_op | source)
XLA Modules:
  0.0 116.3 jit_solution(16110660898089046035)
XLA Ops:
  0.0 0.7 sign_compare_fusion
  0.7 0.7 broadcast_remainder_fusion
  1.4 0.1 copy.29
  1.5 0.1 ne.44
  1.6 0.1 copy.30
  1.6 0.1 rem.26
  1.7 0.1 copy.31
  1.8 0.1 div.14
  1.9 0.1 select_reduce_fusion
  2.0 0.7 copy.32
  2.7 12.0 %all-to-all-start = ((s32[64,1,1]{2,1,0:T(1,128)}), s32[64,1,1]{2,1,0:T(1,128)S(1)}, u32[]{:S(2)}, u32[]{:S(2)}) async-start(s32[64,1,1]{2,1,0:T(1,128)} %copy.32), calls=%async_computation | async-start | bytes 65536 | tf_op jit(solution)/shard_map/all_to_all | solution.py:294
  14.7 0.0 copy-start.6
  14.7 2.8 %copy-done.6 = bf16[24,64,2048]{2,1,0:T(8,128)(2,1)S(1)} copy-done((bf16[24,64,2048]{2,1,0:T(8,128)(2,1)S(1)}, bf16[24,64,2048]{2,1,0:T(8,128)(2,1)}, u32[]{:S(2)}) %copy-start.6) | copy-done | bytes 6291480
  17.5 1.2 %copy-done.9 = bf16[2048,256]{1,0:T(8,128)(2,1)S(1)} copy-done((bf16[2048,256]{1,0:T(8,128)(2,1)S(1)}, bf16[2048,256]{1,0:T(8,128)(2,1)}, u32[]{:S(2)}) %copy-start.9) | copy-done | bytes 1048600
  18.7 1.2 %copy-done.10 = bf16[2048,256]{1,0:T(8,128)(2,1)S(1)} copy-done((bf16[2048,256]{1,0:T(8,128)(2,1)S(1)}, bf16[2048,256]{1,0:T(8,128)(2,1)}, u32[]{:S(2)}) %copy-start.10) | copy-done | bytes 1048600
  19.9 0.7 copy-done.13
  20.6 5.7 %project.1 = bf16[1536,512]{1,0:T(8,128)(2,1)S(1)} custom-call(bf16[1536,2048]{1,0:T(8,128)(2,1)S(1)} %bitcast.7, f32[1,2048]{1,0:T(1,128)S(1)} %bitcast.8, bf16[2048,256]{1,0:T(8,128)(2,1)S(1)} %copy-done.9, bf16[2048,256]{1,0:T(8,128)(2,1)S(1)} %copy-done.10), custom_call_target="tpu_custom_call" | custom-call | flops 3221225472 | bytes 9961472 | tf_op jit(solution)/shard_map/project/pallas_call | solution.py:48
  26.3 0.0 all-to-all-done
  26.3 1.2 %reduce.request_ref = s32[64]{0:T(128)S(1)} reduce(s32[64,1,1]{2,1,0:T(1,128)S(1)} %all-to-all-done, s32[]{:T(128)} %constant.26.clone.1), dimensions={1,2}, to_apply=%all_to_all.6.reduce_sub_computation | reduce | bytes 516 | tf_op jit(solution)/shard_map/all_to_all | solution.py:294
  27.5 5.8 %place.1 = bf16[64,64,512]{2,1,0:T(8,128)(2,1)S(1)} custom-call(s32[64]{0:T(128)S(1)} %reduce.request_ref, bf16[24,64,512]{2,1,0:T(8,128)(2,1)S(1)} %bitcast.6), custom_call_target="tpu_custom_call" | custom-call | bytes 6291456 | tf_op jit(solution)/shard_map/place/pallas_call | solution.py:92
  33.3 0.0 copy-start
  33.3 2.0 %copy-done = bf16[64,64,512]{2,1,0:T(8,128)(2,1)} copy-done((bf16[64,64,512]{2,1,0:T(8,128)(2,1)}, bf16[64,64,512]{2,1,0:T(8,128)(2,1)S(1)}, u32[]{:S(2)}) %copy-start) | copy-done | bytes 4194328
  35.3 10.0 %all-to-all-start.1 = ((bf16[64,64,512]{2,1,0:T(8,128)(2,1)}), bf16[64,64,512]{2,1,0:T(8,128)(2,1)}, u32[]{:S(2)}, u32[]{:S(2)}) async-start(bf16[64,64,512]{2,1,0:T(8,128)(2,1)} %copy-done), calls=%async_computation.1 | async-start | bytes 8388608 | tf_op jit(solution)/shard_map/all_to_all | solution.py:297
  45.3 0.0 copy-start.14
  45.3 0.0 copy-done.15
  45.3 0.0 copy-start.7
  45.3 1.2 %constant_dynamic-slice_fusion = (bf16[512,1024]{1,0:T(8,128)(2,1)}, bf16[512,1024]{1,0:T(8,128)(2,1)S(1)}) fusion(bf16[512,2048]{1,0:T(8,128)(2,1)S(1)} %copy-done.15, s32[]{:T(128)S(6)} %select_n.32, s32[]{:T(128)S(6)} %select_n.31), kind=kLoop, calls=%fused_computation.5 | loop fusion | bytes 4194312 | tf_op jit(solution)/shard_map/dynamic_slice | solution.py:303
  46.6 1.5 %collective-permute-start.3 = (bf16[512,1024]{1,0:T(8,128)(2,1)}, bf16[512,1024]{1,0:T(8,128)(2,1)S(1)}, u32[]{:S(2)}, u32[]{:S(2)}) collective-permute-start(bf16[512,1024]{1,0:T(8,128)(2,1)} %get-tuple-element.11), channel_id=1, source_target_pairs={{0,1},{1,0},{2,3},{3,2},{4,5},{5,4},{6,7},{7,6},{8,9},{9,8},{10,11... | collective-permute-start | bytes 3145736 | tf_op jit(solution)/shard_map/ppermute | solution.py:304
  48.1 0.0 copy-done.12
  48.1 0.0 copy-done.14
  48.1 1.6 %copy-done.8 = bf16[2048,512]{1,0:T(8,128)(2,1)S(1)} copy-done((bf16[2048,512]{1,0:T(8,128)(2,1)S(1)}, bf16[2048,512]{1,0:T(8,128)(2,1)}, u32[]{:S(2)}) %copy-start.8) | copy-done | bytes 2097176
  49.7 1.2 %copy-done.11 = bf16[2048,256]{1,0:T(8,128)(2,1)S(1)} copy-done((bf16[2048,256]{1,0:T(8,128)(2,1)S(1)}, bf16[2048,256]{1,0:T(8,128)(2,1)}, u32[]{:S(2)}) %copy-start.11) | copy-done | bytes 1048600
  50.9 13.8 %front.1 = (bf16[1024,512]{1,0:T(8,128)(2,1)}, bf16[1024,256]{1,0:T(8,128)(2,1)S(1)}, f32[1024,1024]{1,0:T(8,128)S(1)}) custom-call(s32[1]{0:T(128)} %bitcast.half_ref, bf16[1024,2048]{1,0:T(8,128)(2,1)S(1)} %copy-done.7, f32[1,2048]{1,0:T(1,128)S(1)} %bitcast.9, bf16[2048,512]{1,0:T(8,128)(2,1)S(1)} %copy-done.8, bf16[2048,256]{1,0:T(8,128)(2,1)S(1)} %copy-done.11, ...), custom_call_target="tpu_custom_call" | custom-call | flops 7516192768 | bytes 25165824 | tf_op jit(solution)/shard_map/front/pallas_call | solution.py:149
  64.7 2.0 %copy-done.1 = f32[1024,1024]{1,0:T(8,128)} copy-done((f32[1024,1024]{1,0:T(8,128)}, f32[1024,1024]{1,0:T(8,128)S(1)}, u32[]{:S(2)}) %copy-start.1) | copy-done | bytes 4194328
  66.7 1.3 %collective-permute-start.2 = (bf16[1024,512]{1,0:T(8,128)(2,1)}, bf16[1024,512]{1,0:T(8,128)(2,1)}, u32[]{:S(2)}, u32[]{:S(2)}) collective-permute-start(bf16[1024,512]{1,0:T(8,128)(2,1)} %get-tuple-element.9.own_ref), channel_id=1, source_target_pairs={{0,1},{1,0},{2,3},{3,2},{4,5},{5,4},{6,7},{7,6},{8,9},{9,8},{10,11... | collective-permute-start | bytes 3145736 | tf_op jit(solution)/shard_map/ppermute | solution.py:311
  68.0 0.0 copy-done.16
  68.0 0.9 constant_dynamic-slice_fusion.2
  68.9 0.1 collective-permute-start.1
  69.0 27.2 %all-to-all-done.1.kv_ref = bf16[64,64,512]{2,1,0:T(8,128)(2,1)} async-done(((bf16[64,64,512]{2,1,0:T(8,128)(2,1)}), bf16[64,64,512]{2,1,0:T(8,128)(2,1)}, u32[]{:S(2)}, u32[]{:S(2)}) %all-to-all-start.1) | async-done | bytes 4194336 | tf_op jit(solution)/shard_map/all_to_all | solution.py:297
  96.2 1.0 copy-done.4
  97.2 8.2 %attend.1.own_ref = bf16[1024,256]{1,0:T(8,128)(2,1)S(1)} custom-call(s32[32]{0:T(128)S(1)} %get-tuple-element.18.slot_ref, f32[2]{0:T(128)S(1)} %copy-done.5, bf16[1024,256]{1,0:T(8,128)(2,1)S(1)} %copy-done.4, bf16[64,64,512]{2,1,0:T(8,128)(2,1)} %all-to-all-done.1.kv_ref), custom_call_target="tpu_custom_call" | custom-call | flops 1073741824 | bytes 3145728 | tf_op jit(solution)/shard_map/attend/pallas_call | solution.py:238
  105.4 3.1 %collective-permute-start = (bf16[1024,256]{1,0:T(8,128)(2,1)S(1)}, bf16[1024,256]{1,0:T(8,128)(2,1)S(1)}, u32[]{:S(2)}, u32[]{:S(2)}) collective-permute-start(bf16[1024,256]{1,0:T(8,128)(2,1)S(1)} %attend.1.own_ref), channel_id=1, source_target_pairs={{0,1},{1,0},{2,3},{3,2},{4,5},{5,4},{6,7},{7,6},{8,9},{9,8},{10,11... | collective-permute-start | bytes 1572872 | tf_op jit(solution)/shard_map/ppermute | solution.py:313
  108.5 0.0 collective-permute-done.3.w_other_ref
  108.5 0.0 collective-permute-done.2.other_ref
  108.5 4.5 %branch.1.pool_ref = f32[1024,1024]{1,0:T(8,128)S(1)} custom-call(bf16[1024,512]{1,0:T(8,128)(2,1)} %get-tuple-element.9.own_ref, bf16[1024,512]{1,0:T(8,128)(2,1)} %collective-permute-done.2.other_ref, bf16[512,1024]{1,0:T(8,128)(2,1)S(1)} %get-tuple-element.12.w_own_ref, bf16[512,1024]{1,0:T(8,128)(2,1)S(1)} %collective-permute-done.3.w_other_ref), custom_call_target="tpu_custom_call" | custom-call | flops 2147483648 | bytes 8388608 | tf_op jit(solution)/shard_map/branch/pallas_call | solution.py:183
  113.0 0.0 collective-permute-done.1.w_other_ref
  113.0 0.0 collective-permute-done.other_ref
  113.1 3.3 %mixed.1 = bf16[1024,1024]{1,0:T(8,128)(2,1)} custom-call(bf16[1024,256]{1,0:T(8,128)(2,1)S(1)} %attend.1.own_ref, bf16[1024,256]{1,0:T(8,128)(2,1)S(1)} %collective-permute-done.other_ref, bf16[256,1024]{1,0:T(8,128)(2,1)S(1)} %get-tuple-element.14.w_own_ref, bf16[256,1024]{1,0:T(8,128)(2,1)S(1)} %collective-permute-done.1.w_other_ref, ...), custom_call_target="tpu_custom_call" | custom-call | flops 1073741824 | bytes 12582912 | tf_op jit(solution)/shard_map/mixed/pallas_call | solution.py:270
  (18 shorter events, 0.0 us)
Async XLA Ops:
  2.7 23.6 %all-to-all-start = ((s32[64,1,1]{2,1,0:T(1,128)}), s32[64,1,1]{2,1,0:T(1,128)S(1)}, u32[]{:S(2)}, u32[]{:S(2)}) async-start(s32[64,1,1]{2,1,0:T(1,128)} %copy.32), calls=%async_computation | async-start | bytes 65536 | tf_op jit(solution)/shard_map/all_to_all | solution.py:294
  14.7 2.8 %copy-start.6 = (bf16[24,64,2048]{2,1,0:T(8,128)(2,1)S(1)}, bf16[24,64,2048]{2,1,0:T(8,128)(2,1)}, u32[]{:S(2)}) copy-start(bf16[24,64,2048]{2,1,0:T(8,128)(2,1)} %param.16) | copy-start | bytes 18874372
  17.5 1.2 %copy-start.9 = (bf16[2048,256]{1,0:T(8,128)(2,1)S(1)}, bf16[2048,256]{1,0:T(8,128)(2,1)}, u32[]{:S(2)}) copy-start(bf16[2048,256]{1,0:T(8,128)(2,1)} %key_ref.1) | copy-start | bytes 3145732
  18.7 1.2 %copy-start.10 = (bf16[2048,256]{1,0:T(8,128)(2,1)S(1)}, bf16[2048,256]{1,0:T(8,128)(2,1)}, u32[]{:S(2)}) copy-start(bf16[2048,256]{1,0:T(8,128)(2,1)} %value_ref.1) | copy-start | bytes 3145732
  19.9 0.7 copy-start.13
  33.3 2.0 %copy-start = (bf16[64,64,512]{2,1,0:T(8,128)(2,1)}, bf16[64,64,512]{2,1,0:T(8,128)(2,1)S(1)}, u32[]{:S(2)}) copy-start(bf16[64,64,512]{2,1,0:T(8,128)(2,1)S(1)} %place.1) | copy-start | bytes 12582916
  35.3 10.0 %copy-start.15 = (bf16[512,2048]{1,0:T(8,128)(2,1)S(1)}, bf16[512,2048]{1,0:T(8,128)(2,1)}, u32[]{:S(2)}) copy-start(bf16[512,2048]{1,0:T(8,128)(2,1)} %param.21) | copy-start | bytes 6291460
  35.3 12.8 %copy-start.12 = (bf16[2,256,256]{2,1,0:T(8,128)(2,1)S(1)}, bf16[2,256,256]{2,1,0:T(8,128)(2,1)}, u32[]{:S(2)}) copy-start(bf16[2,256,256]{2,1,0:T(8,128)(2,1)} %mix_ref.1) | copy-start | bytes 786436
  35.3 60.8 %all-to-all-start.1 = ((bf16[64,64,512]{2,1,0:T(8,128)(2,1)}), bf16[64,64,512]{2,1,0:T(8,128)(2,1)}, u32[]{:S(2)}, u32[]{:S(2)}) async-start(bf16[64,64,512]{2,1,0:T(8,128)(2,1)} %copy-done), calls=%async_computation.1 | async-start | bytes 8388608 | tf_op jit(solution)/shard_map/all_to_all | solution.py:297
  45.3 2.8 %copy-start.14 = (f32[2048]{0:T(1024)S(1)}, f32[2048]{0:T(1024)}, u32[]{:S(2)}) copy-start(f32[2048]{0:T(1024)} %param.15) | copy-start | bytes 24580
  45.3 2.8 %copy-start.7 = (bf16[1024,2048]{1,0:T(8,128)(2,1)S(1)}, bf16[1024,2048]{1,0:T(8,128)(2,1)}, u32[]{:S(2)}) copy-start(bf16[1024,2048]{1,0:T(8,128)(2,1)} %hidden_ref.1) | copy-start | bytes 12582916
  46.6 61.9 %collective-permute-start.3 = (bf16[512,1024]{1,0:T(8,128)(2,1)}, bf16[512,1024]{1,0:T(8,128)(2,1)S(1)}, u32[]{:S(2)}, u32[]{:S(2)}) collective-permute-start(bf16[512,1024]{1,0:T(8,128)(2,1)} %get-tuple-element.11), channel_id=1, source_target_pairs={{0,1},{1,0},{2,3},{3,2},{4,5},{5,4},{6,7},{7,6},{8,9},{9,8},{10,11... | collective-permute-start | bytes 3145736 | tf_op jit(solution)/shard_map/ppermute | solution.py:304
  48.1 1.6 %copy-start.8 = (bf16[2048,512]{1,0:T(8,128)(2,1)S(1)}, bf16[2048,512]{1,0:T(8,128)(2,1)}, u32[]{:S(2)}) copy-start(bf16[2048,512]{1,0:T(8,128)(2,1)} %pool_ref.1) | copy-start | bytes 6291460
  49.7 1.2 %copy-start.11 = (bf16[2048,256]{1,0:T(8,128)(2,1)S(1)}, bf16[2048,256]{1,0:T(8,128)(2,1)}, u32[]{:S(2)}) copy-start(bf16[2048,256]{1,0:T(8,128)(2,1)} %query_ref.1) | copy-start | bytes 3145732
  50.9 17.1 %copy-start.16 = (bf16[256,2048]{1,0:T(8,128)(2,1)S(1)}, bf16[256,2048]{1,0:T(8,128)(2,1)}, u32[]{:S(2)}) copy-start(bf16[256,2048]{1,0:T(8,128)(2,1)} %param.26) | copy-start | bytes 3145732
  50.9 45.3 %copy-start.5 = (f32[2]{0:T(128)S(1)}, f32[2]{0:T(128)}, u32[]{:S(2)}) copy-start(f32[2]{0:T(128)} %sharp_ref.1) | copy-start | bytes 28
  64.7 2.0 %copy-start.1 = (f32[1024,1024]{1,0:T(8,128)}, f32[1024,1024]{1,0:T(8,128)S(1)}, u32[]{:S(2)}) copy-start(f32[1024,1024]{1,0:T(8,128)S(1)} %get-tuple-element.10.gate_ref) | copy-start | bytes 12582916
  66.7 2.2 %copy-start.3 = (bf16[1024,256]{1,0:T(8,128)(2,1)}, bf16[1024,256]{1,0:T(8,128)(2,1)S(1)}, u32[]{:S(2)}) copy-start(bf16[1024,256]{1,0:T(8,128)(2,1)S(1)} %get-tuple-element.8.query_ref) | copy-start | bytes 1572868
  66.7 41.8 %collective-permute-start.2 = (bf16[1024,512]{1,0:T(8,128)(2,1)}, bf16[1024,512]{1,0:T(8,128)(2,1)}, u32[]{:S(2)}, u32[]{:S(2)}) collective-permute-start(bf16[1024,512]{1,0:T(8,128)(2,1)} %get-tuple-element.9.own_ref), channel_id=1, source_target_pairs={{0,1},{1,0},{2,3},{3,2},{4,5},{5,4},{6,7},{7,6},{8,9},{9,8},{10,11... | collective-permute-start | bytes 3145736 | tf_op jit(solution)/shard_map/ppermute | solution.py:311
  68.9 44.2 %collective-permute-start.1 = (bf16[256,1024]{1,0:T(8,128)(2,1)}, bf16[256,1024]{1,0:T(8,128)(2,1)S(1)}, u32[]{:S(2)}, u32[]{:S(2)}) collective-permute-start(bf16[256,1024]{1,0:T(8,128)(2,1)} %get-tuple-element.13), channel_id=1, source_target_pairs={{0,1},{1,0},{2,3},{3,2},{4,5},{5,4},{6,7},{7,6},{8,9},{9,8},{10,11... | collective-permute-start | bytes 1572872 | tf_op jit(solution)/shard_map/ppermute | solution.py:304
  96.2 1.0 copy-start.4
  105.4 7.7 %collective-permute-start = (bf16[1024,256]{1,0:T(8,128)(2,1)S(1)}, bf16[1024,256]{1,0:T(8,128)(2,1)S(1)}, u32[]{:S(2)}, u32[]{:S(2)}) collective-permute-start(bf16[1024,256]{1,0:T(8,128)(2,1)S(1)} %attend.1.own_ref), channel_id=1, source_target_pairs={{0,1},{1,0},{2,3},{3,2},{4,5},{5,4},{6,7},{7,6},{8,9},{9,8},{10,11... | collective-permute-start | bytes 1572872 | tf_op jit(solution)/shard_map/ppermute | solution.py:313
  108.5 4.5 %copy-start.2 = (f32[1024,1024]{1,0:T(8,128)S(1)}, f32[1024,1024]{1,0:T(8,128)}, u32[]{:S(2)}) copy-start(f32[1024,1024]{1,0:T(8,128)} %copy-done.1) | copy-start | bytes 12582916

commit v2 on v1

v2 whole, which is shorter than its diff:
```python
import functools
import math

import jax
import jax.numpy as jnp
from jax import lax
from jax.experimental import pallas as pl
from jax.experimental.pallas import tpu as pltpu
from jax.sharding import PartitionSpec as P

F32, BF16 = jnp.float32, jnp.bfloat16
EPS = 1e-05
CARRY = 16
AHEAD = 3
SWAP = [(0, 1), (1, 0)]


def rms_norm(wide, gain):
    scale = lax.rsqrt(jnp.mean(wide * wide, axis=-1, keepdims=True) + EPS)
    return (wide * scale * gain).astype(BF16)


def dot(a, b):
    return jnp.dot(a, b, preferred_element_type=F32)


def cost(flops, bytes_accessed, transcendentals=0):
    return pl.CostEstimate(
        flops=flops, bytes_accessed=bytes_accessed, transcendentals=transcendentals
    )


def params(mib, **kw):
    return pltpu.CompilerParams(vmem_limit_bytes=mib << 20, **kw)


def owner_of(p, count):
    return lax.shift_right_logical(p * (-(-(1 << 20) // count)), 20)


def request_kernel(ids_ref, out_ref, *, count):
    holder = lax.broadcasted_iota(jnp.int32, (out_ref.shape[0], out_ref.shape[2]), 0)
    row = jnp.zeros_like(holder)
    for j in range(ids_ref.shape[0]):
        for b in range(ids_ref.shape[1]):
            p = ids_ref[j, b]
            owner = owner_of(p, count)
            row = jnp.where(holder == owner, p - owner * count + 1, row)
    out_ref[...] = row.reshape(out_ref.shape)


def requests(ids, count, holders):
    return pl.pallas_call(
        functools.partial(request_kernel, count=count),
        in_specs=[pl.BlockSpec(memory_space=pltpu.SMEM)],
        out_specs=pl.BlockSpec(memory_space=pltpu.VMEM),
        out_shape=jax.ShapeDtypeStruct((holders, 1, 128), jnp.int32),
        name="requests",
    )(ids)


def offer_kernel(
    asked_ref, store_ref, gain_ref, key_ref, value_ref, out_ref, rows, held, in_sems, out_sems
):
    count, length, width = rows.shape
    tiles = in_sems.shape[0]
    per = count // tiles
    tile = per * length
    half = key_ref.shape[1]

    def load(i):
        part = pl.ds(i * per, per)
        return pltpu.make_async_copy(store_ref.at[part], rows.at[part], in_sems.at[i])

    for i in range(min(AHEAD, tiles)):
        load(i).start()
    for i in range(tiles):
        load(i).wait()
        if i + AHEAD < tiles:
            load(i + AHEAD).start()
        part = slice(i * per, (i + 1) * per)
        normed = rms_norm(rows[part].reshape(tile, width).astype(F32), gain_ref[...])
        held[part, :, :half] = dot(normed, key_ref[...]).astype(BF16).reshape(per, length, half)
        held[part, :, half:] = dot(normed, value_ref[...]).astype(BF16).reshape(per, length, half)
    readers = out_ref.shape[0]
    asked = [asked_ref[r, 0, 0] for r in range(readers)]
    copies = [
        pltpu.make_async_copy(held.at[jnp.maximum(asked[r] - 1, 0)], out_ref.at[r], out_sems.at[r])
        for r in range(readers)
    ]
    for r in range(readers):
        pl.when(asked[r] > 0)(copies[r].start)
    for r in range(readers):
        pl.when(asked[r] > 0)(copies[r].wait)


def offer(asked, store, gain, w_key, w_value):
    count, length, width = store.shape
    readers, tiles, n = asked.shape[0], 6, 2 * w_key.shape[1]
    return pl.pallas_call(
        offer_kernel,
        in_specs=[
            pl.BlockSpec(memory_space=pltpu.SMEM),
            pl.BlockSpec(memory_space=pl.ANY),
            pl.BlockSpec(memory_space=pltpu.VMEM),
            pl.BlockSpec(memory_space=pltpu.VMEM),
            pl.BlockSpec(memory_space=pltpu.VMEM),
        ],
        out_specs=pl.BlockSpec(memory_space=pl.ANY),
        out_shape=jax.ShapeDtypeStruct((readers, length, n), BF16),
        scratch_shapes=[
            pltpu.VMEM(store.shape, BF16),
            pltpu.VMEM((count, length, n), BF16),
            pltpu.SemaphoreType.DMA((tiles,)),
            pltpu.SemaphoreType.DMA((readers,)),
        ],
        compiler_params=params(60),
        cost_estimate=cost(2 * count * length * width * n, 9 << 20),
        name="offer",
    )(asked, store, gain.reshape(1, width), w_key, w_value)


def front_kernel(
    half_ref, hidden_ref, gain_ref, pool_ref, query_ref, gate_ref, mix_ref,
    pool_out_ref, query_out_ref, gate_out_ref, carry,
):
    step = pl.program_id(0)
    tile = hidden_ref.shape[0]
    groups, dim = mix_ref.shape[0], mix_ref.shape[1]

    @pl.when(step == 0)
    def _():
        carry[...] = jnp.zeros_like(carry)

    normed = rms_norm(hidden_ref[...].astype(F32), gain_ref[...])
    pool_in = dot(normed, pool_ref[...]).astype(BF16)
    query_out_ref[...] = dot(normed, query_ref[...]).astype(BF16)
    gate_out_ref[...] = jax.nn.sigmoid(dot(normed, gate_ref[...])).astype(BF16)
    recent = jnp.concatenate([carry[...], pool_in], axis=0)
    carry[...] = pool_in[tile - CARRY :]
    shape = (tile, tile + CARRY)
    back = (
        lax.broadcasted_iota(jnp.int32, shape, 0)
        + CARRY
        - lax.broadcasted_iota(jnp.int32, shape, 1)
    )
    position = step * tile + lax.broadcasted_iota(jnp.int32, (tile, 1), 0)
    for g in range(groups):
        window = jnp.left_shift(2, half_ref[0] * groups + g)
        band = jnp.where((back >= 0) & (back < window), 1.0, 0.0).astype(BF16)
        columns = slice(g * dim, (g + 1) * dim)
        total = dot(band, recent[:, columns])
        count = jnp.minimum(position + 1, window).astype(F32)
        pooled = (total / count - pool_in[:, columns].astype(F32)).astype(BF16)
        pool_out_ref[:, columns] = dot(pooled, mix_ref[g]).astype(BF16)


def front(half, hidden, gain, w_pool, w_query, w_gate, pool_mix):
    tokens, width = hidden.shape
    tile = 256
    fixed = lambda a: pl.BlockSpec(a.shape, lambda i: (0,) * a.ndim)
    rowed = lambda n: pl.BlockSpec((tile, n), lambda i: (i, 0))
    gain = gain.reshape(1, width)
    outs = (w_pool.shape[1], w_query.shape[1], w_gate.shape[1])
    return pl.pallas_call(
        front_kernel,
        grid=(tokens // tile,),
        in_specs=[
            pl.BlockSpec(memory_space=pltpu.SMEM),
            rowed(width),
            fixed(gain),
            fixed(w_pool),
            fixed(w_query),
            fixed(w_gate),
            fixed(pool_mix),
        ],
        out_specs=[rowed(n) for n in outs],
        out_shape=[
            jax.ShapeDtypeStruct((tokens, outs[0]), BF16),
            jax.ShapeDtypeStruct((tokens, outs[1]), BF16),
            jax.ShapeDtypeStruct((tokens, outs[2]), BF16),
        ],
        scratch_shapes=[pltpu.VMEM((CARRY, outs[0]), BF16)],
        compiler_params=params(40),
        cost_estimate=cost(2 * tokens * width * sum(outs), 24 << 20, tokens * outs[2]),
        name="front",
    )(half, hidden, gain, w_pool, w_query, w_gate, pool_mix)


def branch_kernel(half_ref, own_ref, other_ref, w_own_ref, w_other_ref, out_ref, token_ref):
    token_ref[...] = jnp.zeros_like(token_ref)
    columns = half_columns(half_ref, out_ref.shape[1])
    own = dot(own_ref[...], w_own_ref[:, columns]).astype(BF16).astype(F32)
    other = dot(other_ref[...], w_other_ref[:, columns]).astype(BF16).astype(F32)
    out_ref[...] = (own + other).astype(BF16)


def branch(half, own, other, w_own, w_other):
    tokens, depth = own.shape
    width = w_own.shape[1]
    tile = 256
    return pl.pallas_call(
        branch_kernel,
        grid=(tokens // tile,),
        in_specs=[
            pl.BlockSpec(memory_space=pltpu.SMEM),
            pl.BlockSpec((tile, depth), lambda i: (i, 0)),
            pl.BlockSpec((tile, depth), lambda i: (i, 0)),
            pl.BlockSpec((depth, width), lambda i: (0, 0)),
            pl.BlockSpec((depth, width), lambda i: (0, 0)),
        ],
        out_specs=[
            pl.BlockSpec((tile, width // 2), lambda i: (i, 0)),
            pl.BlockSpec((8, 128), lambda i: (0, 0)),
        ],
        out_shape=[
            jax.ShapeDtypeStruct((tokens, width // 2), BF16),
            jax.ShapeDtypeStruct((8, 128), F32),
        ],
        compiler_params=params(24),
        cost_estimate=cost(2 * tokens * depth * width, 8 << 20),
        name="branch",
    )(half, own, other, w_own, w_other)


def attend_kernel(
    ids_ref, sharp_ref, query_hbm, kv_ref, _, out_ref,
    held, query_ref, scores_ref, weights_ref, sems, *, count
):
    reads, blocks = ids_ref.shape
    heads = sharp_ref.shape[0]
    length, half = held.shape[1], held.shape[2] // 2
    dim = half // heads
    block = query_ref.shape[0] // blocks
    copies = [
        pltpu.make_async_copy(
            kv_ref.at[owner_of(ids_ref[at % reads, at // reads], count)], held.at[at], sems.at[at]
        )
        for at in range(reads * blocks)
    ]

    def memory(b, at):
        rows = held[b * reads : (b + 1) * reads, :, at : at + dim]
        return rows.reshape(reads * length, dim)

    first = pltpu.make_async_copy(query_hbm, query_ref, sems.at[reads * blocks])
    first.start()
    for copy in copies:
        copy.start()
    first.wait()
    for b in range(blocks):
        for copy in copies[b * reads : (b + 1) * reads]:
            copy.wait()
        for h in range(heads):
            query = query_ref[b * block : (b + 1) * block, h * dim : (h + 1) * dim]
            scores_ref[b * heads + h] = lax.dot_general(
                memory(b, h * dim), query, (((1,), (1,)), ((), ())), preferred_element_type=F32
            )

    def soften(b, _):
        for h in range(heads):
            scores = scores_ref[b * heads + h] * (sharp_ref[h] / math.sqrt(dim))
            scores = jnp.exp(scores - jnp.max(scores, axis=0, keepdims=True))
            weights = scores * (1.0 / jnp.sum(scores, axis=0, keepdims=True))
            weights_ref[b * heads + h] = weights.astype(BF16)
        return 0

    lax.fori_loop(0, blocks, soften, 0)
    for b in range(blocks):
        for h in range(heads):
            read = lax.dot_general(
                weights_ref[b * heads + h], memory(b, half + h * dim), (((0,), (0,)), ((), ())),
                preferred_element_type=F32,
            )
            out_ref[b * block : (b + 1) * block, h * dim : (h + 1) * dim] = read.astype(BF16)


def attend(ids, sharpness, query, kv, behind, count):
    reads, blocks = ids.shape
    shape = (blocks * sharpness.shape[0], reads * kv.shape[1], query.shape[0] // blocks)
    return pl.pallas_call(
        functools.partial(attend_kernel, count=count),
        in_specs=[
            pl.BlockSpec(memory_space=pltpu.SMEM),
            pl.BlockSpec(memory_space=pltpu.SMEM),
            pl.BlockSpec(memory_space=pl.ANY),
            pl.BlockSpec(memory_space=pl.ANY),
            pl.BlockSpec(memory_space=pl.ANY),
        ],
        out_specs=pl.BlockSpec(memory_space=pltpu.VMEM),
        out_shape=jax.ShapeDtypeStruct(query.shape, BF16),
        scratch_shapes=[
            pltpu.VMEM((ids.size,) + kv.shape[1:], BF16),
            pltpu.VMEM(query.shape, BF16),
            pltpu.VMEM(shape, F32),
            pltpu.VMEM(shape, BF16),
            pltpu.SemaphoreType.DMA((ids.size + 1,)),
        ],
        compiler_params=params(16),
        cost_estimate=cost(1 << 30, 3 << 20, 1 << 19),
        name="attend",
    )(ids, sharpness, query, kv, behind)


def half_columns(half_ref, width):
    return pl.ds(pl.multiple_of(half_ref[0] * width, width), width)


def mixed_kernel(
    half_ref, own_ref, other_ref, w_own_ref, w_other_ref, pool_ref, gate_ref, out_ref, done, sems
):
    tile = own_ref.shape[0] // sems.shape[0]
    columns = half_columns(half_ref, done.shape[1])
    w_own, w_other = w_own_ref[:, columns], w_other_ref[:, columns]
    copies = []
    for i in range(sems.shape[0]):
        rows = slice(i * tile, (i + 1) * tile)
        own = dot(own_ref[rows], w_own).astype(BF16).astype(F32)
        read = own + dot(other_ref[rows], w_other).astype(BF16).astype(F32)
        done[rows] = (pool_ref[rows].astype(F32) + gate_ref[rows].astype(F32) * read).astype(BF16)
        part = pl.ds(i * tile, tile)
        copies.append(pltpu.make_async_copy(done.at[part], out_ref.at[part], sems.at[i]))
        copies[-1].start()
    for copy in copies:
        copy.wait()


def mix(half, own, other, w_own, w_other, pool, gate):
    tokens, depth = own.shape
    width = gate.shape[1]
    return pl.pallas_call(
        mixed_kernel,
        in_specs=[pl.BlockSpec(memory_space=pltpu.SMEM)]
        + [pl.BlockSpec(memory_space=pltpu.VMEM)] * 6,
        out_specs=pl.BlockSpec(memory_space=pl.ANY),
        out_shape=jax.ShapeDtypeStruct((tokens, width), BF16),
        scratch_shapes=[pltpu.VMEM((tokens, width), BF16), pltpu.SemaphoreType.DMA((4,))],
        compiler_params=params(24),
        cost_estimate=cost(4 * tokens * depth * width, 12 << 20),
        name="mixed",
    )(half, own, other, w_own, w_other, pool, gate)


def body(
    hidden, norm_gain, store, store_gain, passage_ids, w_pool, pool_mix, w_branch,
    w_query, w_key, w_value, sharpness, w_out, w_gate,
):
    half = lax.axis_index("tp").reshape(1)
    swapped = lambda a: lax.ppermute(a, "tp", SWAP)
    across = lambda a: lax.all_to_all(a, "st", split_axis=0, concat_axis=0, tiled=True)
    count = store.shape[0]
    ids = passage_ids.T
    asked = across(requests(ids, count, lax.axis_size("st")))
    offered = offer(asked, store, store_gain, w_key, w_value)
    kv = across(offered)
    w_branch, w_out, offered = lax.optimization_barrier((w_branch, w_out, offered))
    branch_other, out_other = swapped(w_branch), swapped(w_out)
    pool_out, query, gate = front(half, hidden, norm_gain, w_pool, w_query, w_gate, pool_mix)
    pool, token = branch(half, pool_out, swapped(pool_out), w_branch, branch_other)
    read = attend(ids, sharpness, query, kv, token, count)
    return mix(half, read, swapped(read), w_out, out_other, pool, gate)


def solution(mesh):
    placed = (
        P("st", None), P(), P("st", None, None), P(), P("st", None), P(None, "tp"),
        P("tp", None, None), P("tp", None), P(None, "tp"), P(None, "tp"), P(None, "tp"),
        P("tp"), P("tp", None), P(None, "tp"),
    )
    return jax.shard_map(body, mesh=mesh, in_specs=placed, out_specs=P("st", "tp"), check_vma=False)
```

time: 117 us -> 105 us (0.90)
  blocking collectives: 0 us -> 20.6 us
  starting transfers between devices: 28 us -> 12.9 us
  local copies, waits for them, and re-layouts: 17.1 us -> 8.17 us
  waiting for transfers between devices: 27.2 us -> 24.1 us
  Pallas kernels: 41.1 us -> 38.2 us
  other arithmetic: 2.7 us -> 0 us
    all_to_all x0 -> x1, blocking collectives: none -> 20.6 us  [body(): lax.all_to_all(a, 'st', split_axis=0, concat_axis=0, tiled=True)]
    all_to_all x2 -> x1, starting transfers between devices: 21.9 us -> 5.81 us  [body(): lax.all_to_all(a, 'st', split_axis=0, concat_axis=0, tiled=True)]
    all_to_all x2 -> x1, waiting for transfers between devices: 27.2 us -> 20.4 us  [body(): lax.all_to_all(a, 'st', split_axis=0, concat_axis=0, tiled=True)]
    unnamed x34 -> x24, local copies, waits for them, and re-layouts: 13.8 us -> 8.17 us
    ppermute x4, waiting for transfers between devices: 0.01 us -> 3.69 us  [body(): swapped = lambda a: lax.ppermute(a, 'tp', SWAP)]
    pallas_call x4, Pallas kernels: 22.9 us -> 20.3 us  [the longest x1 10.4 us: offer(): pl.pallas_call(offer_kernel, in_specs=[pl.BlockSpec(memory_space=pltpu.SM...]
    dynamic_slice x2 -> x0, local copies, waits for them, and re-layouts: 2.08 us -> none  [weights(): theirs = lax.dynamic_slice_in_dim(w, (1 - half) * columns, columns, axis=1)]
    all_to_all x1 -> x0, other arithmetic: 1.22 us -> none  [body(): lax.all_to_all(request, 'st', split_axis=0, concat_axis=0, tiled=True)]
  transfers between devices with their start and end apart: 6 -> 5, of which waited for: 1 -> 3; matrix products, arithmetic and copies ran while one was open for 2% -> 0% of each run, Pallas kernels for 28% -> 22%
where the time goes in v2:
time: 105 us; the launch traced here: 104 us
  Pallas kernels  38.2 us (36%)
  waiting for transfers between devices  24.1 us (23%)
  blocking collectives  20.6 us (20%)
  starting transfers between devices  12.9 us (12%)
  local copies, waits for them, and re-layouts  8.17 us (8%)
    all_to_all x1, blocking collectives, body(): lax.all_to_all(a, 'st', split_axis=0, concat_axis=0, tiled=True)  20.6 us
    all_to_all x1, waiting for transfers between devices, body(): lax.all_to_all(a, 'st', split_axis=0, concat_axis=0, tiled=True)  20.4 us
    pallas_call x1, Pallas kernels, front(): pl.pallas_call(front_kernel, grid=(tokens // tile,), in_specs=[pl.BlockSp...  12.8 us
    pallas_call x1, Pallas kernels, offer(): pl.pallas_call(offer_kernel, in_specs=[pl.BlockSpec(memory_space=pltpu.SM...  10.4 us
    unnamed x24, local copies, waits for them, and re-layouts  8.17 us
    ppermute x4, starting transfers between devices, body(): swapped = lambda a: lax.ppermute(a, 'tp', SWAP)  7.07 us
    all_to_all x1, starting transfers between devices, body(): lax.all_to_all(a, 'st', split_axis=0, concat_axis=0, tiled=True)  5.81 us
    pallas_call x1, Pallas kernels, branch(): pl.pallas_call(branch_kernel, grid=(tokens // tile,), in_specs=[pl.BlockS...  5.15 us
  transfers between devices with their start and end apart: 5, of which 3 were waited for; matrix products, arithmetic and copies ran while one was open for 0% of the time, Pallas kernels for 22%

profile of v2, /device:TPU:1, one launch (start us, length us, event | category | flops | bytes accessed | tf_op | source)
XLA Modules:
  0.0 104.2 jit_solution(1023719780536051663)
XLA Ops:
  0.0 1.4 %requests.1 = s32[64,1,128]{2,1,0:T(1,128)} custom-call(s32[4,8]{1,0:T(4,128)} %bitcast.4), custom_call_target="tpu_custom_call" | custom-call | tf_op jit(solution)/shard_map/requests/pallas_call | solution.py:53
  1.4 20.6 %all_to_all.10.asked_ref = s32[64,1,128]{2,1,0:T(1,128)} all-to-all(s32[64,1,128]{2,1,0:T(1,128)} %requests.1), channel_id=1, replica_groups=mesh['st'=64,'tp'=2] {'st'}, dimensions={0} | all-to-all | bytes 65536 | tf_op jit(solution)/shard_map/all_to_all | solution.py:350
  22.0 10.4 %offer.1 = bf16[64,64,512]{2,1,0:T(8,128)(2,1)} custom-call(s32[64,1,128]{2,1,0:T(1,128)} %all_to_all.10.asked_ref, bf16[24,64,2048]{2,1,0:T(8,128)(2,1)} %store_ref.1, f32[1,2048]{1,0:T(1,128)} %bitcast.7, bf16[2048,256]{1,0:T(8,128)(2,1)} %key_ref.1, bf16[2048,256]{1,0:T(8,128)(2,1)} %value_ref.1), custom_call_target="tpu_custom_call" | custom-call | flops 3221225472 | bytes 9437184 | tf_op jit(solution)/shard_map/offer/pallas_call | solution.py:100
  32.4 0.0 copy-start.10
  32.4 0.0 copy-start.11
  32.4 5.8 %all-to-all-start.1 = ((bf16[64,64,512]{2,1,0:T(8,128)(2,1)}), bf16[64,64,512]{2,1,0:T(8,128)(2,1)}, u32[]{:S(2)}, u32[]{:S(2)}) async-start(bf16[64,64,512]{2,1,0:T(8,128)(2,1)} %offer.1), calls=%async_computation.1 | async-start | bytes 8388608 | tf_op jit(solution)/shard_map/all_to_all | solution.py:350
  38.2 2.0 %collective-permute-start.1 = (bf16[512,2048]{1,0:T(8,128)(2,1)}, bf16[512,2048]{1,0:T(8,128)(2,1)}, u32[]{:S(2)}, u32[]{:S(2)}) collective-permute-start(bf16[512,2048]{1,0:T(8,128)(2,1)} %w_own_ref), channel_id=1, source_target_pairs={{0,1},{1,0},{2,3},{3,2},{4,5},{5,4},{6,7},{7,6},{8,9},{9,8},{10,11... | collective-permute-start | bytes 6291464 | tf_op jit(solution)/shard_map/ppermute | solution.py:349
  40.3 0.0 copy-done.10
  40.3 0.0 copy-done.11
  40.3 0.0 copy-start.7
  40.3 2.2 %copy-done.7 = bf16[1024,2048]{1,0:T(8,128)(2,1)S(1)} copy-done((bf16[1024,2048]{1,0:T(8,128)(2,1)S(1)}, bf16[1024,2048]{1,0:T(8,128)(2,1)}, u32[]{:S(2)}) %copy-start.7) | copy-done | bytes 4194328
  42.5 0.0 copy-start.8
  42.5 1.6 %copy-done.8 = bf16[2048,512]{1,0:T(8,128)(2,1)S(1)} copy-done((bf16[2048,512]{1,0:T(8,128)(2,1)S(1)}, bf16[2048,512]{1,0:T(8,128)(2,1)}, u32[]{:S(2)}) %copy-start.8) | copy-done | bytes 2097176
  44.1 0.0 copy-start.9
  44.1 1.2 %copy-done.9 = bf16[2048,256]{1,0:T(8,128)(2,1)S(1)} copy-done((bf16[2048,256]{1,0:T(8,128)(2,1)S(1)}, bf16[2048,256]{1,0:T(8,128)(2,1)}, u32[]{:S(2)}) %copy-start.9) | copy-done | bytes 1048600
  45.3 0.0 copy-start.2
  45.3 12.8 %front.1 = (bf16[1024,512]{1,0:T(8,128)(2,1)S(1)}, bf16[1024,256]{1,0:T(8,128)(2,1)S(1)}, bf16[1024,1024]{1,0:T(8,128)(2,1)S(1)}) custom-call(s32[1]{0:T(128)} %bitcast.half_ref, bf16[1024,2048]{1,0:T(8,128)(2,1)S(1)} %copy-done.7, f32[1,2048]{1,0:T(1,128)S(1)} %bitcast.6, bf16[2048,512]{1,0:T(8,128)(2,1)S(1)} %copy-done.8, bf16[2048,256]{1,0:T(8,128)(2,1)S(1)} %copy-done.9, ...), custom_call_target="tpu_custom_call" | custom-call | flops 7516192768 | bytes 25165824 | tf_op jit(solution)/shard_map/front/pallas_call | solution.py:165
  58.0 0.0 copy-start.3
  58.1 0.8 copy-done.3
  58.8 0.0 copy-start.5
  58.8 0.0 copy-start.6
  58.8 0.0 collective-permute-start
  58.9 0.0 copy-done.2
  58.9 0.5 collective-permute-start.3
  59.4 2.1 %collective-permute-done.other_ref = bf16[1024,512]{1,0:T(8,128)(2,1)S(1)} collective-permute-done((bf16[1024,512]{1,0:T(8,128)(2,1)S(1)}, bf16[1024,512]{1,0:T(8,128)(2,1)S(1)}, u32[]{:S(2)}, u32[]{:S(2)}) %collective-permute-start) | collective-permute-done | bytes 1048608 | tf_op jit(solution)/shard_map/ppermute | solution.py:349
  61.5 0.0 collective-permute-done.1.w_other_ref
  61.5 5.1 %branch.1 = (bf16[1024,1024]{1,0:T(8,128)(2,1)S(1)}, f32[8,128]{1,0:T(8,128)S(1)}) custom-call(s32[1]{0:T(128)} %bitcast.half_ref, bf16[1024,512]{1,0:T(8,128)(2,1)S(1)} %get-tuple-element.13.own_ref, bf16[1024,512]{1,0:T(8,128)(2,1)S(1)} %collective-permute-done.other_ref, bf16[512,2048]{1,0:T(8,128)(2,1)} %w_own_ref, ...), custom_call_target="tpu_custom_call" | custom-call | flops 2147483648 | bytes 8388608 | tf_op jit(solution)/shard_map/branch/pallas_call | solution.py:202
  66.7 0.0 copy-start
  66.7 1.3 %copy-done = bf16[1024,1024]{1,0:T(8,128)(2,1)} copy-done((bf16[1024,1024]{1,0:T(8,128)(2,1)}, bf16[1024,1024]{1,0:T(8,128)(2,1)S(1)}, u32[]{:S(2)}) %copy-start) | copy-done | bytes 2097176
  68.0 20.4 %all-to-all-done.1.kv_ref = bf16[64,64,512]{2,1,0:T(8,128)(2,1)} async-done(((bf16[64,64,512]{2,1,0:T(8,128)(2,1)}), bf16[64,64,512]{2,1,0:T(8,128)(2,1)}, u32[]{:S(2)}, u32[]{:S(2)}) %all-to-all-start.1) | async-done | bytes 4194336 | tf_op jit(solution)/shard_map/all_to_all | solution.py:350
  88.4 0.0 copy-done.5
  88.4 0.0 copy-done.6
  88.4 0.0 copy-start.4
  88.4 1.0 copy-done.4
  89.5 0.0 copy-start.1
  89.5 4.8 %attend.1.own_ref = bf16[1024,256]{1,0:T(8,128)(2,1)S(1)} custom-call(s32[4,8]{1,0:T(4,128)S(1)} %bitcast.5, f32[2]{0:T(128)S(1)} %copy-done.6, bf16[1024,256]{1,0:T(8,128)(2,1)S(1)} %copy-done.4, bf16[64,64,512]{2,1,0:T(8,128)(2,1)} %all-to-all-done.1.kv_ref, f32[8,128]{1,0:T(8,128)S(1)} %get-tuple-element.15._), custom_call_target="tpu_custom_call" | custom-call | flops 1073741824 | bytes 3145728 | tf_op jit(solution)/shard_map/attend/pallas_call | solution.py:281
  94.2 4.5 %collective-permute-start.2 = (bf16[1024,256]{1,0:T(8,128)(2,1)S(1)}, bf16[1024,256]{1,0:T(8,128)(2,1)S(1)}, u32[]{:S(2)}, u32[]{:S(2)}) collective-permute-start(bf16[1024,256]{1,0:T(8,128)(2,1)S(1)} %attend.1.own_ref), channel_id=1, source_target_pairs={{0,1},{1,0},{2,3},{3,2},{4,5},{5,4},{6,7},{7,6},{8,9},{9,8},{10,11... | collective-permute-start | bytes 1572872 | tf_op jit(solution)/shard_map/ppermute | solution.py:349
  98.7 0.0 collective-permute-done.3.w_other_ref
  98.8 1.5 %collective-permute-done.2.other_ref = bf16[1024,256]{1,0:T(8,128)(2,1)S(1)} collective-permute-done((bf16[1024,256]{1,0:T(8,128)(2,1)S(1)}, bf16[1024,256]{1,0:T(8,128)(2,1)S(1)}, u32[]{:S(2)}, u32[]{:S(2)}) %collective-permute-start.2) | collective-permute-done | bytes 524320 | tf_op jit(solution)/shard_map/ppermute | solution.py:349
  100.3 0.0 copy-done.1
  100.3 3.7 %mixed.1 = bf16[1024,1024]{1,0:T(8,128)(2,1)} custom-call(s32[1]{0:T(128)} %bitcast.half_ref, bf16[1024,256]{1,0:T(8,128)(2,1)S(1)} %attend.1.own_ref, bf16[1024,256]{1,0:T(8,128)(2,1)S(1)} %collective-permute-done.2.other_ref, bf16[256,2048]{1,0:T(8,128)(2,1)S(1)} %copy-done.2, bf16[256,2048]{1,0:T(8,128)(2,1)} %collective-permute-done.3.w_other_ref, ...), custom_call_target="tpu_custom_call" | custom-call | flops 1073741824 | bytes 12582912 | tf_op jit(solution)/shard_map/mixed/pallas_call | solution.py:331
Async XLA Ops:
  32.4 7.9 %copy-start.10 = (bf16[2,256,256]{2,1,0:T(8,128)(2,1)S(1)}, bf16[2,256,256]{2,1,0:T(8,128)(2,1)}, u32[]{:S(2)}) copy-start(bf16[2,256,256]{2,1,0:T(8,128)(2,1)} %mix_ref.1) | copy-start | bytes 786436
  32.4 7.9 %copy-start.11 = (f32[2048]{0:T(1024)S(1)}, f32[2048]{0:T(1024)}, u32[]{:S(2)}) copy-start(f32[2048]{0:T(1024)} %param.15) | copy-start | bytes 24580
  32.4 56.0 %all-to-all-start.1 = ((bf16[64,64,512]{2,1,0:T(8,128)(2,1)}), bf16[64,64,512]{2,1,0:T(8,128)(2,1)}, u32[]{:S(2)}, u32[]{:S(2)}) async-start(bf16[64,64,512]{2,1,0:T(8,128)(2,1)} %offer.1), calls=%async_computation.1 | async-start | bytes 8388608 | tf_op jit(solution)/shard_map/all_to_all | solution.py:350
  38.2 23.3 %collective-permute-start.1 = (bf16[512,2048]{1,0:T(8,128)(2,1)}, bf16[512,2048]{1,0:T(8,128)(2,1)}, u32[]{:S(2)}, u32[]{:S(2)}) collective-permute-start(bf16[512,2048]{1,0:T(8,128)(2,1)} %w_own_ref), channel_id=1, source_target_pairs={{0,1},{1,0},{2,3},{3,2},{4,5},{5,4},{6,7},{7,6},{8,9},{9,8},{10,11... | collective-permute-start | bytes 6291464 | tf_op jit(solution)/shard_map/ppermute | solution.py:349
  40.3 2.2 %copy-start.7 = (bf16[1024,2048]{1,0:T(8,128)(2,1)S(1)}, bf16[1024,2048]{1,0:T(8,128)(2,1)}, u32[]{:S(2)}) copy-start(bf16[1024,2048]{1,0:T(8,128)(2,1)} %hidden_ref.1) | copy-start | bytes 12582916
  42.5 1.6 %copy-start.8 = (bf16[2048,512]{1,0:T(8,128)(2,1)S(1)}, bf16[2048,512]{1,0:T(8,128)(2,1)}, u32[]{:S(2)}) copy-start(bf16[2048,512]{1,0:T(8,128)(2,1)} %pool_ref.1) | copy-start | bytes 6291460
  44.1 1.2 %copy-start.9 = (bf16[2048,256]{1,0:T(8,128)(2,1)S(1)}, bf16[2048,256]{1,0:T(8,128)(2,1)}, u32[]{:S(2)}) copy-start(bf16[2048,256]{1,0:T(8,128)(2,1)} %query_ref.1) | copy-start | bytes 3145732
  45.3 13.6 %copy-start.2 = (bf16[256,2048]{1,0:T(8,128)(2,1)S(1)}, bf16[256,2048]{1,0:T(8,128)(2,1)}, u32[]{:S(2)}) copy-start(bf16[256,2048]{1,0:T(8,128)(2,1)} %w_own_ref.1) | copy-start | bytes 3145732
  58.0 0.8 copy-start.3
  58.8 29.6 %copy-start.5 = (s32[8,4]{0,1:T(4,128)S(1)}, s32[8,4]{0,1:T(4,128)}, u32[]{:S(2)}) copy-start(s32[8,4]{0,1:T(4,128)} %param.18) | copy-start | bytes 388
  58.8 29.6 %copy-start.6 = (f32[2]{0:T(128)S(1)}, f32[2]{0:T(128)}, u32[]{:S(2)}) copy-start(f32[2]{0:T(128)} %sharp_ref.1) | copy-start | bytes 28
  58.8 2.7 %collective-permute-start = (bf16[1024,512]{1,0:T(8,128)(2,1)S(1)}, bf16[1024,512]{1,0:T(8,128)(2,1)S(1)}, u32[]{:S(2)}, u32[]{:S(2)}) collective-permute-start(bf16[1024,512]{1,0:T(8,128)(2,1)S(1)} %get-tuple-element.13.own_ref), channel_id=1, source_target_pairs={{0,1},{1,0},{2,3},{3,2},{4,5},{5,4},{6,7},{7,6},{8,9},{9,8},{10,11... | collective-permute-start | bytes 3145736 | tf_op jit(solution)/shard_map/ppermute | solution.py:349
  58.9 39.9 %collective-permute-start.3 = (bf16[256,2048]{1,0:T(8,128)(2,1)S(1)}, bf16[256,2048]{1,0:T(8,128)(2,1)}, u32[]{:S(2)}, u32[]{:S(2)}) collective-permute-start(bf16[256,2048]{1,0:T(8,128)(2,1)S(1)} %copy-done.2), channel_id=1, source_target_pairs={{0,1},{1,0},{2,3},{3,2},{4,5},{5,4},{6,7},{7,6},{8,9},{9,8},{10,11... | collective-permute-start | bytes 3145736 | tf_op jit(solution)/shard_map/ppermute | solution.py:349
  66.7 1.3 %copy-start = (bf16[1024,1024]{1,0:T(8,128)(2,1)}, bf16[1024,1024]{1,0:T(8,128)(2,1)S(1)}, u32[]{:S(2)}) copy-start(bf16[1024,1024]{1,0:T(8,128)(2,1)S(1)} %get-tuple-element.17.pool_ref) | copy-start | bytes 6291460
  88.4 1.0 %copy-start.4 = (bf16[1024,256]{1,0:T(8,128)(2,1)S(1)}, bf16[1024,256]{1,0:T(8,128)(2,1)}, u32[]{:S(2)}) copy-start(bf16[1024,256]{1,0:T(8,128)(2,1)} %copy-done.3) | copy-start | bytes 1572868
  89.5 10.8 %copy-start.1 = (bf16[1024,1024]{1,0:T(8,128)(2,1)S(1)}, bf16[1024,1024]{1,0:T(8,128)(2,1)}, u32[]{:S(2)}) copy-start(bf16[1024,1024]{1,0:T(8,128)(2,1)} %copy-done) | copy-start | bytes 6291460
  94.2 6.1 %collective-permute-start.2 = (bf16[1024,256]{1,0:T(8,128)(2,1)S(1)}, bf16[1024,256]{1,0:T(8,128)(2,1)S(1)}, u32[]{:S(2)}, u32[]{:S(2)}) collective-permute-start(bf16[1024,256]{1,0:T(8,128)(2,1)S(1)} %attend.1.own_ref), channel_id=1, source_target_pairs={{0,1},{1,0},{2,3},{3,2},{4,5},{5,4},{6,7},{7,6},{8,9},{9,8},{10,11... | collective-permute-start | bytes 1572872 | tf_op jit(solution)/shard_map/ppermute | solution.py:349

commit v3 on v2

--- a/solution.py
+++ b/solution.py
@@ -11,7 +11,8 @@
 F32, BF16 = jnp.float32, jnp.bfloat16
 EPS = 1e-05
 CARRY = 16
-AHEAD = 3
+STRIP = 32
+TOGETHER = 2
 SWAP = [(0, 1), (1, 0)]
 
 
@@ -60,28 +61,47 @@
 
 
 def offer_kernel(
-    asked_ref, store_ref, gain_ref, key_ref, value_ref, out_ref, rows, held, in_sems, out_sems
+    asked_hbm, store_ref, gain_hbm, key_hbm, value_hbm, out_ref,
+    rows, normed, gain_ref, w_ref, held, asked_ref, sems, out_sems,
 ):
     count, length, width = rows.shape
-    tiles = in_sems.shape[0]
-    per = count // tiles
-    tile = per * length
-    half = key_ref.shape[1]
-
-    def load(i):
-        part = pl.ds(i * per, per)
-        return pltpu.make_async_copy(store_ref.at[part], rows.at[part], in_sems.at[i])
-
-    for i in range(min(AHEAD, tiles)):
-        load(i).start()
+    tile = normed.shape[1]
+    per = tile // length
+    tiles = count // per
+    half = w_ref.shape[2]
+    loads = [
+        pltpu.make_async_copy(
+            store_ref.at[pl.ds(i * per, per)], rows.at[pl.ds(i * per, per)], sems.at[i]
+        )
+        for i in range(tiles)
+    ]
+    gain = pltpu.make_async_copy(gain_hbm, gain_ref, sems.at[tiles])
+    key = pltpu.make_async_copy(key_hbm, w_ref.at[0], sems.at[tiles + 1])
+    value = pltpu.make_async_copy(value_hbm, w_ref.at[1], sems.at[tiles + 2])
+    wanted = pltpu.make_async_copy(asked_hbm, asked_ref, sems.at[tiles + 3])
+    for copy in [gain, loads[0], key, value, *loads[1:], wanted]:
+        copy.start()
+
+    def norm(i, first, last):
+        for at in range(first, last, STRIP):
+            row = at % length
+            wide = rows[i * per + at // length, row : row + STRIP].astype(F32)
+            normed[i % 2, at : at + STRIP] = rms_norm(wide, gain_ref[...])
+
+    gain.wait()
+    loads[0].wait()
+    norm(0, 0, tile)
+    key.wait()
+    value.wait()
     for i in range(tiles):
-        load(i).wait()
-        if i + AHEAD < tiles:
-            load(i + AHEAD).start()
-        part = slice(i * per, (i + 1) * per)
-        normed = rms_norm(rows[part].reshape(tile, width).astype(F32), gain_ref[...])
-        held[part, :, :half] = dot(normed, key_ref[...]).astype(BF16).reshape(per, length, half)
-        held[part, :, half:] = dot(normed, value_ref[...]).astype(BF16).reshape(per, length, half)
+        if i + 1 < tiles:
+            loads[i + 1].wait()
+        for p in range(2):
+            if i + 1 < tiles:
+                norm(i + 1, p * tile // 2, (p + 1) * tile // 2)
+            found = dot(normed[i % 2], w_ref[p]).astype(BF16).reshape(per, length, half)
+            held[i * per : (i + 1) * per, :, p * half : (p + 1) * half] = found
+    wanted.wait()
     readers = out_ref.shape[0]
     asked = [asked_ref[r, 0, 0] for r in range(readers)]
     copies = [
@@ -96,32 +116,30 @@
 
 def offer(asked, store, gain, w_key, w_value):
     count, length, width = store.shape
-    readers, tiles, n = asked.shape[0], 6, 2 * w_key.shape[1]
+    readers, half, tile = asked.shape[0], w_key.shape[1], 256
     return pl.pallas_call(
         offer_kernel,
-        in_specs=[
-            pl.BlockSpec(memory_space=pltpu.SMEM),
-            pl.BlockSpec(memory_space=pl.ANY),
-            pl.BlockSpec(memory_space=pltpu.VMEM),
-            pl.BlockSpec(memory_space=pltpu.VMEM),
-            pl.BlockSpec(memory_space=pltpu.VMEM),
-        ],
+        in_specs=[pl.BlockSpec(memory_space=pltpu.HBM)] * 5,
         out_specs=pl.BlockSpec(memory_space=pl.ANY),
-        out_shape=jax.ShapeDtypeStruct((readers, length, n), BF16),
+        out_shape=jax.ShapeDtypeStruct((readers, length, 2 * half), BF16),
         scratch_shapes=[
             pltpu.VMEM(store.shape, BF16),
-            pltpu.VMEM((count, length, n), BF16),
-            pltpu.SemaphoreType.DMA((tiles,)),
+            pltpu.VMEM((2, tile, width), BF16),
+            pltpu.VMEM((1, width), F32),
+            pltpu.VMEM((2, width, half), BF16),
+            pltpu.VMEM((count, length, 2 * half), BF16),
+            pltpu.SMEM(asked.shape, jnp.int32),
+            pltpu.SemaphoreType.DMA((count * length // tile + 4,)),
             pltpu.SemaphoreType.DMA((readers,)),
         ],
         compiler_params=params(60),
-        cost_estimate=cost(2 * count * length * width * n, 9 << 20),
+        cost_estimate=cost(4 * count * length * width * half, 9 << 20),
         name="offer",
     )(asked, store, gain.reshape(1, width), w_key, w_value)
 
 
 def front_kernel(
-    half_ref, hidden_ref, gain_ref, pool_ref, query_ref, gate_ref, mix_ref,
+    hidden_ref, gain_ref, pool_ref, query_ref, gate_ref, mix_ref,
     pool_out_ref, query_out_ref, gate_out_ref, carry,
 ):
     step = pl.program_id(0)
@@ -146,7 +164,7 @@
     )
     position = step * tile + lax.broadcasted_iota(jnp.int32, (tile, 1), 0)
     for g in range(groups):
-        window = jnp.left_shift(2, half_ref[0] * groups + g)
+        window = jnp.left_shift(2, lax.axis_index("tp") * groups + g)
         band = jnp.where((back >= 0) & (back < window), 1.0, 0.0).astype(BF16)
         columns = slice(g * dim, (g + 1) * dim)
         total = dot(band, recent[:, columns])
@@ -155,7 +173,7 @@
         pool_out_ref[:, columns] = dot(pooled, mix_ref[g]).astype(BF16)
 
 
-def front(half, hidden, gain, w_pool, w_query, w_gate, pool_mix):
+def front(hidden, gain, w_pool, w_query, w_gate, pool_mix):
     tokens, width = hidden.shape
     tile = 256
     fixed = lambda a: pl.BlockSpec(a.shape, lambda i: (0,) * a.ndim)
@@ -166,7 +184,6 @@
         front_kernel,
         grid=(tokens // tile,),
         in_specs=[
-            pl.BlockSpec(memory_space=pltpu.SMEM),
             rowed(width),
             fixed(gain),
             fixed(w_pool),
@@ -184,18 +201,22 @@
         compiler_params=params(40),
         cost_estimate=cost(2 * tokens * width * sum(outs), 24 << 20, tokens * outs[2]),
         name="front",
-    )(half, hidden, gain, w_pool, w_query, w_gate, pool_mix)
-
-
-def branch_kernel(half_ref, own_ref, other_ref, w_own_ref, w_other_ref, out_ref, token_ref):
+    )(hidden, gain, w_pool, w_query, w_gate, pool_mix)
+
+
+def half_columns(width):
+    return pl.ds(pl.multiple_of(lax.axis_index("tp") * width, width), width)
+
+
+def branch_kernel(own_ref, other_ref, w_own_ref, w_other_ref, out_ref, token_ref):
     token_ref[...] = jnp.zeros_like(token_ref)
-    columns = half_columns(half_ref, out_ref.shape[1])
+    columns = half_columns(out_ref.shape[1])
     own = dot(own_ref[...], w_own_ref[:, columns]).astype(BF16).astype(F32)
     other = dot(other_ref[...], w_other_ref[:, columns]).astype(BF16).astype(F32)
     out_ref[...] = (own + other).astype(BF16)
 
 
-def branch(half, own, other, w_own, w_other):
+def branch(own, other, w_own, w_other):
     tokens, depth = own.shape
     width = w_own.shape[1]
     tile = 256
@@ -203,7 +224,6 @@
         branch_kernel,
         grid=(tokens // tile,),
         in_specs=[
-            pl.BlockSpec(memory_space=pltpu.SMEM),
             pl.BlockSpec((tile, depth), lambda i: (i, 0)),
             pl.BlockSpec((tile, depth), lambda i: (i, 0)),
             pl.BlockSpec((depth, width), lambda i: (0, 0)),
@@ -220,7 +240,7 @@
         compiler_params=params(24),
         cost_estimate=cost(2 * tokens * depth * width, 8 << 20),
         name="branch",
-    )(half, own, other, w_own, w_other)
+    )(own, other, w_own, w_other)
 
 
 def attend_kernel(
@@ -243,12 +263,7 @@
         rows = held[b * reads : (b + 1) * reads, :, at : at + dim]
         return rows.reshape(reads * length, dim)
 
-    first = pltpu.make_async_copy(query_hbm, query_ref, sems.at[reads * blocks])
-    first.start()
-    for copy in copies:
-        copy.start()
-    first.wait()
-    for b in range(blocks):
+    def score(b):
         for copy in copies[b * reads : (b + 1) * reads]:
             copy.wait()
         for h in range(heads):
@@ -257,22 +272,32 @@
                 memory(b, h * dim), query, (((1,), (1,)), ((), ())), preferred_element_type=F32
             )
 
-    def soften(b, _):
+    def soften(b):
         for h in range(heads):
             scores = scores_ref[b * heads + h] * (sharp_ref[h] / math.sqrt(dim))
             scores = jnp.exp(scores - jnp.max(scores, axis=0, keepdims=True))
             weights = scores * (1.0 / jnp.sum(scores, axis=0, keepdims=True))
             weights_ref[b * heads + h] = weights.astype(BF16)
-        return 0
-
-    lax.fori_loop(0, blocks, soften, 0)
-    for b in range(blocks):
+
+    def read(b):
         for h in range(heads):
-            read = lax.dot_general(
+            found = lax.dot_general(
                 weights_ref[b * heads + h], memory(b, half + h * dim), (((0,), (0,)), ((), ())),
                 preferred_element_type=F32,
             )
-            out_ref[b * block : (b + 1) * block, h * dim : (h + 1) * dim] = read.astype(BF16)
+            out_ref[b * block : (b + 1) * block, h * dim : (h + 1) * dim] = found.astype(BF16)
+
+    first = pltpu.make_async_copy(query_hbm, query_ref, sems.at[reads * blocks])
+    first.start()
+    for copy in copies:
+        copy.start()
+    first.wait()
+    rounds = blocks // TOGETHER
+    for i in range(rounds + 2):
+        for delay, act in enumerate((score, soften, read)):
+            if 0 <= i - delay < rounds:
+                for b in range(TOGETHER):
+                    act((i - delay) * TOGETHER + b)
 
 
 def attend(ids, sharpness, query, kv, behind, count):
@@ -283,8 +308,8 @@
         in_specs=[
             pl.BlockSpec(memory_space=pltpu.SMEM),
             pl.BlockSpec(memory_space=pltpu.SMEM),
-            pl.BlockSpec(memory_space=pl.ANY),
-            pl.BlockSpec(memory_space=pl.ANY),
+            pl.BlockSpec(memory_space=pltpu.HBM),
+            pl.BlockSpec(memory_space=pltpu.HBM),
             pl.BlockSpec(memory_space=pl.ANY),
         ],
         out_specs=pl.BlockSpec(memory_space=pltpu.VMEM),
@@ -302,22 +327,46 @@
     )(ids, sharpness, query, kv, behind)
 
 
-def half_columns(half_ref, width):
-    return pl.ds(pl.multiple_of(half_ref[0] * width, width), width)
-
-
-def mixed_kernel(
-    half_ref, own_ref, other_ref, w_own_ref, w_other_ref, pool_ref, gate_ref, out_ref, done, sems
+def own_kernel(
+    own_ref, w_own_ref, w_other_ref, pool_ref, gate_ref, out_ref, columns_ref, sem
 ):
-    tile = own_ref.shape[0] // sems.shape[0]
-    columns = half_columns(half_ref, done.shape[1])
-    w_own, w_other = w_own_ref[:, columns], w_other_ref[:, columns]
+    columns = half_columns(gate_ref.shape[1])
+    copy = pltpu.make_async_copy(w_other_ref.at[:, columns], columns_ref, sem)
+    copy.start()
+    tile = own_ref.shape[0] // 4
+    for i in range(4):
+        rows = slice(i * tile, (i + 1) * tile)
+        own = dot(own_ref[rows], w_own_ref[:, columns]).astype(BF16).astype(F32)
+        out_ref[rows] = pool_ref[rows].astype(F32) + gate_ref[rows].astype(F32) * own
+    copy.wait()
+
+
+def own_part(own, w_own, w_other, pool, gate):
+    tokens, depth = own.shape
+    width = gate.shape[1]
+    vmem = pl.BlockSpec(memory_space=pltpu.VMEM)
+    return pl.pallas_call(
+        own_kernel,
+        in_specs=[vmem, vmem, pl.BlockSpec(memory_space=pl.ANY), vmem, vmem],
+        out_specs=[vmem, vmem],
+        out_shape=[
+            jax.ShapeDtypeStruct((tokens, width), F32),
+            jax.ShapeDtypeStruct((depth, width), BF16),
+        ],
+        scratch_shapes=[pltpu.SemaphoreType.DMA],
+        compiler_params=params(16),
+        cost_estimate=cost(2 * tokens * depth * width, 12 << 20),
+        name="own_part",
+    )(own, w_own, w_other, pool, gate)
+
+
+def mixed_kernel(other_ref, w_ref, sum_ref, gate_ref, out_ref, done, sems):
+    tile = other_ref.shape[0] // sems.shape[0]
     copies = []
     for i in range(sems.shape[0]):
         rows = slice(i * tile, (i + 1) * tile)
-        own = dot(own_ref[rows], w_own).astype(BF16).astype(F32)
-        read = own + dot(other_ref[rows], w_other).astype(BF16).astype(F32)
-        done[rows] = (pool_ref[rows].astype(F32) + gate_ref[rows].astype(F32) * read).astype(BF16)
+        other = dot(other_ref[rows], w_ref[...]).astype(BF16).astype(F32)
+        done[rows] = (sum_ref[rows] + gate_ref[rows].astype(F32) * other).astype(BF16)
         part = pl.ds(i * tile, tile)
         copies.append(pltpu.make_async_copy(done.at[part], out_ref.at[part], sems.at[i]))
         copies[-1].start()
@@ -325,27 +374,25 @@
         copy.wait()
 
 
-def mix(half, own, other, w_own, w_other, pool, gate):
-    tokens, depth = own.shape
+def mix(other, w_other, summed, gate):
+    tokens, depth = other.shape
     width = gate.shape[1]
     return pl.pallas_call(
         mixed_kernel,
-        in_specs=[pl.BlockSpec(memory_space=pltpu.SMEM)]
-        + [pl.BlockSpec(memory_space=pltpu.VMEM)] * 6,
+        in_specs=[pl.BlockSpec(memory_space=pltpu.VMEM)] * 4,
         out_specs=pl.BlockSpec(memory_space=pl.ANY),
         out_shape=jax.ShapeDtypeStruct((tokens, width), BF16),
-        scratch_shapes=[pltpu.VMEM((tokens, width), BF16), pltpu.SemaphoreType.DMA((4,))],
+        scratch_shapes=[pltpu.VMEM((tokens, width), BF16), pltpu.SemaphoreType.DMA((8,))],
         compiler_params=params(24),
-        cost_estimate=cost(4 * tokens * depth * width, 12 << 20),
+        cost_estimate=cost(2 * tokens * depth * width, 12 << 20),
         name="mixed",
-    )(half, own, other, w_own, w_other, pool, gate)
+    )(other, w_other, summed, gate)
 
 
 def body(
     hidden, norm_gain, store, store_gain, passage_ids, w_pool, pool_mix, w_branch,
     w_query, w_key, w_value, sharpness, w_out, w_gate,
 ):
-    half = lax.axis_index("tp").reshape(1)
     swapped = lambda a: lax.ppermute(a, "tp", SWAP)
     across = lambda a: lax.all_to_all(a, "st", split_axis=0, concat_axis=0, tiled=True)
     count = store.shape[0]
@@ -355,10 +402,11 @@
     kv = across(offered)
     w_branch, w_out, offered = lax.optimization_barrier((w_branch, w_out, offered))
     branch_other, out_other = swapped(w_branch), swapped(w_out)
-    pool_out, query, gate = front(half, hidden, norm_gain, w_pool, w_query, w_gate, pool_mix)
-    pool, token = branch(half, pool_out, swapped(pool_out), w_branch, branch_other)
+    pool_out, query, gate = front(hidden, norm_gain, w_pool, w_query, w_gate, pool_mix)
+    pool, token = branch(pool_out, swapped(pool_out), w_branch, branch_other)
     read = attend(ids, sharpness, query, kv, token, count)
-    return mix(half, read, swapped(read), w_out, out_other, pool, gate)
+    summed, columns = own_part(read, w_out, out_other, pool, gate)
+    return mix(swapped(read), columns, summed, gate)
 
 
 def solution(mesh):

time: 105 us -> 102 us (0.971)
  Pallas kernels: 38.2 us -> 36.1 us
    ppermute x4, waiting for transfers between devices: 3.69 us -> 2.15 us  [body(): swapped = lambda a: lax.ppermute(a, 'tp', SWAP)]
    pallas_call x3 -> x4, Pallas kernels: 26.8 us -> 26.1 us  [the longest x1 12.8 us: front(): pl.pallas_call(front_kernel, grid=(tokens // tile,), in_specs=[rowed(widt...]
  transfers between devices with their start and end apart: 5 -> 5, of which waited for: 3 -> 2; matrix products, arithmetic and copies ran while one was open for 0% -> 0% of each run, Pallas kernels for 22% -> 23%
where the time goes in v3:
time: 102 us; the launch traced here: 101 us
  Pallas kernels  36.1 us (35%)
  waiting for transfers between devices  23.2 us (23%)
  blocking collectives  20.6 us (20%)
  starting transfers between devices  12.9 us (13%)
  local copies, waits for them, and re-layouts  8.32 us (8%)
    all_to_all x1, waiting for transfers between devices, body(): lax.all_to_all(a, 'st', split_axis=0, concat_axis=0, tiled=True)  21.1 us
    all_to_all x1, blocking collectives, body(): lax.all_to_all(a, 'st', split_axis=0, concat_axis=0, tiled=True)  20.6 us
    pallas_call x1, Pallas kernels, front(): pl.pallas_call(front_kernel, grid=(tokens // tile,), in_specs=[rowed(widt...  12.8 us
    pallas_call x1, Pallas kernels, offer(): pl.pallas_call(offer_kernel, in_specs=[pl.BlockSpec(memory_space=pltpu.HB...  9.56 us
    unnamed x24, local copies, waits for them, and re-layouts  8.32 us
    ppermute x4, starting transfers between devices, body(): swapped = lambda a: lax.ppermute(a, 'tp', SWAP)  7.07 us
    all_to_all x1, starting transfers between devices, body(): lax.all_to_all(a, 'st', split_axis=0, concat_axis=0, tiled=True)  5.8 us
    pallas_call x1, Pallas kernels, branch(): pl.pallas_call(branch_kernel, grid=(tokens // tile,), in_specs=[pl.BlockS...  4.52 us
  transfers between devices with their start and end apart: 5, of which 2 were waited for; matrix products, arithmetic and copies ran while one was open for 0% of the time, Pallas kernels for 23%

profile of v3, /device:TPU:1, one launch (start us, length us, event | category | flops | bytes accessed | tf_op | source)
XLA Modules:
  0.0 101.4 jit_solution(7944289007393407598)
XLA Ops:
  0.0 1.4 %requests.1 = s32[64,1,128]{2,1,0:T(1,128)} custom-call(s32[4,8]{1,0:T(4,128)} %bitcast.3), custom_call_target="tpu_custom_call" | custom-call | tf_op jit(solution)/shard_map/requests/pallas_call | solution.py:54
  1.4 20.6 %all_to_all.10.asked_hbm = s32[64,1,128]{2,1,0:T(1,128)} all-to-all(s32[64,1,128]{2,1,0:T(1,128)} %requests.1), channel_id=1, replica_groups=mesh['st'=64,'tp'=2] {'st'}, dimensions={0} | all-to-all | bytes 65536 | tf_op jit(solution)/shard_map/all_to_all | solution.py:397
  22.0 9.6 %offer.1 = bf16[64,64,512]{2,1,0:T(8,128)(2,1)} custom-call(s32[64,1,128]{2,1,0:T(1,128)} %all_to_all.10.asked_hbm, bf16[24,64,2048]{2,1,0:T(8,128)(2,1)} %store_ref.1, f32[1,2048]{1,0:T(1,128)} %bitcast.6, bf16[2048,256]{1,0:T(8,128)(2,1)} %key_hbm.1, bf16[2048,256]{1,0:T(8,128)(2,1)} %value_hbm.1), custom_call_target="tpu_custom_call" | custom-call | flops 3221225472 | bytes 9437184 | tf_op jit(solution)/shard_map/offer/pallas_call | solution.py:120
  31.6 0.0 copy-start.10
  31.6 0.0 copy-start.11
  31.6 5.8 %all-to-all-start.1 = ((bf16[64,64,512]{2,1,0:T(8,128)(2,1)}), bf16[64,64,512]{2,1,0:T(8,128)(2,1)}, u32[]{:S(2)}, u32[]{:S(2)}) async-start(bf16[64,64,512]{2,1,0:T(8,128)(2,1)} %offer.1), calls=%async_computation.1 | async-start | bytes 8388608 | tf_op jit(solution)/shard_map/all_to_all | solution.py:397
  37.4 2.0 %collective-permute-start.1 = (bf16[512,2048]{1,0:T(8,128)(2,1)}, bf16[512,2048]{1,0:T(8,128)(2,1)S(1)}, u32[]{:S(2)}, u32[]{:S(2)}) collective-permute-start(bf16[512,2048]{1,0:T(8,128)(2,1)} %w_own_ref), channel_id=1, source_target_pairs={{0,1},{1,0},{2,3},{3,2},{4,5},{5,4},{6,7},{7,6},{8,9},{9,8},{10,11... | collective-permute-start | bytes 6291464 | tf_op jit(solution)/shard_map/ppermute | solution.py:396
  39.4 0.0 copy-done.10
  39.4 0.0 copy-done.11
  39.4 0.0 copy-start.7
  39.4 2.2 %copy-done.7 = bf16[1024,2048]{1,0:T(8,128)(2,1)S(1)} copy-done((bf16[1024,2048]{1,0:T(8,128)(2,1)S(1)}, bf16[1024,2048]{1,0:T(8,128)(2,1)}, u32[]{:S(2)}) %copy-start.7) | copy-done | bytes 4194328
  41.6 0.0 copy-start.8
  41.6 1.6 %copy-done.8 = bf16[2048,512]{1,0:T(8,128)(2,1)S(1)} copy-done((bf16[2048,512]{1,0:T(8,128)(2,1)S(1)}, bf16[2048,512]{1,0:T(8,128)(2,1)}, u32[]{:S(2)}) %copy-start.8) | copy-done | bytes 2097176
  43.2 0.0 copy-start.9
  43.2 1.2 %copy-done.9 = bf16[2048,256]{1,0:T(8,128)(2,1)S(1)} copy-done((bf16[2048,256]{1,0:T(8,128)(2,1)S(1)}, bf16[2048,256]{1,0:T(8,128)(2,1)}, u32[]{:S(2)}) %copy-start.9) | copy-done | bytes 1048600
  44.4 0.0 copy-start.2
  44.4 12.8 %front.1 = (bf16[1024,512]{1,0:T(8,128)(2,1)S(1)}, bf16[1024,256]{1,0:T(8,128)(2,1)S(1)}, bf16[1024,1024]{1,0:T(8,128)(2,1)S(1)}) custom-call(bf16[1024,2048]{1,0:T(8,128)(2,1)S(1)} %copy-done.7, f32[1,2048]{1,0:T(1,128)S(1)} %bitcast.5, bf16[2048,512]{1,0:T(8,128)(2,1)S(1)} %copy-done.8, bf16[2048,256]{1,0:T(8,128)(2,1)S(1)} %copy-done.9, ...), custom_call_target="tpu_custom_call" | custom-call | flops 7516192768 | bytes 25165824 | tf_op jit(solution)/shard_map/front/pallas_call | solution.py:183
  57.2 0.0 copy-start.3
  57.2 0.8 copy-done.3
  58.0 0.0 copy-start.5
  58.0 0.0 copy-start.6
  58.0 0.0 collective-permute-start
  58.1 0.0 copy-done.2
  58.1 0.5 collective-permute-start.3
  58.5 2.1 %collective-permute-done.other_ref = bf16[1024,512]{1,0:T(8,128)(2,1)S(1)} collective-permute-done((bf16[1024,512]{1,0:T(8,128)(2,1)S(1)}, bf16[1024,512]{1,0:T(8,128)(2,1)S(1)}, u32[]{:S(2)}, u32[]{:S(2)}) %collective-permute-start) | collective-permute-done | bytes 1048608 | tf_op jit(solution)/shard_map/ppermute | solution.py:396
  60.7 0.0 collective-permute-done.1.w_other_ref
  60.7 4.5 %branch.1 = (bf16[1024,1024]{1,0:T(8,128)(2,1)S(1)}, f32[8,128]{1,0:T(8,128)S(1)}) custom-call(bf16[1024,512]{1,0:T(8,128)(2,1)S(1)} %get-tuple-element.15.own_ref, bf16[1024,512]{1,0:T(8,128)(2,1)S(1)} %collective-permute-done.other_ref, bf16[512,2048]{1,0:T(8,128)(2,1)} %w_own_ref, bf16[512,2048]{1,0:T(8,128)(2,1)S(1)} %collective-permute-done.1.w_other_ref), custom_call_target="tpu_custom_call" | custom-call | flops 2147483648 | bytes 8388608 | tf_op jit(solution)/shard_map/branch/pallas_call | solution.py:223
  65.2 0.0 copy-start
  65.2 1.3 %copy-done = bf16[1024,1024]{1,0:T(8,128)(2,1)} copy-done((bf16[1024,1024]{1,0:T(8,128)(2,1)}, bf16[1024,1024]{1,0:T(8,128)(2,1)S(1)}, u32[]{:S(2)}) %copy-start) | copy-done | bytes 2097176
  66.5 21.1 %all-to-all-done.1.kv_ref = bf16[64,64,512]{2,1,0:T(8,128)(2,1)} async-done(((bf16[64,64,512]{2,1,0:T(8,128)(2,1)}), bf16[64,64,512]{2,1,0:T(8,128)(2,1)}, u32[]{:S(2)}, u32[]{:S(2)}) %all-to-all-start.1) | async-done | bytes 4194336 | tf_op jit(solution)/shard_map/all_to_all | solution.py:397
  87.6 0.0 copy-start.1
  87.6 0.0 copy-done.5
  87.6 0.0 copy-done.6
  87.6 0.0 copy-start.4
  87.6 1.2 %copy-done.4 = bf16[1024,256]{1,0:T(8,128)(2,1)S(1)} copy-done((bf16[1024,256]{1,0:T(8,128)(2,1)S(1)}, bf16[1024,256]{1,0:T(8,128)(2,1)}, u32[]{:S(2)}) %copy-start.4) | copy-done | bytes 524312
  88.8 4.1 %attend.1.own_ref = bf16[1024,256]{1,0:T(8,128)(2,1)S(1)} custom-call(s32[4,8]{1,0:T(4,128)S(1)} %bitcast.4, f32[2]{0:T(128)S(1)} %copy-done.6, bf16[1024,256]{1,0:T(8,128)(2,1)S(1)} %copy-done.4, bf16[64,64,512]{2,1,0:T(8,128)(2,1)} %all-to-all-done.1.kv_ref, f32[8,128]{1,0:T(8,128)S(1)} %get-tuple-element.17._), custom_call_target="tpu_custom_call" | custom-call | flops 1073741824 | bytes 3145728 | tf_op jit(solution)/shard_map/attend/pallas_call | solution.py:306
  92.9 4.5 %collective-permute-start.2 = (bf16[1024,256]{1,0:T(8,128)(2,1)S(1)}, bf16[1024,256]{1,0:T(8,128)(2,1)S(1)}, u32[]{:S(2)}, u32[]{:S(2)}) collective-permute-start(bf16[1024,256]{1,0:T(8,128)(2,1)S(1)} %attend.1.own_ref), channel_id=1, source_target_pairs={{0,1},{1,0},{2,3},{3,2},{4,5},{5,4},{6,7},{7,6},{8,9},{9,8},{10,11... | collective-permute-start | bytes 1572872 | tf_op jit(solution)/shard_map/ppermute | solution.py:396
  97.4 0.0 collective-permute-done.3.w_other_ref
  97.4 0.0 copy-done.1
  97.4 1.8 %own_part.1 = (f32[1024,1024]{1,0:T(8,128)S(1)}, bf16[256,1024]{1,0:T(8,128)(2,1)S(1)}) custom-call(bf16[1024,256]{1,0:T(8,128)(2,1)S(1)} %attend.1.own_ref, bf16[256,2048]{1,0:T(8,128)(2,1)S(1)} %copy-done.2, bf16[256,2048]{1,0:T(8,128)(2,1)} %collective-permute-done.3.w_other_ref, bf16[1024,1024]{1,0:T(8,128)(2,1)S(1)} %copy-done.1, ...), custom_call_target="tpu_custom_call" | custom-call | flops 536870912 | bytes 12582912 | tf_op jit(solution)/shard_map/own_part/pallas_call | solution.py:348
  99.3 0.0 collective-permute-done.2.other_ref
  99.3 1.9 %mixed.1 = bf16[1024,1024]{1,0:T(8,128)(2,1)} custom-call(bf16[1024,256]{1,0:T(8,128)(2,1)S(1)} %collective-permute-done.2.other_ref, bf16[256,1024]{1,0:T(8,128)(2,1)S(1)} %get-tuple-element.21.w_ref, f32[1024,1024]{1,0:T(8,128)S(1)} %get-tuple-element.22.sum_ref, bf16[1024,1024]{1,0:T(8,128)(2,1)S(1)} %get-tuple-element.20.gate_ref), custom_call_target="tpu_custom_call" | custom-call | flops 536870912 | bytes 12582912 | tf_op jit(solution)/shard_map/mixed/pallas_call | solution.py:380
Async XLA Ops:
  31.6 7.9 %copy-start.10 = (bf16[2,256,256]{2,1,0:T(8,128)(2,1)S(1)}, bf16[2,256,256]{2,1,0:T(8,128)(2,1)}, u32[]{:S(2)}) copy-start(bf16[2,256,256]{2,1,0:T(8,128)(2,1)} %mix_ref.1) | copy-start | bytes 786436
  31.6 7.9 %copy-start.11 = (f32[2048]{0:T(1024)S(1)}, f32[2048]{0:T(1024)}, u32[]{:S(2)}) copy-start(f32[2048]{0:T(1024)} %param.15) | copy-start | bytes 24580
  31.6 56.0 %all-to-all-start.1 = ((bf16[64,64,512]{2,1,0:T(8,128)(2,1)}), bf16[64,64,512]{2,1,0:T(8,128)(2,1)}, u32[]{:S(2)}, u32[]{:S(2)}) async-start(bf16[64,64,512]{2,1,0:T(8,128)(2,1)} %offer.1), calls=%async_computation.1 | async-start | bytes 8388608 | tf_op jit(solution)/shard_map/all_to_all | solution.py:397
  37.4 23.3 %collective-permute-start.1 = (bf16[512,2048]{1,0:T(8,128)(2,1)}, bf16[512,2048]{1,0:T(8,128)(2,1)S(1)}, u32[]{:S(2)}, u32[]{:S(2)}) collective-permute-start(bf16[512,2048]{1,0:T(8,128)(2,1)} %w_own_ref), channel_id=1, source_target_pairs={{0,1},{1,0},{2,3},{3,2},{4,5},{5,4},{6,7},{7,6},{8,9},{9,8},{10,11... | collective-permute-start | bytes 6291464 | tf_op jit(solution)/shard_map/ppermute | solution.py:396
  39.4 2.2 %copy-start.7 = (bf16[1024,2048]{1,0:T(8,128)(2,1)S(1)}, bf16[1024,2048]{1,0:T(8,128)(2,1)}, u32[]{:S(2)}) copy-start(bf16[1024,2048]{1,0:T(8,128)(2,1)} %hidden_ref.1) | copy-start | bytes 12582916
  41.6 1.6 %copy-start.8 = (bf16[2048,512]{1,0:T(8,128)(2,1)S(1)}, bf16[2048,512]{1,0:T(8,128)(2,1)}, u32[]{:S(2)}) copy-start(bf16[2048,512]{1,0:T(8,128)(2,1)} %pool_ref.1) | copy-start | bytes 6291460
  43.2 1.2 %copy-start.9 = (bf16[2048,256]{1,0:T(8,128)(2,1)S(1)}, bf16[2048,256]{1,0:T(8,128)(2,1)}, u32[]{:S(2)}) copy-start(bf16[2048,256]{1,0:T(8,128)(2,1)} %query_ref.1) | copy-start | bytes 3145732
  44.4 13.6 %copy-start.2 = (bf16[256,2048]{1,0:T(8,128)(2,1)S(1)}, bf16[256,2048]{1,0:T(8,128)(2,1)}, u32[]{:S(2)}) copy-start(bf16[256,2048]{1,0:T(8,128)(2,1)} %w_own_ref.1) | copy-start | bytes 3145732
  57.2 0.8 copy-start.3
  58.0 29.6 %copy-start.5 = (s32[8,4]{0,1:T(4,128)S(1)}, s32[8,4]{0,1:T(4,128)}, u32[]{:S(2)}) copy-start(s32[8,4]{0,1:T(4,128)} %param.18) | copy-start | bytes 388
  58.0 29.6 %copy-start.6 = (f32[2]{0:T(128)S(1)}, f32[2]{0:T(128)}, u32[]{:S(2)}) copy-start(f32[2]{0:T(128)} %sharp_ref.1) | copy-start | bytes 28
  58.0 2.7 %collective-permute-start = (bf16[1024,512]{1,0:T(8,128)(2,1)S(1)}, bf16[1024,512]{1,0:T(8,128)(2,1)S(1)}, u32[]{:S(2)}, u32[]{:S(2)}) collective-permute-start(bf16[1024,512]{1,0:T(8,128)(2,1)S(1)} %get-tuple-element.15.own_ref), channel_id=1, source_target_pairs={{0,1},{1,0},{2,3},{3,2},{4,5},{5,4},{6,7},{7,6},{8,9},{9,8},{10,11... | collective-permute-start | bytes 3145736 | tf_op jit(solution)/shard_map/ppermute | solution.py:396
  58.1 39.4 %collective-permute-start.3 = (bf16[256,2048]{1,0:T(8,128)(2,1)S(1)}, bf16[256,2048]{1,0:T(8,128)(2,1)}, u32[]{:S(2)}, u32[]{:S(2)}) collective-permute-start(bf16[256,2048]{1,0:T(8,128)(2,1)S(1)} %copy-done.2), channel_id=1, source_target_pairs={{0,1},{1,0},{2,3},{3,2},{4,5},{5,4},{6,7},{7,6},{8,9},{9,8},{10,11... | collective-permute-start | bytes 3145736 | tf_op jit(solution)/shard_map/ppermute | solution.py:396
  65.2 1.3 %copy-start = (bf16[1024,1024]{1,0:T(8,128)(2,1)}, bf16[1024,1024]{1,0:T(8,128)(2,1)S(1)}, u32[]{:S(2)}) copy-start(bf16[1024,1024]{1,0:T(8,128)(2,1)S(1)} %get-tuple-element.19.pool_ref) | copy-start | bytes 6291460
  87.6 9.9 %copy-start.1 = (bf16[1024,1024]{1,0:T(8,128)(2,1)S(1)}, bf16[1024,1024]{1,0:T(8,128)(2,1)}, u32[]{:S(2)}) copy-start(bf16[1024,1024]{1,0:T(8,128)(2,1)} %copy-done) | copy-start | bytes 6291460
  87.6 1.2 %copy-start.4 = (bf16[1024,256]{1,0:T(8,128)(2,1)S(1)}, bf16[1024,256]{1,0:T(8,128)(2,1)}, u32[]{:S(2)}) copy-start(bf16[1024,256]{1,0:T(8,128)(2,1)} %copy-done.3) | copy-start | bytes 1572868
  92.9 6.4 %collective-permute-start.2 = (bf16[1024,256]{1,0:T(8,128)(2,1)S(1)}, bf16[1024,256]{1,0:T(8,128)(2,1)S(1)}, u32[]{:S(2)}, u32[]{:S(2)}) collective-permute-start(bf16[1024,256]{1,0:T(8,128)(2,1)S(1)} %attend.1.own_ref), channel_id=1, source_target_pairs={{0,1},{1,0},{2,3},{3,2},{4,5},{5,4},{6,7},{7,6},{8,9},{9,8},{10,11... | collective-permute-start | bytes 1572872 | tf_op jit(solution)/shard_map/ppermute | solution.py:396

commit v4 on v3

--- a/solution.py
+++ b/solution.py
@@ -60,9 +60,8 @@
     )(ids)
 
 
-def offer_kernel(
-    asked_hbm, store_ref, gain_hbm, key_hbm, value_hbm, out_ref,
-    rows, normed, gain_ref, w_ref, held, asked_ref, sems, out_sems,
+def project_kernel(
+    store_ref, gain_hbm, key_hbm, value_hbm, out_ref, rows, normed, gain_ref, w_ref, sems
 ):
     count, length, width = rows.shape
     tile = normed.shape[1]
@@ -78,8 +77,7 @@
     gain = pltpu.make_async_copy(gain_hbm, gain_ref, sems.at[tiles])
     key = pltpu.make_async_copy(key_hbm, w_ref.at[0], sems.at[tiles + 1])
     value = pltpu.make_async_copy(value_hbm, w_ref.at[1], sems.at[tiles + 2])
-    wanted = pltpu.make_async_copy(asked_hbm, asked_ref, sems.at[tiles + 3])
-    for copy in [gain, loads[0], key, value, *loads[1:], wanted]:
+    for copy in [gain, loads[0], key, value, *loads[1:]]:
         copy.start()
 
     def norm(i, first, last):
@@ -100,12 +98,42 @@
             if i + 1 < tiles:
                 norm(i + 1, p * tile // 2, (p + 1) * tile // 2)
             found = dot(normed[i % 2], w_ref[p]).astype(BF16).reshape(per, length, half)
-            held[i * per : (i + 1) * per, :, p * half : (p + 1) * half] = found
+            out_ref[i * per : (i + 1) * per, :, p * half : (p + 1) * half] = found
+
+
+def in_hbm(*arrays):
+    return [pltpu.with_memory_space_constraint(a, pltpu.HBM) for a in arrays]
+
+
+def project(store, gain, w_key, w_value):
+    count, length, width = store.shape
+    half, tile = w_key.shape[1], 256
+    return pl.pallas_call(
+        project_kernel,
+        in_specs=[pl.BlockSpec(memory_space=pltpu.HBM)] * 4,
+        out_specs=pl.BlockSpec(memory_space=pltpu.VMEM),
+        out_shape=jax.ShapeDtypeStruct((count, length, 2 * half), BF16),
+        scratch_shapes=[
+            pltpu.VMEM(store.shape, BF16),
+            pltpu.VMEM((2, tile, width), BF16),
+            pltpu.VMEM((1, width), F32),
+            pltpu.VMEM((2, width, half), BF16),
+            pltpu.SemaphoreType.DMA((count * length // tile + 3,)),
+        ],
+        compiler_params=params(20),
+        cost_estimate=cost(4 * count * length * width * half, 9 << 20),
+        name="project",
+    )(*in_hbm(store, gain.reshape(1, width), w_key, w_value))
+
+
+def place_kernel(asked_hbm, kv_ref, out_ref, asked_ref, sem, out_sems):
+    wanted = pltpu.make_async_copy(asked_hbm, asked_ref, sem)
+    wanted.start()
     wanted.wait()
     readers = out_ref.shape[0]
     asked = [asked_ref[r, 0, 0] for r in range(readers)]
     copies = [
-        pltpu.make_async_copy(held.at[jnp.maximum(asked[r] - 1, 0)], out_ref.at[r], out_sems.at[r])
+        pltpu.make_async_copy(kv_ref.at[jnp.maximum(asked[r] - 1, 0)], out_ref.at[r], out_sems.at[r])
         for r in range(readers)
     ]
     for r in range(readers):
@@ -114,28 +142,22 @@
         pl.when(asked[r] > 0)(copies[r].wait)
 
 
-def offer(asked, store, gain, w_key, w_value):
-    count, length, width = store.shape
-    readers, half, tile = asked.shape[0], w_key.shape[1], 256
-    return pl.pallas_call(
-        offer_kernel,
-        in_specs=[pl.BlockSpec(memory_space=pltpu.HBM)] * 5,
+def place(asked, kv):
+    readers = asked.shape[0]
+    return pl.pallas_call(
+        place_kernel,
+        in_specs=[pl.BlockSpec(memory_space=pltpu.HBM), pl.BlockSpec(memory_space=pltpu.VMEM)],
         out_specs=pl.BlockSpec(memory_space=pl.ANY),
-        out_shape=jax.ShapeDtypeStruct((readers, length, 2 * half), BF16),
+        out_shape=pltpu.HBM((readers,) + kv.shape[1:], BF16),
         scratch_shapes=[
-            pltpu.VMEM(store.shape, BF16),
-            pltpu.VMEM((2, tile, width), BF16),
-            pltpu.VMEM((1, width), F32),
-            pltpu.VMEM((2, width, half), BF16),
-            pltpu.VMEM((count, length, 2 * half), BF16),
             pltpu.SMEM(asked.shape, jnp.int32),
-            pltpu.SemaphoreType.DMA((count * length // tile + 4,)),
+            pltpu.SemaphoreType.DMA,
             pltpu.SemaphoreType.DMA((readers,)),
         ],
-        compiler_params=params(60),
-        cost_estimate=cost(4 * count * length * width * half, 9 << 20),
-        name="offer",
-    )(asked, store, gain.reshape(1, width), w_key, w_value)
+        compiler_params=params(8),
+        cost_estimate=cost(0, 5 << 20),
+        name="place",
+    )(asked, kv)
 
 
 def front_kernel(
@@ -324,7 +346,7 @@
         compiler_params=params(16),
         cost_estimate=cost(1 << 30, 3 << 20, 1 << 19),
         name="attend",
-    )(ids, sharpness, query, kv, behind)
+    )(ids, sharpness, *in_hbm(query), kv, behind)
 
 
 def own_kernel(
@@ -398,7 +420,7 @@
     count = store.shape[0]
     ids = passage_ids.T
     asked = across(requests(ids, count, lax.axis_size("st")))
-    offered = offer(asked, store, store_gain, w_key, w_value)
+    offered = place(asked, project(store, store_gain, w_key, w_value))
     kv = across(offered)
     w_branch, w_out, offered = lax.optimization_barrier((w_branch, w_out, offered))
     branch_other, out_other = swapped(w_branch), swapped(w_out)

time: 102 us -> 96.5 us (0.946)
  blocking collectives: 20.6 us -> 0 us
  starting transfers between devices: 12.9 us -> 26.4 us
  waiting for transfers between devices: 23.2 us -> 25.3 us
  local copies, waits for them, and re-layouts: 8.32 us -> 7.13 us
    all_to_all x1 -> x0, blocking collectives: 20.6 us -> none  [body(): lax.all_to_all(a, 'st', split_axis=0, concat_axis=0, tiled=True)]
    all_to_all x1 -> x2, starting transfers between devices: 5.8 us -> 21.2 us  [body(): lax.all_to_all(a, 'st', split_axis=0, concat_axis=0, tiled=True)]
    all_to_all x1 -> x2, waiting for transfers between devices: 21.1 us -> 23.2 us  [body(): lax.all_to_all(a, 'st', split_axis=0, concat_axis=0, tiled=True)]
    ppermute x4, starting transfers between devices: 7.07 us -> 5.23 us  [body(): swapped = lambda a: lax.ppermute(a, 'tp', SWAP)]
    unnamed x24 -> x22, local copies, waits for them, and re-layouts: 8.32 us -> 7.13 us
    pallas_call x1 -> x2, Pallas kernels: 9.56 us -> 10.3 us  [the longest x1 7.37 us: project(): pl.pallas_call(project_kernel, in_specs=[pl.BlockSpec(memory_space=pltpu....]
  transfers between devices with their start and end apart: 5 -> 6, of which waited for: 2 -> 3; matrix products, arithmetic and copies ran while one was open for 0% -> 0% of each run, Pallas kernels for 23% -> 32%
where the time goes in v4:
time: 96.5 us; the launch traced here: 96.1 us
  Pallas kernels  37 us (38%)
  starting transfers between devices  26.4 us (27%)
  waiting for transfers between devices  25.3 us (26%)
  local copies, waits for them, and re-layouts  7.13 us (7%)
    all_to_all x2, waiting for transfers between devices, body(): lax.all_to_all(a, 'st', split_axis=0, concat_axis=0, tiled=True)  23.2 us
    all_to_all x2, starting transfers between devices, body(): lax.all_to_all(a, 'st', split_axis=0, concat_axis=0, tiled=True)  21.2 us
    pallas_call x1, Pallas kernels, front(): pl.pallas_call(front_kernel, grid=(tokens // tile,), in_specs=[rowed(widt...  12.8 us
    pallas_call x1, Pallas kernels, project(): pl.pallas_call(project_kernel, in_specs=[pl.BlockSpec(memory_space=pltpu....  7.37 us
    unnamed x22, local copies, waits for them, and re-layouts  7.13 us
    ppermute x4, starting transfers between devices, body(): swapped = lambda a: lax.ppermute(a, 'tp', SWAP)  5.23 us
    pallas_call x1, Pallas kernels, branch(): pl.pallas_call(branch_kernel, grid=(tokens // tile,), in_specs=[pl.BlockS...  4.52 us
    pallas_call x1, Pallas kernels, attend(): pl.pallas_call(functools.partial(attend_kernel, count=count), in_specs=[p...  4.23 us
  transfers between devices with their start and end apart: 6, of which 3 were waited for; matrix products, arithmetic and copies ran while one was open for 0% of the time, Pallas kernels for 32%

profile of v4, /device:TPU:1, one launch (start us, length us, event | category | flops | bytes accessed | tf_op | source)
XLA Modules:
  0.0 96.1 jit_solution(7240653319175077234)
XLA Ops:
  0.0 1.4 %requests.1 = s32[64,1,128]{2,1,0:T(1,128)} custom-call(s32[4,8]{1,0:T(4,128)} %bitcast.3), custom_call_target="tpu_custom_call" | custom-call | tf_op jit(solution)/shard_map/requests/pallas_call | solution.py:54
  1.4 12.0 %all-to-all-start = ((s32[64,1,128]{2,1,0:T(1,128)}), s32[64,1,128]{2,1,0:T(1,128)S(1)}, u32[]{:S(2)}, u32[]{:S(2)}) async-start(s32[64,1,128]{2,1,0:T(1,128)} %requests.1), calls=%async_computation | async-start | bytes 65536 | tf_op jit(solution)/shard_map/all_to_all | solution.py:419
  13.4 7.4 %project.1.kv_ref = bf16[24,64,512]{2,1,0:T(8,128)(2,1)S(1)} custom-call(bf16[24,64,2048]{2,1,0:T(8,128)(2,1)} %store_ref.1, f32[1,2048]{1,0:T(1,128)} %bitcast.6, bf16[2048,256]{1,0:T(8,128)(2,1)} %key_hbm.1, bf16[2048,256]{1,0:T(8,128)(2,1)} %value_hbm.1), custom_call_target="tpu_custom_call" | custom-call | flops 3221225472 | bytes 9437184 | tf_op jit(solution)/shard_map/project/pallas_call | solution.py:111
  20.8 1.0 %all-to-all-done.asked_hbm = s32[64,1,128]{2,1,0:T(1,128)S(1)} async-done(((s32[64,1,128]{2,1,0:T(1,128)}), s32[64,1,128]{2,1,0:T(1,128)S(1)}, u32[]{:S(2)}, u32[]{:S(2)}) %all-to-all-start) | async-done | bytes 32800 | tf_op jit(solution)/shard_map/all_to_all | solution.py:419
  21.7 3.0 %place.1 = bf16[64,64,512]{2,1,0:T(8,128)(2,1)} custom-call(s32[64,1,128]{2,1,0:T(1,128)S(1)} %all-to-all-done.asked_hbm, bf16[24,64,512]{2,1,0:T(8,128)(2,1)S(1)} %project.1.kv_ref), custom_call_target="tpu_custom_call" | custom-call | bytes 5242880 | tf_op jit(solution)/shard_map/place/pallas_call | solution.py:147
  24.7 0.0 copy-start.9
  24.7 0.0 copy-start.10
  24.7 9.2 %all-to-all-start.1 = ((bf16[64,64,512]{2,1,0:T(8,128)(2,1)}), bf16[64,64,512]{2,1,0:T(8,128)(2,1)}, u32[]{:S(2)}, u32[]{:S(2)}) async-start(bf16[64,64,512]{2,1,0:T(8,128)(2,1)} %place.1), calls=%async_computation.1 | async-start | bytes 8388608 | tf_op jit(solution)/shard_map/all_to_all | solution.py:419
  34.0 1.6 %collective-permute-start.1 = (bf16[512,2048]{1,0:T(8,128)(2,1)}, bf16[512,2048]{1,0:T(8,128)(2,1)S(1)}, u32[]{:S(2)}, u32[]{:S(2)}) collective-permute-start(bf16[512,2048]{1,0:T(8,128)(2,1)} %w_own_ref), channel_id=1, source_target_pairs={{0,1},{1,0},{2,3},{3,2},{4,5},{5,4},{6,7},{7,6},{8,9},{9,8},{10,11... | collective-permute-start | bytes 6291464 | tf_op jit(solution)/shard_map/ppermute | solution.py:418
  35.6 0.0 copy-done.9
  35.6 0.0 copy-done.10
  35.6 0.0 copy-start.6
  35.6 2.2 %copy-done.6 = bf16[1024,2048]{1,0:T(8,128)(2,1)S(1)} copy-done((bf16[1024,2048]{1,0:T(8,128)(2,1)S(1)}, bf16[1024,2048]{1,0:T(8,128)(2,1)}, u32[]{:S(2)}) %copy-start.6) | copy-done | bytes 4194328
  37.8 0.0 copy-start.7
  37.8 1.6 %copy-done.7 = bf16[2048,512]{1,0:T(8,128)(2,1)S(1)} copy-done((bf16[2048,512]{1,0:T(8,128)(2,1)S(1)}, bf16[2048,512]{1,0:T(8,128)(2,1)}, u32[]{:S(2)}) %copy-start.7) | copy-done | bytes 2097176
  39.4 0.0 copy-start.8
  39.4 1.2 %copy-done.8 = bf16[2048,256]{1,0:T(8,128)(2,1)S(1)} copy-done((bf16[2048,256]{1,0:T(8,128)(2,1)S(1)}, bf16[2048,256]{1,0:T(8,128)(2,1)}, u32[]{:S(2)}) %copy-start.8) | copy-done | bytes 1048600
  40.6 0.0 copy-start.2
  40.6 12.8 %front.1 = (bf16[1024,512]{1,0:T(8,128)(2,1)S(1)}, bf16[1024,256]{1,0:T(8,128)(2,1)S(1)}, bf16[1024,1024]{1,0:T(8,128)(2,1)S(1)}) custom-call(bf16[1024,2048]{1,0:T(8,128)(2,1)S(1)} %copy-done.6, f32[1,2048]{1,0:T(1,128)S(1)} %bitcast.5, bf16[2048,512]{1,0:T(8,128)(2,1)S(1)} %copy-done.7, bf16[2048,256]{1,0:T(8,128)(2,1)S(1)} %copy-done.8, ...), custom_call_target="tpu_custom_call" | custom-call | flops 7516192768 | bytes 25165824 | tf_op jit(solution)/shard_map/front/pallas_call | solution.py:205
  53.3 0.0 copy-start.3
  53.4 0.8 copy-done.3
  54.1 0.0 copy-start.4
  54.1 0.0 copy-start.5
  54.1 0.0 collective-permute-start
  54.2 0.0 copy-done.2
  54.2 0.5 collective-permute-start.3
  54.7 2.1 %collective-permute-done.other_ref = bf16[1024,512]{1,0:T(8,128)(2,1)S(1)} collective-permute-done((bf16[1024,512]{1,0:T(8,128)(2,1)S(1)}, bf16[1024,512]{1,0:T(8,128)(2,1)S(1)}, u32[]{:S(2)}, u32[]{:S(2)}) %collective-permute-start) | collective-permute-done | bytes 1048608 | tf_op jit(solution)/shard_map/ppermute | solution.py:418
  56.8 0.0 collective-permute-done.1.w_other_ref
  56.8 4.5 %branch.1 = (bf16[1024,1024]{1,0:T(8,128)(2,1)S(1)}, f32[8,128]{1,0:T(8,128)S(1)}) custom-call(bf16[1024,512]{1,0:T(8,128)(2,1)S(1)} %get-tuple-element.15.own_ref, bf16[1024,512]{1,0:T(8,128)(2,1)S(1)} %collective-permute-done.other_ref, bf16[512,2048]{1,0:T(8,128)(2,1)} %w_own_ref, bf16[512,2048]{1,0:T(8,128)(2,1)S(1)} %collective-permute-done.1.w_other_ref), custom_call_target="tpu_custom_call" | custom-call | flops 2147483648 | bytes 8388608 | tf_op jit(solution)/shard_map/branch/pallas_call | solution.py:245
  61.3 0.0 copy-start
  61.3 1.3 %copy-done = bf16[1024,1024]{1,0:T(8,128)(2,1)} copy-done((bf16[1024,1024]{1,0:T(8,128)(2,1)}, bf16[1024,1024]{1,0:T(8,128)(2,1)S(1)}, u32[]{:S(2)}) %copy-start) | copy-done | bytes 2097176
  62.7 22.2 %all-to-all-done.1.kv_ref = bf16[64,64,512]{2,1,0:T(8,128)(2,1)} async-done(((bf16[64,64,512]{2,1,0:T(8,128)(2,1)}), bf16[64,64,512]{2,1,0:T(8,128)(2,1)}, u32[]{:S(2)}, u32[]{:S(2)}) %all-to-all-start.1) | async-done | bytes 4194336 | tf_op jit(solution)/shard_map/all_to_all | solution.py:419
  84.8 0.0 copy-done.4
  84.8 0.0 copy-done.5
  84.8 0.0 copy-start.1
  84.8 4.2 %attend.1.own_ref = bf16[1024,256]{1,0:T(8,128)(2,1)S(1)} custom-call(s32[4,8]{1,0:T(4,128)S(1)} %bitcast.4, f32[2]{0:T(128)S(1)} %copy-done.5, bf16[1024,256]{1,0:T(8,128)(2,1)} %copy-done.3, bf16[64,64,512]{2,1,0:T(8,128)(2,1)} %all-to-all-done.1.kv_ref, f32[8,128]{1,0:T(8,128)S(1)} %get-tuple-element.17._), custom_call_target="tpu_custom_call" | custom-call | flops 1073741824 | bytes 3145728 | tf_op jit(solution)/shard_map/attend/pallas_call | solution.py:328
  89.1 3.1 %collective-permute-start.2 = (bf16[1024,256]{1,0:T(8,128)(2,1)S(1)}, bf16[1024,256]{1,0:T(8,128)(2,1)S(1)}, u32[]{:S(2)}, u32[]{:S(2)}) collective-permute-start(bf16[1024,256]{1,0:T(8,128)(2,1)S(1)} %attend.1.own_ref), channel_id=1, source_target_pairs={{0,1},{1,0},{2,3},{3,2},{4,5},{5,4},{6,7},{7,6},{8,9},{9,8},{10,11... | collective-permute-start | bytes 1572872 | tf_op jit(solution)/shard_map/ppermute | solution.py:418
  92.2 0.0 collective-permute-done.3.w_other_ref
  92.2 0.0 copy-done.1
  92.2 1.8 %own_part.1 = (f32[1024,1024]{1,0:T(8,128)S(1)}, bf16[256,1024]{1,0:T(8,128)(2,1)S(1)}) custom-call(bf16[1024,256]{1,0:T(8,128)(2,1)S(1)} %attend.1.own_ref, bf16[256,2048]{1,0:T(8,128)(2,1)S(1)} %copy-done.2, bf16[256,2048]{1,0:T(8,128)(2,1)} %collective-permute-done.3.w_other_ref, bf16[1024,1024]{1,0:T(8,128)(2,1)S(1)} %copy-done.1, ...), custom_call_target="tpu_custom_call" | custom-call | flops 536870912 | bytes 12582912 | tf_op jit(solution)/shard_map/own_part/pallas_call | solution.py:370
  94.1 0.0 collective-permute-done.2.other_ref
  94.1 1.9 %mixed.1 = bf16[1024,1024]{1,0:T(8,128)(2,1)} custom-call(bf16[1024,256]{1,0:T(8,128)(2,1)S(1)} %collective-permute-done.2.other_ref, bf16[256,1024]{1,0:T(8,128)(2,1)S(1)} %get-tuple-element.21.w_ref, f32[1024,1024]{1,0:T(8,128)S(1)} %get-tuple-element.22.sum_ref, bf16[1024,1024]{1,0:T(8,128)(2,1)S(1)} %get-tuple-element.20.gate_ref), custom_call_target="tpu_custom_call" | custom-call | flops 536870912 | bytes 12582912 | tf_op jit(solution)/shard_map/mixed/pallas_call | solution.py:402
Async XLA Ops:
  1.4 20.3 %all-to-all-start = ((s32[64,1,128]{2,1,0:T(1,128)}), s32[64,1,128]{2,1,0:T(1,128)S(1)}, u32[]{:S(2)}, u32[]{:S(2)}) async-start(s32[64,1,128]{2,1,0:T(1,128)} %requests.1), calls=%async_computation | async-start | bytes 65536 | tf_op jit(solution)/shard_map/all_to_all | solution.py:419
  24.7 10.9 %copy-start.9 = (bf16[2,256,256]{2,1,0:T(8,128)(2,1)S(1)}, bf16[2,256,256]{2,1,0:T(8,128)(2,1)}, u32[]{:S(2)}) copy-start(bf16[2,256,256]{2,1,0:T(8,128)(2,1)} %mix_ref.1) | copy-start | bytes 786436
  24.7 10.9 %copy-start.10 = (f32[2048]{0:T(1024)S(1)}, f32[2048]{0:T(1024)}, u32[]{:S(2)}) copy-start(f32[2048]{0:T(1024)} %param.15) | copy-start | bytes 24580
  24.7 60.1 %all-to-all-start.1 = ((bf16[64,64,512]{2,1,0:T(8,128)(2,1)}), bf16[64,64,512]{2,1,0:T(8,128)(2,1)}, u32[]{:S(2)}, u32[]{:S(2)}) async-start(bf16[64,64,512]{2,1,0:T(8,128)(2,1)} %place.1), calls=%async_computation.1 | async-start | bytes 8388608 | tf_op jit(solution)/shard_map/all_to_all | solution.py:419
  34.0 22.8 %collective-permute-start.1 = (bf16[512,2048]{1,0:T(8,128)(2,1)}, bf16[512,2048]{1,0:T(8,128)(2,1)S(1)}, u32[]{:S(2)}, u32[]{:S(2)}) collective-permute-start(bf16[512,2048]{1,0:T(8,128)(2,1)} %w_own_ref), channel_id=1, source_target_pairs={{0,1},{1,0},{2,3},{3,2},{4,5},{5,4},{6,7},{7,6},{8,9},{9,8},{10,11... | collective-permute-start | bytes 6291464 | tf_op jit(solution)/shard_map/ppermute | solution.py:418
  35.6 2.2 %copy-start.6 = (bf16[1024,2048]{1,0:T(8,128)(2,1)S(1)}, bf16[1024,2048]{1,0:T(8,128)(2,1)}, u32[]{:S(2)}) copy-start(bf16[1024,2048]{1,0:T(8,128)(2,1)} %hidden_ref.1) | copy-start | bytes 12582916
  37.8 1.6 %copy-start.7 = (bf16[2048,512]{1,0:T(8,128)(2,1)S(1)}, bf16[2048,512]{1,0:T(8,128)(2,1)}, u32[]{:S(2)}) copy-start(bf16[2048,512]{1,0:T(8,128)(2,1)} %pool_ref.1) | copy-start | bytes 6291460
  39.4 1.2 %copy-start.8 = (bf16[2048,256]{1,0:T(8,128)(2,1)S(1)}, bf16[2048,256]{1,0:T(8,128)(2,1)}, u32[]{:S(2)}) copy-start(bf16[2048,256]{1,0:T(8,128)(2,1)} %query_ref.1) | copy-start | bytes 3145732
  40.6 13.6 %copy-start.2 = (bf16[256,2048]{1,0:T(8,128)(2,1)S(1)}, bf16[256,2048]{1,0:T(8,128)(2,1)}, u32[]{:S(2)}) copy-start(bf16[256,2048]{1,0:T(8,128)(2,1)} %w_own_ref.1) | copy-start | bytes 3145732
  53.3 0.8 copy-start.3
  54.1 30.7 %copy-start.4 = (s32[8,4]{0,1:T(4,128)S(1)}, s32[8,4]{0,1:T(4,128)}, u32[]{:S(2)}) copy-start(s32[8,4]{0,1:T(4,128)} %param.18) | copy-start | bytes 388
  54.1 30.7 %copy-start.5 = (f32[2]{0:T(128)S(1)}, f32[2]{0:T(128)}, u32[]{:S(2)}) copy-start(f32[2]{0:T(128)} %sharp_ref.1) | copy-start | bytes 28
  54.1 2.7 %collective-permute-start = (bf16[1024,512]{1,0:T(8,128)(2,1)S(1)}, bf16[1024,512]{1,0:T(8,128)(2,1)S(1)}, u32[]{:S(2)}, u32[]{:S(2)}) collective-permute-start(bf16[1024,512]{1,0:T(8,128)(2,1)S(1)} %get-tuple-element.15.own_ref), channel_id=1, source_target_pairs={{0,1},{1,0},{2,3},{3,2},{4,5},{5,4},{6,7},{7,6},{8,9},{9,8},{10,11... | collective-permute-start | bytes 3145736 | tf_op jit(solution)/shard_map/ppermute | solution.py:418
  54.2 38.0 %collective-permute-start.3 = (bf16[256,2048]{1,0:T(8,128)(2,1)S(1)}, bf16[256,2048]{1,0:T(8,128)(2,1)}, u32[]{:S(2)}, u32[]{:S(2)}) collective-permute-start(bf16[256,2048]{1,0:T(8,128)(2,1)S(1)} %copy-done.2), channel_id=1, source_target_pairs={{0,1},{1,0},{2,3},{3,2},{4,5},{5,4},{6,7},{7,6},{8,9},{9,8},{10,11... | collective-permute-start | bytes 3145736 | tf_op jit(solution)/shard_map/ppermute | solution.py:418
  61.3 1.3 %copy-start = (bf16[1024,1024]{1,0:T(8,128)(2,1)}, bf16[1024,1024]{1,0:T(8,128)(2,1)S(1)}, u32[]{:S(2)}) copy-start(bf16[1024,1024]{1,0:T(8,128)(2,1)S(1)} %get-tuple-element.19.pool_ref) | copy-start | bytes 6291460
  84.8 7.4 %copy-start.1 = (bf16[1024,1024]{1,0:T(8,128)(2,1)S(1)}, bf16[1024,1024]{1,0:T(8,128)(2,1)}, u32[]{:S(2)}) copy-start(bf16[1024,1024]{1,0:T(8,128)(2,1)} %copy-done) | copy-start | bytes 6291460
  89.1 5.0 %collective-permute-start.2 = (bf16[1024,256]{1,0:T(8,128)(2,1)S(1)}, bf16[1024,256]{1,0:T(8,128)(2,1)S(1)}, u32[]{:S(2)}, u32[]{:S(2)}) collective-permute-start(bf16[1024,256]{1,0:T(8,128)(2,1)S(1)} %attend.1.own_ref), channel_id=1, source_target_pairs={{0,1},{1,0},{2,3},{3,2},{4,5},{5,4},{6,7},{7,6},{8,9},{9,8},{10,11... | collective-permute-start | bytes 1572872 | tf_op jit(solution)/shard_map/ppermute | solution.py:418

commit v5 on v4

--- a/solution.py
+++ b/solution.py
@@ -266,7 +266,7 @@
 
 
 def attend_kernel(
-    ids_ref, sharp_ref, query_hbm, kv_ref, _, out_ref,
+    ids_ref, sharp_ref, query_hbm, kv_ref, w_other_ref, _, out_ref, columns_ref,
     held, query_ref, scores_ref, weights_ref, sems, *, count
 ):
     reads, blocks = ids_ref.shape
@@ -310,9 +310,14 @@
             out_ref[b * block : (b + 1) * block, h * dim : (h + 1) * dim] = found.astype(BF16)
 
     first = pltpu.make_async_copy(query_hbm, query_ref, sems.at[reads * blocks])
+    last = pltpu.make_async_copy(
+        w_other_ref.at[:, half_columns(columns_ref.shape[1])], columns_ref,
+        sems.at[reads * blocks + 1],
+    )
     first.start()
     for copy in copies:
         copy.start()
+    last.start()
     first.wait()
     rounds = blocks // TOGETHER
     for i in range(rounds + 2):
@@ -320,9 +325,10 @@
             if 0 <= i - delay < rounds:
                 for b in range(TOGETHER):
                     act((i - delay) * TOGETHER + b)
-
-
-def attend(ids, sharpness, query, kv, behind, count):
+    last.wait()
+
+
+def attend(ids, sharpness, query, kv, w_other, behind, count):
     reads, blocks = ids.shape
     shape = (blocks * sharpness.shape[0], reads * kv.shape[1], query.shape[0] // blocks)
     return pl.pallas_call(
@@ -332,54 +338,49 @@
             pl.BlockSpec(memory_space=pltpu.SMEM),
             pl.BlockSpec(memory_space=pltpu.HBM),
             pl.BlockSpec(memory_space=pltpu.HBM),
+            pl.BlockSpec(memory_space=pltpu.HBM),
             pl.BlockSpec(memory_space=pl.ANY),
         ],
-        out_specs=pl.BlockSpec(memory_space=pltpu.VMEM),
-        out_shape=jax.ShapeDtypeStruct(query.shape, BF16),
+        out_specs=[pl.BlockSpec(memory_space=pltpu.VMEM)] * 2,
+        out_shape=[
+            pltpu.VMEM(query.shape, BF16),
+            pltpu.VMEM((w_other.shape[0], w_other.shape[1] // 2), BF16),
+        ],
         scratch_shapes=[
             pltpu.VMEM((ids.size,) + kv.shape[1:], BF16),
             pltpu.VMEM(query.shape, BF16),
             pltpu.VMEM(shape, F32),
             pltpu.VMEM(shape, BF16),
-            pltpu.SemaphoreType.DMA((ids.size + 1,)),
+            pltpu.SemaphoreType.DMA((ids.size + 2,)),
         ],
         compiler_params=params(16),
         cost_estimate=cost(1 << 30, 3 << 20, 1 << 19),
         name="attend",
-    )(ids, sharpness, *in_hbm(query), kv, behind)
-
-
-def own_kernel(
-    own_ref, w_own_ref, w_other_ref, pool_ref, gate_ref, out_ref, columns_ref, sem
-):
+    )(ids, sharpness, *in_hbm(query), kv, *in_hbm(w_other), behind)
+
+
+def own_kernel(own_ref, w_ref, pool_ref, gate_ref, out_ref):
     columns = half_columns(gate_ref.shape[1])
-    copy = pltpu.make_async_copy(w_other_ref.at[:, columns], columns_ref, sem)
-    copy.start()
     tile = own_ref.shape[0] // 4
     for i in range(4):
         rows = slice(i * tile, (i + 1) * tile)
-        own = dot(own_ref[rows], w_own_ref[:, columns]).astype(BF16).astype(F32)
+        own = dot(own_ref[rows], w_ref[:, columns]).astype(BF16).astype(F32)
         out_ref[rows] = pool_ref[rows].astype(F32) + gate_ref[rows].astype(F32) * own
-    copy.wait()
-
-
-def own_part(own, w_own, w_other, pool, gate):
+
+
+def own_part(own, w_own, pool, gate):
     tokens, depth = own.shape
     width = gate.shape[1]
     vmem = pl.BlockSpec(memory_space=pltpu.VMEM)
     return pl.pallas_call(
         own_kernel,
-        in_specs=[vmem, vmem, pl.BlockSpec(memory_space=pl.ANY), vmem, vmem],
-        out_specs=[vmem, vmem],
-        out_shape=[
-            jax.ShapeDtypeStruct((tokens, width), F32),
-            jax.ShapeDtypeStruct((depth, width), BF16),
-        ],
-        scratch_shapes=[pltpu.SemaphoreType.DMA],
+        in_specs=[vmem] * 4,
+        out_specs=vmem,
+        out_shape=pltpu.VMEM((tokens, width), F32),
         compiler_params=params(16),
         cost_estimate=cost(2 * tokens * depth * width, 12 << 20),
         name="own_part",
-    )(own, w_own, w_other, pool, gate)
+    )(own, w_own, pool, gate)
 
 
 def mixed_kernel(other_ref, w_ref, sum_ref, gate_ref, out_ref, done, sems):
@@ -426,8 +427,8 @@
     branch_other, out_other = swapped(w_branch), swapped(w_out)
     pool_out, query, gate = front(hidden, norm_gain, w_pool, w_query, w_gate, pool_mix)
     pool, token = branch(pool_out, swapped(pool_out), w_branch, branch_other)
-    read = attend(ids, sharpness, query, kv, token, count)
-    summed, columns = own_part(read, w_out, out_other, pool, gate)
+    read, columns = attend(ids, sharpness, query, kv, out_other, token, count)
+    summed = own_part(read, w_out, pool, gate)
     return mix(swapped(read), columns, summed, gate)
 
 

time: 96.5 us -> 96.2 us (level)
  waiting for transfers between devices: 25.3 us -> 26.4 us
  transfers between devices with their start and end apart: 6 -> 6, of which waited for: 3 -> 4; matrix products, arithmetic and copies ran while one was open for 0% -> 0% of each run, Pallas kernels for 32% -> 27%
where the time goes in v5:
time: 96.2 us; the launch traced here: 95.8 us
  Pallas kernels  36.3 us (38%)
  starting transfers between devices  26.4 us (27%)
  waiting for transfers between devices  26.4 us (27%)
  local copies, waits for them, and re-layouts  6.35 us (7%)
    all_to_all x2, waiting for transfers between devices, body(): lax.all_to_all(a, 'st', split_axis=0, concat_axis=0, tiled=True)  23.8 us
    all_to_all x2, starting transfers between devices, body(): lax.all_to_all(a, 'st', split_axis=0, concat_axis=0, tiled=True)  21.1 us
    pallas_call x1, Pallas kernels, front(): pl.pallas_call(front_kernel, grid=(tokens // tile,), in_specs=[rowed(widt...  12.8 us
    pallas_call x1, Pallas kernels, project(): pl.pallas_call(project_kernel, in_specs=[pl.BlockSpec(memory_space=pltpu....  7.37 us
    unnamed x22, local copies, waits for them, and re-layouts  6.35 us
    ppermute x4, starting transfers between devices, body(): swapped = lambda a: lax.ppermute(a, 'tp', SWAP)  5.3 us
    pallas_call x1, Pallas kernels, branch(): pl.pallas_call(branch_kernel, grid=(tokens // tile,), in_specs=[pl.BlockS...  4.52 us
    pallas_call x1, Pallas kernels, attend(): pl.pallas_call(functools.partial(attend_kernel, count=count), in_specs=[p...  4.25 us
  transfers between devices with their start and end apart: 6, of which 4 were waited for; matrix products, arithmetic and copies ran while one was open for 0% of the time, Pallas kernels for 27%

profile of v5, /device:TPU:1, one launch (start us, length us, event | category | flops | bytes accessed | tf_op | source)
XLA Modules:
  0.0 95.8 jit_solution(4394665263239640429)
XLA Ops:
  0.0 1.4 %requests.1 = s32[64,1,128]{2,1,0:T(1,128)} custom-call(s32[4,8]{1,0:T(4,128)} %bitcast.3), custom_call_target="tpu_custom_call" | custom-call | tf_op jit(solution)/shard_map/requests/pallas_call | solution.py:54
  1.4 12.0 %all-to-all-start = ((s32[64,1,128]{2,1,0:T(1,128)}), s32[64,1,128]{2,1,0:T(1,128)S(1)}, u32[]{:S(2)}, u32[]{:S(2)}) async-start(s32[64,1,128]{2,1,0:T(1,128)} %requests.1), calls=%async_computation | async-start | bytes 65536 | tf_op jit(solution)/shard_map/all_to_all | solution.py:420
  13.4 7.4 %project.1.kv_ref = bf16[24,64,512]{2,1,0:T(8,128)(2,1)S(1)} custom-call(bf16[24,64,2048]{2,1,0:T(8,128)(2,1)} %store_ref.1, f32[1,2048]{1,0:T(1,128)} %bitcast.6, bf16[2048,256]{1,0:T(8,128)(2,1)} %key_hbm.1, bf16[2048,256]{1,0:T(8,128)(2,1)} %value_hbm.1), custom_call_target="tpu_custom_call" | custom-call | flops 3221225472 | bytes 9437184 | tf_op jit(solution)/shard_map/project/pallas_call | solution.py:111
  20.8 1.0 %all-to-all-done.asked_hbm = s32[64,1,128]{2,1,0:T(1,128)S(1)} async-done(((s32[64,1,128]{2,1,0:T(1,128)}), s32[64,1,128]{2,1,0:T(1,128)S(1)}, u32[]{:S(2)}, u32[]{:S(2)}) %all-to-all-start) | async-done | bytes 32800 | tf_op jit(solution)/shard_map/all_to_all | solution.py:420
  21.7 3.0 %place.1 = bf16[64,64,512]{2,1,0:T(8,128)(2,1)} custom-call(s32[64,1,128]{2,1,0:T(1,128)S(1)} %all-to-all-done.asked_hbm, bf16[24,64,512]{2,1,0:T(8,128)(2,1)S(1)} %project.1.kv_ref), custom_call_target="tpu_custom_call" | custom-call | bytes 5242880 | tf_op jit(solution)/shard_map/place/pallas_call | solution.py:147
  24.8 0.0 copy-start.9
  24.8 0.0 copy-start.10
  24.8 9.1 %all-to-all-start.1 = ((bf16[64,64,512]{2,1,0:T(8,128)(2,1)}), bf16[64,64,512]{2,1,0:T(8,128)(2,1)}, u32[]{:S(2)}, u32[]{:S(2)}) async-start(bf16[64,64,512]{2,1,0:T(8,128)(2,1)} %place.1), calls=%async_computation.1 | async-start | bytes 8388608 | tf_op jit(solution)/shard_map/all_to_all | solution.py:420
  33.9 1.6 %collective-permute-start.2 = (bf16[512,2048]{1,0:T(8,128)(2,1)}, bf16[512,2048]{1,0:T(8,128)(2,1)S(1)}, u32[]{:S(2)}, u32[]{:S(2)}) collective-permute-start(bf16[512,2048]{1,0:T(8,128)(2,1)} %w_own_ref), channel_id=1, source_target_pairs={{0,1},{1,0},{2,3},{3,2},{4,5},{5,4},{6,7},{7,6},{8,9},{9,8},{10,11... | collective-permute-start | bytes 6291464 | tf_op jit(solution)/shard_map/ppermute | solution.py:419
  35.5 0.0 copy-done.9
  35.5 0.0 copy-done.10
  35.5 0.0 copy-start.6
  35.5 2.2 %copy-done.6 = bf16[1024,2048]{1,0:T(8,128)(2,1)S(1)} copy-done((bf16[1024,2048]{1,0:T(8,128)(2,1)S(1)}, bf16[1024,2048]{1,0:T(8,128)(2,1)}, u32[]{:S(2)}) %copy-start.6) | copy-done | bytes 4194328
  37.7 0.0 copy-start.7
  37.7 1.6 %copy-done.7 = bf16[2048,512]{1,0:T(8,128)(2,1)S(1)} copy-done((bf16[2048,512]{1,0:T(8,128)(2,1)S(1)}, bf16[2048,512]{1,0:T(8,128)(2,1)}, u32[]{:S(2)}) %copy-start.7) | copy-done | bytes 2097176
  39.3 0.0 copy-start.8
  39.3 1.2 %copy-done.8 = bf16[2048,256]{1,0:T(8,128)(2,1)S(1)} copy-done((bf16[2048,256]{1,0:T(8,128)(2,1)S(1)}, bf16[2048,256]{1,0:T(8,128)(2,1)}, u32[]{:S(2)}) %copy-start.8) | copy-done | bytes 1048600
  40.5 0.0 copy-start.2
  40.5 12.8 %front.1 = (bf16[1024,512]{1,0:T(8,128)(2,1)S(1)}, bf16[1024,256]{1,0:T(8,128)(2,1)S(1)}, bf16[1024,1024]{1,0:T(8,128)(2,1)S(1)}) custom-call(bf16[1024,2048]{1,0:T(8,128)(2,1)S(1)} %copy-done.6, f32[1,2048]{1,0:T(1,128)S(1)} %bitcast.5, bf16[2048,512]{1,0:T(8,128)(2,1)S(1)} %copy-done.7, bf16[2048,256]{1,0:T(8,128)(2,1)S(1)} %copy-done.8, ...), custom_call_target="tpu_custom_call" | custom-call | flops 7516192768 | bytes 25165824 | tf_op jit(solution)/shard_map/front/pallas_call | solution.py:205
  53.3 0.0 copy-start.3
  53.3 0.0 copy-start.4
  53.3 0.0 copy-start.5
  53.3 0.1 collective-permute-start.1
  53.5 0.0 copy-done.2
  53.5 0.5 collective-permute-start
  53.9 2.1 %collective-permute-done.1.other_ref = bf16[1024,512]{1,0:T(8,128)(2,1)S(1)} collective-permute-done((bf16[1024,512]{1,0:T(8,128)(2,1)S(1)}, bf16[1024,512]{1,0:T(8,128)(2,1)S(1)}, u32[]{:S(2)}, u32[]{:S(2)}) %collective-permute-start.1) | collective-permute-done | bytes 1048608 | tf_op jit(solution)/shard_map/ppermute | solution.py:419
  56.1 0.0 collective-permute-done.2.w_other_ref
  56.1 4.5 %branch.1 = (bf16[1024,1024]{1,0:T(8,128)(2,1)S(1)}, f32[8,128]{1,0:T(8,128)S(1)}) custom-call(bf16[1024,512]{1,0:T(8,128)(2,1)S(1)} %get-tuple-element.16.own_ref, bf16[1024,512]{1,0:T(8,128)(2,1)S(1)} %collective-permute-done.1.other_ref, bf16[512,2048]{1,0:T(8,128)(2,1)} %w_own_ref, bf16[512,2048]{1,0:T(8,128)(2,1)S(1)} %collective-permute-done.2.w_other_ref), custom_call_target="tpu_custom_call" | custom-call | flops 2147483648 | bytes 8388608 | tf_op jit(solution)/shard_map/branch/pallas_call | solution.py:245
  60.6 0.0 copy-done.3
  60.6 0.0 copy-start
  60.6 1.3 %copy-done = bf16[1024,1024]{1,0:T(8,128)(2,1)} copy-done((bf16[1024,1024]{1,0:T(8,128)(2,1)}, bf16[1024,1024]{1,0:T(8,128)(2,1)S(1)}, u32[]{:S(2)}) %copy-start) | copy-done | bytes 2097176
  61.9 0.0 collective-permute-done.w_other_ref
  61.9 22.9 %all-to-all-done.1.kv_ref = bf16[64,64,512]{2,1,0:T(8,128)(2,1)} async-done(((bf16[64,64,512]{2,1,0:T(8,128)(2,1)}), bf16[64,64,512]{2,1,0:T(8,128)(2,1)}, u32[]{:S(2)}, u32[]{:S(2)}) %all-to-all-start.1) | async-done | bytes 4194336 | tf_op jit(solution)/shard_map/all_to_all | solution.py:420
  84.8 0.0 copy-done.4
  84.8 0.0 copy-done.5
  84.8 0.0 copy-start.1
  84.8 4.2 %attend.1 = (bf16[1024,256]{1,0:T(8,128)(2,1)S(1)}, bf16[256,1024]{1,0:T(8,128)(2,1)S(1)}) custom-call(s32[4,8]{1,0:T(4,128)S(1)} %bitcast.4, f32[2]{0:T(128)S(1)} %copy-done.5, bf16[1024,256]{1,0:T(8,128)(2,1)} %copy-done.3, bf16[64,64,512]{2,1,0:T(8,128)(2,1)} %all-to-all-done.1.kv_ref, bf16[256,2048]{1,0:T(8,128)(2,1)} %collective-permute-done.w_other_ref, ...), custom_call_target="tpu_custom_call" | custom-call | flops 1073741824 | bytes 3145728 | tf_op jit(solution)/shard_map/attend/pallas_call | solution.py:334
  89.1 3.1 %collective-permute-start.3 = (bf16[1024,256]{1,0:T(8,128)(2,1)S(1)}, bf16[1024,256]{1,0:T(8,128)(2,1)S(1)}, u32[]{:S(2)}, u32[]{:S(2)}) collective-permute-start(bf16[1024,256]{1,0:T(8,128)(2,1)S(1)} %get-tuple-element.19.own_ref), channel_id=1, source_target_pairs={{0,1},{1,0},{2,3},{3,2},{4,5},{5,4},{6,7},{7,6},{8,9},{9,8},{10,11... | collective-permute-start | bytes 1572872 | tf_op jit(solution)/shard_map/ppermute | solution.py:419
  92.2 0.0 copy-done.1
  92.2 1.1 %own_part.1.sum_ref = f32[1024,1024]{1,0:T(8,128)S(1)} custom-call(bf16[1024,256]{1,0:T(8,128)(2,1)S(1)} %get-tuple-element.19.own_ref, bf16[256,2048]{1,0:T(8,128)(2,1)S(1)} %copy-done.2, bf16[1024,1024]{1,0:T(8,128)(2,1)S(1)} %copy-done.1, bf16[1024,1024]{1,0:T(8,128)(2,1)S(1)} %get-tuple-element.22.gate_ref), custom_call_target="tpu_custom_call" | custom-call | flops 536870912 | bytes 12582912 | tf_op jit(solution)/shard_map/own_part/pallas_call | solution.py:375
  93.3 0.5 collective-permute-done.3.other_ref
  93.7 1.9 %mixed.1 = bf16[1024,1024]{1,0:T(8,128)(2,1)} custom-call(bf16[1024,256]{1,0:T(8,128)(2,1)S(1)} %collective-permute-done.3.other_ref, bf16[256,1024]{1,0:T(8,128)(2,1)S(1)} %get-tuple-element.20.w_ref, f32[1024,1024]{1,0:T(8,128)S(1)} %own_part.1.sum_ref, bf16[1024,1024]{1,0:T(8,128)(2,1)S(1)} %get-tuple-element.22.gate_ref), custom_call_target="tpu_custom_call" | custom-call | flops 536870912 | bytes 12582912 | tf_op jit(solution)/shard_map/mixed/pallas_call | solution.py:403
Async XLA Ops:
  1.4 20.3 %all-to-all-start = ((s32[64,1,128]{2,1,0:T(1,128)}), s32[64,1,128]{2,1,0:T(1,128)S(1)}, u32[]{:S(2)}, u32[]{:S(2)}) async-start(s32[64,1,128]{2,1,0:T(1,128)} %requests.1), calls=%async_computation | async-start | bytes 65536 | tf_op jit(solution)/shard_map/all_to_all | solution.py:420
  24.8 10.7 %copy-start.9 = (bf16[2,256,256]{2,1,0:T(8,128)(2,1)S(1)}, bf16[2,256,256]{2,1,0:T(8,128)(2,1)}, u32[]{:S(2)}) copy-start(bf16[2,256,256]{2,1,0:T(8,128)(2,1)} %mix_ref.1) | copy-start | bytes 786436
  24.8 10.7 %copy-start.10 = (f32[2048]{0:T(1024)S(1)}, f32[2048]{0:T(1024)}, u32[]{:S(2)}) copy-start(f32[2048]{0:T(1024)} %param.15) | copy-start | bytes 24580
  24.8 60.0 %all-to-all-start.1 = ((bf16[64,64,512]{2,1,0:T(8,128)(2,1)}), bf16[64,64,512]{2,1,0:T(8,128)(2,1)}, u32[]{:S(2)}, u32[]{:S(2)}) async-start(bf16[64,64,512]{2,1,0:T(8,128)(2,1)} %place.1), calls=%async_computation.1 | async-start | bytes 8388608 | tf_op jit(solution)/shard_map/all_to_all | solution.py:420
  33.9 22.1 %collective-permute-start.2 = (bf16[512,2048]{1,0:T(8,128)(2,1)}, bf16[512,2048]{1,0:T(8,128)(2,1)S(1)}, u32[]{:S(2)}, u32[]{:S(2)}) collective-permute-start(bf16[512,2048]{1,0:T(8,128)(2,1)} %w_own_ref), channel_id=1, source_target_pairs={{0,1},{1,0},{2,3},{3,2},{4,5},{5,4},{6,7},{7,6},{8,9},{9,8},{10,11... | collective-permute-start | bytes 6291464 | tf_op jit(solution)/shard_map/ppermute | solution.py:419
  35.5 2.2 %copy-start.6 = (bf16[1024,2048]{1,0:T(8,128)(2,1)S(1)}, bf16[1024,2048]{1,0:T(8,128)(2,1)}, u32[]{:S(2)}) copy-start(bf16[1024,2048]{1,0:T(8,128)(2,1)} %hidden_ref.1) | copy-start | bytes 12582916
  37.7 1.6 %copy-start.7 = (bf16[2048,512]{1,0:T(8,128)(2,1)S(1)}, bf16[2048,512]{1,0:T(8,128)(2,1)}, u32[]{:S(2)}) copy-start(bf16[2048,512]{1,0:T(8,128)(2,1)} %pool_ref.1) | copy-start | bytes 6291460
  39.3 1.2 %copy-start.8 = (bf16[2048,256]{1,0:T(8,128)(2,1)S(1)}, bf16[2048,256]{1,0:T(8,128)(2,1)}, u32[]{:S(2)}) copy-start(bf16[2048,256]{1,0:T(8,128)(2,1)} %query_ref.1) | copy-start | bytes 3145732
  40.5 12.9 %copy-start.2 = (bf16[256,2048]{1,0:T(8,128)(2,1)S(1)}, bf16[256,2048]{1,0:T(8,128)(2,1)}, u32[]{:S(2)}) copy-start(bf16[256,2048]{1,0:T(8,128)(2,1)} %w_ref) | copy-start | bytes 3145732
  53.3 7.3 %copy-start.3 = (bf16[1024,256]{1,0:T(8,128)(2,1)}, bf16[1024,256]{1,0:T(8,128)(2,1)S(1)}, u32[]{:S(2)}) copy-start(bf16[1024,256]{1,0:T(8,128)(2,1)S(1)} %get-tuple-element.14.query_hbm) | copy-start | bytes 1572868
  53.3 31.5 %copy-start.4 = (s32[8,4]{0,1:T(4,128)S(1)}, s32[8,4]{0,1:T(4,128)}, u32[]{:S(2)}) copy-start(s32[8,4]{0,1:T(4,128)} %param.18) | copy-start | bytes 388
  53.3 31.5 %copy-start.5 = (f32[2]{0:T(128)S(1)}, f32[2]{0:T(128)}, u32[]{:S(2)}) copy-start(f32[2]{0:T(128)} %sharp_ref.1) | copy-start | bytes 28
  53.3 2.7 %collective-permute-start.1 = (bf16[1024,512]{1,0:T(8,128)(2,1)S(1)}, bf16[1024,512]{1,0:T(8,128)(2,1)S(1)}, u32[]{:S(2)}, u32[]{:S(2)}) collective-permute-start(bf16[1024,512]{1,0:T(8,128)(2,1)S(1)} %get-tuple-element.16.own_ref), channel_id=1, source_target_pairs={{0,1},{1,0},{2,3},{3,2},{4,5},{5,4},{6,7},{7,6},{8,9},{9,8},{10,11... | collective-permute-start | bytes 3145736 | tf_op jit(solution)/shard_map/ppermute | solution.py:419
  53.5 8.5 %collective-permute-start = (bf16[256,2048]{1,0:T(8,128)(2,1)S(1)}, bf16[256,2048]{1,0:T(8,128)(2,1)}, u32[]{:S(2)}, u32[]{:S(2)}) collective-permute-start(bf16[256,2048]{1,0:T(8,128)(2,1)S(1)} %copy-done.2), channel_id=1, source_target_pairs={{0,1},{1,0},{2,3},{3,2},{4,5},{5,4},{6,7},{7,6},{8,9},{9,8},{10,11... | collective-permute-start | bytes 3145736 | tf_op jit(solution)/shard_map/ppermute | solution.py:419
  60.6 1.3 %copy-start = (bf16[1024,1024]{1,0:T(8,128)(2,1)}, bf16[1024,1024]{1,0:T(8,128)(2,1)S(1)}, u32[]{:S(2)}) copy-start(bf16[1024,1024]{1,0:T(8,128)(2,1)S(1)} %get-tuple-element.21.pool_ref) | copy-start | bytes 6291460
  84.8 7.4 %copy-start.1 = (bf16[1024,1024]{1,0:T(8,128)(2,1)S(1)}, bf16[1024,1024]{1,0:T(8,128)(2,1)}, u32[]{:S(2)}) copy-start(bf16[1024,1024]{1,0:T(8,128)(2,1)} %copy-done) | copy-start | bytes 6291460
  89.1 4.7 %collective-permute-start.3 = (bf16[1024,256]{1,0:T(8,128)(2,1)S(1)}, bf16[1024,256]{1,0:T(8,128)(2,1)S(1)}, u32[]{:S(2)}, u32[]{:S(2)}) collective-permute-start(bf16[1024,256]{1,0:T(8,128)(2,1)S(1)} %get-tuple-element.19.own_ref), channel_id=1, source_target_pairs={{0,1},{1,0},{2,3},{3,2},{4,5},{5,4},{6,7},{7,6},{8,9},{9,8},{10,11... | collective-permute-start | bytes 1572872 | tf_op jit(solution)/shard_map/ppermute | solution.py:419

commit v6 on v5

--- a/solution.py
+++ b/solution.py
@@ -11,8 +11,8 @@
 F32, BF16 = jnp.float32, jnp.bfloat16
 EPS = 1e-05
 CARRY = 16
-STRIP = 32
-TOGETHER = 2
+STRIP = 64
+TOGETHER = 1
 SWAP = [(0, 1), (1, 0)]
 
 
@@ -405,7 +405,7 @@
         in_specs=[pl.BlockSpec(memory_space=pltpu.VMEM)] * 4,
         out_specs=pl.BlockSpec(memory_space=pl.ANY),
         out_shape=jax.ShapeDtypeStruct((tokens, width), BF16),
-        scratch_shapes=[pltpu.VMEM((tokens, width), BF16), pltpu.SemaphoreType.DMA((8,))],
+        scratch_shapes=[pltpu.VMEM((tokens, width), BF16), pltpu.SemaphoreType.DMA((4,))],
         compiler_params=params(24),
         cost_estimate=cost(2 * tokens * depth * width, 12 << 20),
         name="mixed",

time: 96.2 us -> 96.1 us (level)
  no operation moved by 1% of the time
where the time goes in v6:
time: 96.1 us; the launch traced here: 95.6 us
  Pallas kernels  36 us (37%)
  starting transfers between devices  26.5 us (28%)
  waiting for transfers between devices  26.4 us (27%)
  local copies, waits for them, and re-layouts  6.35 us (7%)
    all_to_all x2, waiting for transfers between devices, body(): lax.all_to_all(a, 'st', split_axis=0, concat_axis=0, tiled=True)  23.8 us
    all_to_all x2, starting transfers between devices, body(): lax.all_to_all(a, 'st', split_axis=0, concat_axis=0, tiled=True)  21.2 us
    pallas_call x1, Pallas kernels, front(): pl.pallas_call(front_kernel, grid=(tokens // tile,), in_specs=[rowed(widt...  12.8 us
    pallas_call x1, Pallas kernels, project(): pl.pallas_call(project_kernel, in_specs=[pl.BlockSpec(memory_space=pltpu....  7.37 us
    unnamed x22, local copies, waits for them, and re-layouts  6.35 us
    ppermute x4, starting transfers between devices, body(): swapped = lambda a: lax.ppermute(a, 'tp', SWAP)  5.31 us
    pallas_call x1, Pallas kernels, branch(): pl.pallas_call(branch_kernel, grid=(tokens // tile,), in_specs=[pl.BlockS...  4.52 us
    pallas_call x1, Pallas kernels, attend(): pl.pallas_call(functools.partial(attend_kernel, count=count), in_specs=[p...  4.2 us
  transfers between devices with their start and end apart: 6, of which 4 were waited for; matrix products, arithmetic and copies ran while one was open for 0% of the time, Pallas kernels for 27%

profile of v6, /device:TPU:1, one launch (start us, length us, event | category | flops | bytes accessed | tf_op | source)
XLA Modules:
  0.0 95.6 jit_solution(17467801651292504906)
XLA Ops:
  0.0 1.4 %requests.1 = s32[64,1,128]{2,1,0:T(1,128)} custom-call(s32[4,8]{1,0:T(4,128)} %bitcast.3), custom_call_target="tpu_custom_call" | custom-call | tf_op jit(solution)/shard_map/requests/pallas_call | solution.py:54
  1.4 12.0 %all-to-all-start = ((s32[64,1,128]{2,1,0:T(1,128)}), s32[64,1,128]{2,1,0:T(1,128)S(1)}, u32[]{:S(2)}, u32[]{:S(2)}) async-start(s32[64,1,128]{2,1,0:T(1,128)} %requests.1), calls=%async_computation | async-start | bytes 65536 | tf_op jit(solution)/shard_map/all_to_all | solution.py:420
  13.4 7.4 %project.1.kv_ref = bf16[24,64,512]{2,1,0:T(8,128)(2,1)S(1)} custom-call(bf16[24,64,2048]{2,1,0:T(8,128)(2,1)} %store_ref.1, f32[1,2048]{1,0:T(1,128)} %bitcast.6, bf16[2048,256]{1,0:T(8,128)(2,1)} %key_hbm.1, bf16[2048,256]{1,0:T(8,128)(2,1)} %value_hbm.1), custom_call_target="tpu_custom_call" | custom-call | flops 3221225472 | bytes 9437184 | tf_op jit(solution)/shard_map/project/pallas_call | solution.py:111
  20.8 1.0 %all-to-all-done.asked_hbm = s32[64,1,128]{2,1,0:T(1,128)S(1)} async-done(((s32[64,1,128]{2,1,0:T(1,128)}), s32[64,1,128]{2,1,0:T(1,128)S(1)}, u32[]{:S(2)}, u32[]{:S(2)}) %all-to-all-start) | async-done | bytes 32800 | tf_op jit(solution)/shard_map/all_to_all | solution.py:420
  21.7 2.8 %place.1 = bf16[64,64,512]{2,1,0:T(8,128)(2,1)} custom-call(s32[64,1,128]{2,1,0:T(1,128)S(1)} %all-to-all-done.asked_hbm, bf16[24,64,512]{2,1,0:T(8,128)(2,1)S(1)} %project.1.kv_ref), custom_call_target="tpu_custom_call" | custom-call | bytes 5242880 | tf_op jit(solution)/shard_map/place/pallas_call | solution.py:147
  24.6 0.0 copy-start.9
  24.6 0.0 copy-start.10
  24.6 9.3 %all-to-all-start.1 = ((bf16[64,64,512]{2,1,0:T(8,128)(2,1)}), bf16[64,64,512]{2,1,0:T(8,128)(2,1)}, u32[]{:S(2)}, u32[]{:S(2)}) async-start(bf16[64,64,512]{2,1,0:T(8,128)(2,1)} %place.1), calls=%async_computation.1 | async-start | bytes 8388608 | tf_op jit(solution)/shard_map/all_to_all | solution.py:420
  33.9 1.6 %collective-permute-start.2 = (bf16[512,2048]{1,0:T(8,128)(2,1)}, bf16[512,2048]{1,0:T(8,128)(2,1)S(1)}, u32[]{:S(2)}, u32[]{:S(2)}) collective-permute-start(bf16[512,2048]{1,0:T(8,128)(2,1)} %w_own_ref), channel_id=1, source_target_pairs={{0,1},{1,0},{2,3},{3,2},{4,5},{5,4},{6,7},{7,6},{8,9},{9,8},{10,11... | collective-permute-start | bytes 6291464 | tf_op jit(solution)/shard_map/ppermute | solution.py:419
  35.4 0.0 copy-done.9
  35.5 0.0 copy-done.10
  35.5 0.0 copy-start.6
  35.5 2.2 %copy-done.6 = bf16[1024,2048]{1,0:T(8,128)(2,1)S(1)} copy-done((bf16[1024,2048]{1,0:T(8,128)(2,1)S(1)}, bf16[1024,2048]{1,0:T(8,128)(2,1)}, u32[]{:S(2)}) %copy-start.6) | copy-done | bytes 4194328
  37.6 0.0 copy-start.7
  37.6 1.6 %copy-done.7 = bf16[2048,512]{1,0:T(8,128)(2,1)S(1)} copy-done((bf16[2048,512]{1,0:T(8,128)(2,1)S(1)}, bf16[2048,512]{1,0:T(8,128)(2,1)}, u32[]{:S(2)}) %copy-start.7) | copy-done | bytes 2097176
  39.2 0.0 copy-start.8
  39.2 1.2 %copy-done.8 = bf16[2048,256]{1,0:T(8,128)(2,1)S(1)} copy-done((bf16[2048,256]{1,0:T(8,128)(2,1)S(1)}, bf16[2048,256]{1,0:T(8,128)(2,1)}, u32[]{:S(2)}) %copy-start.8) | copy-done | bytes 1048600
  40.5 0.0 copy-start.2
  40.5 12.8 %front.1 = (bf16[1024,512]{1,0:T(8,128)(2,1)S(1)}, bf16[1024,256]{1,0:T(8,128)(2,1)S(1)}, bf16[1024,1024]{1,0:T(8,128)(2,1)S(1)}) custom-call(bf16[1024,2048]{1,0:T(8,128)(2,1)S(1)} %copy-done.6, f32[1,2048]{1,0:T(1,128)S(1)} %bitcast.5, bf16[2048,512]{1,0:T(8,128)(2,1)S(1)} %copy-done.7, bf16[2048,256]{1,0:T(8,128)(2,1)S(1)} %copy-done.8, ...), custom_call_target="tpu_custom_call" | custom-call | flops 7516192768 | bytes 25165824 | tf_op jit(solution)/shard_map/front/pallas_call | solution.py:205
  53.2 0.0 copy-start.3
  53.2 0.0 copy-start.4
  53.2 0.0 copy-start.5
  53.3 0.1 collective-permute-start.1
  53.4 0.0 copy-done.2
  53.4 0.5 collective-permute-start
  53.9 2.1 %collective-permute-done.1.other_ref = bf16[1024,512]{1,0:T(8,128)(2,1)S(1)} collective-permute-done((bf16[1024,512]{1,0:T(8,128)(2,1)S(1)}, bf16[1024,512]{1,0:T(8,128)(2,1)S(1)}, u32[]{:S(2)}, u32[]{:S(2)}) %collective-permute-start.1) | collective-permute-done | bytes 1048608 | tf_op jit(solution)/shard_map/ppermute | solution.py:419
  56.0 0.0 collective-permute-done.2.w_other_ref
  56.0 4.5 %branch.1 = (bf16[1024,1024]{1,0:T(8,128)(2,1)S(1)}, f32[8,128]{1,0:T(8,128)S(1)}) custom-call(bf16[1024,512]{1,0:T(8,128)(2,1)S(1)} %get-tuple-element.16.own_ref, bf16[1024,512]{1,0:T(8,128)(2,1)S(1)} %collective-permute-done.1.other_ref, bf16[512,2048]{1,0:T(8,128)(2,1)} %w_own_ref, bf16[512,2048]{1,0:T(8,128)(2,1)S(1)} %collective-permute-done.2.w_other_ref), custom_call_target="tpu_custom_call" | custom-call | flops 2147483648 | bytes 8388608 | tf_op jit(solution)/shard_map/branch/pallas_call | solution.py:245
  60.5 0.0 copy-done.3
  60.5 0.0 copy-start
  60.6 1.3 %copy-done = bf16[1024,1024]{1,0:T(8,128)(2,1)} copy-done((bf16[1024,1024]{1,0:T(8,128)(2,1)}, bf16[1024,1024]{1,0:T(8,128)(2,1)S(1)}, u32[]{:S(2)}) %copy-start) | copy-done | bytes 2097176
  61.9 0.0 collective-permute-done.w_other_ref
  61.9 22.8 %all-to-all-done.1.kv_ref = bf16[64,64,512]{2,1,0:T(8,128)(2,1)} async-done(((bf16[64,64,512]{2,1,0:T(8,128)(2,1)}), bf16[64,64,512]{2,1,0:T(8,128)(2,1)}, u32[]{:S(2)}, u32[]{:S(2)}) %all-to-all-start.1) | async-done | bytes 4194336 | tf_op jit(solution)/shard_map/all_to_all | solution.py:420
  84.7 0.0 copy-done.4
  84.7 0.0 copy-done.5
  84.7 0.0 copy-start.1
  84.7 4.2 %attend.1 = (bf16[1024,256]{1,0:T(8,128)(2,1)S(1)}, bf16[256,1024]{1,0:T(8,128)(2,1)S(1)}) custom-call(s32[4,8]{1,0:T(4,128)S(1)} %bitcast.4, f32[2]{0:T(128)S(1)} %copy-done.5, bf16[1024,256]{1,0:T(8,128)(2,1)} %copy-done.3, bf16[64,64,512]{2,1,0:T(8,128)(2,1)} %all-to-all-done.1.kv_ref, bf16[256,2048]{1,0:T(8,128)(2,1)} %collective-permute-done.w_other_ref, ...), custom_call_target="tpu_custom_call" | custom-call | flops 1073741824 | bytes 3145728 | tf_op jit(solution)/shard_map/attend/pallas_call | solution.py:334
  88.9 3.1 %collective-permute-start.3 = (bf16[1024,256]{1,0:T(8,128)(2,1)S(1)}, bf16[1024,256]{1,0:T(8,128)(2,1)S(1)}, u32[]{:S(2)}, u32[]{:S(2)}) collective-permute-start(bf16[1024,256]{1,0:T(8,128)(2,1)S(1)} %get-tuple-element.19.own_ref), channel_id=1, source_target_pairs={{0,1},{1,0},{2,3},{3,2},{4,5},{5,4},{6,7},{7,6},{8,9},{9,8},{10,11... | collective-permute-start | bytes 1572872 | tf_op jit(solution)/shard_map/ppermute | solution.py:419
  92.1 0.0 copy-done.1
  92.1 1.1 %own_part.1.sum_ref = f32[1024,1024]{1,0:T(8,128)S(1)} custom-call(bf16[1024,256]{1,0:T(8,128)(2,1)S(1)} %get-tuple-element.19.own_ref, bf16[256,2048]{1,0:T(8,128)(2,1)S(1)} %copy-done.2, bf16[1024,1024]{1,0:T(8,128)(2,1)S(1)} %copy-done.1, bf16[1024,1024]{1,0:T(8,128)(2,1)S(1)} %get-tuple-element.22.gate_ref), custom_call_target="tpu_custom_call" | custom-call | flops 536870912 | bytes 12582912 | tf_op jit(solution)/shard_map/own_part/pallas_call | solution.py:375
  93.1 0.5 collective-permute-done.3.other_ref
  93.6 1.8 %mixed.1 = bf16[1024,1024]{1,0:T(8,128)(2,1)} custom-call(bf16[1024,256]{1,0:T(8,128)(2,1)S(1)} %collective-permute-done.3.other_ref, bf16[256,1024]{1,0:T(8,128)(2,1)S(1)} %get-tuple-element.20.w_ref, f32[1024,1024]{1,0:T(8,128)S(1)} %own_part.1.sum_ref, bf16[1024,1024]{1,0:T(8,128)(2,1)S(1)} %get-tuple-element.22.gate_ref), custom_call_target="tpu_custom_call" | custom-call | flops 536870912 | bytes 12582912 | tf_op jit(solution)/shard_map/mixed/pallas_call | solution.py:403
Async XLA Ops:
  1.4 20.3 %all-to-all-start = ((s32[64,1,128]{2,1,0:T(1,128)}), s32[64,1,128]{2,1,0:T(1,128)S(1)}, u32[]{:S(2)}, u32[]{:S(2)}) async-start(s32[64,1,128]{2,1,0:T(1,128)} %requests.1), calls=%async_computation | async-start | bytes 65536 | tf_op jit(solution)/shard_map/all_to_all | solution.py:420
  24.6 10.9 %copy-start.9 = (bf16[2,256,256]{2,1,0:T(8,128)(2,1)S(1)}, bf16[2,256,256]{2,1,0:T(8,128)(2,1)}, u32[]{:S(2)}) copy-start(bf16[2,256,256]{2,1,0:T(8,128)(2,1)} %mix_ref.1) | copy-start | bytes 786436
  24.6 10.9 %copy-start.10 = (f32[2048]{0:T(1024)S(1)}, f32[2048]{0:T(1024)}, u32[]{:S(2)}) copy-start(f32[2048]{0:T(1024)} %param.15) | copy-start | bytes 24580
  24.6 60.1 %all-to-all-start.1 = ((bf16[64,64,512]{2,1,0:T(8,128)(2,1)}), bf16[64,64,512]{2,1,0:T(8,128)(2,1)}, u32[]{:S(2)}, u32[]{:S(2)}) async-start(bf16[64,64,512]{2,1,0:T(8,128)(2,1)} %place.1), calls=%async_computation.1 | async-start | bytes 8388608 | tf_op jit(solution)/shard_map/all_to_all | solution.py:420
  33.9 22.1 %collective-permute-start.2 = (bf16[512,2048]{1,0:T(8,128)(2,1)}, bf16[512,2048]{1,0:T(8,128)(2,1)S(1)}, u32[]{:S(2)}, u32[]{:S(2)}) collective-permute-start(bf16[512,2048]{1,0:T(8,128)(2,1)} %w_own_ref), channel_id=1, source_target_pairs={{0,1},{1,0},{2,3},{3,2},{4,5},{5,4},{6,7},{7,6},{8,9},{9,8},{10,11... | collective-permute-start | bytes 6291464 | tf_op jit(solution)/shard_map/ppermute | solution.py:419
  35.5 2.2 %copy-start.6 = (bf16[1024,2048]{1,0:T(8,128)(2,1)S(1)}, bf16[1024,2048]{1,0:T(8,128)(2,1)}, u32[]{:S(2)}) copy-start(bf16[1024,2048]{1,0:T(8,128)(2,1)} %hidden_ref.1) | copy-start | bytes 12582916
  37.6 1.6 %copy-start.7 = (bf16[2048,512]{1,0:T(8,128)(2,1)S(1)}, bf16[2048,512]{1,0:T(8,128)(2,1)}, u32[]{:S(2)}) copy-start(bf16[2048,512]{1,0:T(8,128)(2,1)} %pool_ref.1) | copy-start | bytes 6291460
  39.2 1.2 %copy-start.8 = (bf16[2048,256]{1,0:T(8,128)(2,1)S(1)}, bf16[2048,256]{1,0:T(8,128)(2,1)}, u32[]{:S(2)}) copy-start(bf16[2048,256]{1,0:T(8,128)(2,1)} %query_ref.1) | copy-start | bytes 3145732
  40.5 12.9 %copy-start.2 = (bf16[256,2048]{1,0:T(8,128)(2,1)S(1)}, bf16[256,2048]{1,0:T(8,128)(2,1)}, u32[]{:S(2)}) copy-start(bf16[256,2048]{1,0:T(8,128)(2,1)} %w_ref) | copy-start | bytes 3145732
  53.2 7.3 %copy-start.3 = (bf16[1024,256]{1,0:T(8,128)(2,1)}, bf16[1024,256]{1,0:T(8,128)(2,1)S(1)}, u32[]{:S(2)}) copy-start(bf16[1024,256]{1,0:T(8,128)(2,1)S(1)} %get-tuple-element.14.query_hbm) | copy-start | bytes 1572868
  53.2 31.5 %copy-start.4 = (s32[8,4]{0,1:T(4,128)S(1)}, s32[8,4]{0,1:T(4,128)}, u32[]{:S(2)}) copy-start(s32[8,4]{0,1:T(4,128)} %param.18) | copy-start | bytes 388
  53.2 31.5 %copy-start.5 = (f32[2]{0:T(128)S(1)}, f32[2]{0:T(128)}, u32[]{:S(2)}) copy-start(f32[2]{0:T(128)} %sharp_ref.1) | copy-start | bytes 28
  53.3 2.7 %collective-permute-start.1 = (bf16[1024,512]{1,0:T(8,128)(2,1)S(1)}, bf16[1024,512]{1,0:T(8,128)(2,1)S(1)}, u32[]{:S(2)}, u32[]{:S(2)}) collective-permute-start(bf16[1024,512]{1,0:T(8,128)(2,1)S(1)} %get-tuple-element.16.own_ref), channel_id=1, source_target_pairs={{0,1},{1,0},{2,3},{3,2},{4,5},{5,4},{6,7},{7,6},{8,9},{9,8},{10,11... | collective-permute-start | bytes 3145736 | tf_op jit(solution)/shard_map/ppermute | solution.py:419
  53.4 8.5 %collective-permute-start = (bf16[256,2048]{1,0:T(8,128)(2,1)S(1)}, bf16[256,2048]{1,0:T(8,128)(2,1)}, u32[]{:S(2)}, u32[]{:S(2)}) collective-permute-start(bf16[256,2048]{1,0:T(8,128)(2,1)S(1)} %copy-done.2), channel_id=1, source_target_pairs={{0,1},{1,0},{2,3},{3,2},{4,5},{5,4},{6,7},{7,6},{8,9},{9,8},{10,11... | collective-permute-start | bytes 3145736 | tf_op jit(solution)/shard_map/ppermute | solution.py:419
  60.5 1.3 %copy-start = (bf16[1024,1024]{1,0:T(8,128)(2,1)}, bf16[1024,1024]{1,0:T(8,128)(2,1)S(1)}, u32[]{:S(2)}) copy-start(bf16[1024,1024]{1,0:T(8,128)(2,1)S(1)} %get-tuple-element.21.pool_ref) | copy-start | bytes 6291460
  84.7 7.3 %copy-start.1 = (bf16[1024,1024]{1,0:T(8,128)(2,1)S(1)}, bf16[1024,1024]{1,0:T(8,128)(2,1)}, u32[]{:S(2)}) copy-start(bf16[1024,1024]{1,0:T(8,128)(2,1)} %copy-done) | copy-start | bytes 6291460
  88.9 4.7 %collective-permute-start.3 = (bf16[1024,256]{1,0:T(8,128)(2,1)S(1)}, bf16[1024,256]{1,0:T(8,128)(2,1)S(1)}, u32[]{:S(2)}, u32[]{:S(2)}) collective-permute-start(bf16[1024,256]{1,0:T(8,128)(2,1)S(1)} %get-tuple-element.19.own_ref), channel_id=1, source_target_pairs={{0,1},{1,0},{2,3},{3,2},{4,5},{5,4},{6,7},{7,6},{8,9},{9,8},{10,11... | collective-permute-start | bytes 1572872 | tf_op jit(solution)/shard_map/ppermute | solution.py:419

commit v7 on v6

--- a/solution.py
+++ b/solution.py
@@ -90,13 +90,14 @@
     loads[0].wait()
     norm(0, 0, tile)
     key.wait()
-    value.wait()
     for i in range(tiles):
         if i + 1 < tiles:
             loads[i + 1].wait()
         for p in range(2):
             if i + 1 < tiles:
                 norm(i + 1, p * tile // 2, (p + 1) * tile // 2)
+            if i == 0 and p == 1:
+                value.wait()
             found = dot(normed[i % 2], w_ref[p]).astype(BF16).reshape(per, length, half)
             out_ref[i * per : (i + 1) * per, :, p * half : (p + 1) * half] = found
 

time: 96.1 us -> 96.8 us (level)
  no operation moved by 1% of the time
where the time goes in v7:
time: 96.8 us; the launch traced here: 96.3 us
  Pallas kernels  36.7 us (38%)
  starting transfers between devices  27.2 us (28%)
  waiting for transfers between devices  25.8 us (27%)
  local copies, waits for them, and re-layouts  6.35 us (7%)
    all_to_all x2, waiting for transfers between devices, body(): lax.all_to_all(a, 'st', split_axis=0, concat_axis=0, tiled=True)  23.2 us
    all_to_all x2, starting transfers between devices, body(): lax.all_to_all(a, 'st', split_axis=0, concat_axis=0, tiled=True)  21.8 us
    pallas_call x1, Pallas kernels, front(): pl.pallas_call(front_kernel, grid=(tokens // tile,), in_specs=[rowed(widt...  12.8 us
    pallas_call x1, Pallas kernels, project(): pl.pallas_call(project_kernel, in_specs=[pl.BlockSpec(memory_space=pltpu....  8.02 us
    unnamed x22, local copies, waits for them, and re-layouts  6.35 us
    ppermute x4, starting transfers between devices, body(): swapped = lambda a: lax.ppermute(a, 'tp', SWAP)  5.31 us
    pallas_call x1, Pallas kernels, branch(): pl.pallas_call(branch_kernel, grid=(tokens // tile,), in_specs=[pl.BlockS...  4.52 us
    pallas_call x1, Pallas kernels, attend(): pl.pallas_call(functools.partial(attend_kernel, count=count), in_specs=[p...  4.2 us
  transfers between devices with their start and end apart: 6, of which 4 were waited for; matrix products, arithmetic and copies ran while one was open for 0% of the time, Pallas kernels for 27%

profile of v7, /device:TPU:1, one launch (start us, length us, event | category | flops | bytes accessed | tf_op | source)
XLA Modules:
  0.0 96.3 jit_solution(9942437692141865008)
XLA Ops:
  0.0 1.4 %requests.1 = s32[64,1,128]{2,1,0:T(1,128)} custom-call(s32[4,8]{1,0:T(4,128)} %bitcast.3), custom_call_target="tpu_custom_call" | custom-call | tf_op jit(solution)/shard_map/requests/pallas_call | solution.py:54
  1.4 12.0 %all-to-all-start = ((s32[64,1,128]{2,1,0:T(1,128)}), s32[64,1,128]{2,1,0:T(1,128)S(1)}, u32[]{:S(2)}, u32[]{:S(2)}) async-start(s32[64,1,128]{2,1,0:T(1,128)} %requests.1), calls=%async_computation | async-start | bytes 65536 | tf_op jit(solution)/shard_map/all_to_all | solution.py:421
  13.4 8.0 %project.1.kv_ref = bf16[24,64,512]{2,1,0:T(8,128)(2,1)S(1)} custom-call(bf16[24,64,2048]{2,1,0:T(8,128)(2,1)} %store_ref.1, f32[1,2048]{1,0:T(1,128)} %bitcast.6, bf16[2048,256]{1,0:T(8,128)(2,1)} %key_hbm.1, bf16[2048,256]{1,0:T(8,128)(2,1)} %value_hbm.1), custom_call_target="tpu_custom_call" | custom-call | flops 3221225472 | bytes 9437184 | tf_op jit(solution)/shard_map/project/pallas_call | solution.py:112
  21.4 0.3 all-to-all-done.asked_hbm
  21.7 2.9 %place.1 = bf16[64,64,512]{2,1,0:T(8,128)(2,1)} custom-call(s32[64,1,128]{2,1,0:T(1,128)S(1)} %all-to-all-done.asked_hbm, bf16[24,64,512]{2,1,0:T(8,128)(2,1)S(1)} %project.1.kv_ref), custom_call_target="tpu_custom_call" | custom-call | bytes 5242880 | tf_op jit(solution)/shard_map/place/pallas_call | solution.py:148
  24.6 0.0 copy-start.9
  24.7 0.0 copy-start.10
  24.7 9.9 %all-to-all-start.1 = ((bf16[64,64,512]{2,1,0:T(8,128)(2,1)}), bf16[64,64,512]{2,1,0:T(8,128)(2,1)}, u32[]{:S(2)}, u32[]{:S(2)}) async-start(bf16[64,64,512]{2,1,0:T(8,128)(2,1)} %place.1), calls=%async_computation.1 | async-start | bytes 8388608 | tf_op jit(solution)/shard_map/all_to_all | solution.py:421
  34.6 1.6 %collective-permute-start.2 = (bf16[512,2048]{1,0:T(8,128)(2,1)}, bf16[512,2048]{1,0:T(8,128)(2,1)S(1)}, u32[]{:S(2)}, u32[]{:S(2)}) collective-permute-start(bf16[512,2048]{1,0:T(8,128)(2,1)} %w_own_ref), channel_id=1, source_target_pairs={{0,1},{1,0},{2,3},{3,2},{4,5},{5,4},{6,7},{7,6},{8,9},{9,8},{10,11... | collective-permute-start | bytes 6291464 | tf_op jit(solution)/shard_map/ppermute | solution.py:420
  36.2 0.0 copy-done.9
  36.2 0.0 copy-done.10
  36.2 0.0 copy-start.6
  36.2 2.2 %copy-done.6 = bf16[1024,2048]{1,0:T(8,128)(2,1)S(1)} copy-done((bf16[1024,2048]{1,0:T(8,128)(2,1)S(1)}, bf16[1024,2048]{1,0:T(8,128)(2,1)}, u32[]{:S(2)}) %copy-start.6) | copy-done | bytes 4194328
  38.4 0.0 copy-start.7
  38.4 1.6 %copy-done.7 = bf16[2048,512]{1,0:T(8,128)(2,1)S(1)} copy-done((bf16[2048,512]{1,0:T(8,128)(2,1)S(1)}, bf16[2048,512]{1,0:T(8,128)(2,1)}, u32[]{:S(2)}) %copy-start.7) | copy-done | bytes 2097176
  39.9 0.0 copy-start.8
  39.9 1.2 %copy-done.8 = bf16[2048,256]{1,0:T(8,128)(2,1)S(1)} copy-done((bf16[2048,256]{1,0:T(8,128)(2,1)S(1)}, bf16[2048,256]{1,0:T(8,128)(2,1)}, u32[]{:S(2)}) %copy-start.8) | copy-done | bytes 1048600
  41.2 0.0 copy-start.2
  41.2 12.8 %front.1 = (bf16[1024,512]{1,0:T(8,128)(2,1)S(1)}, bf16[1024,256]{1,0:T(8,128)(2,1)S(1)}, bf16[1024,1024]{1,0:T(8,128)(2,1)S(1)}) custom-call(bf16[1024,2048]{1,0:T(8,128)(2,1)S(1)} %copy-done.6, f32[1,2048]{1,0:T(1,128)S(1)} %bitcast.5, bf16[2048,512]{1,0:T(8,128)(2,1)S(1)} %copy-done.7, bf16[2048,256]{1,0:T(8,128)(2,1)S(1)} %copy-done.8, ...), custom_call_target="tpu_custom_call" | custom-call | flops 7516192768 | bytes 25165824 | tf_op jit(solution)/shard_map/front/pallas_call | solution.py:206
  53.9 0.0 copy-start.3
  53.9 0.0 copy-start.4
  54.0 0.0 copy-start.5
  54.0 0.1 collective-permute-start.1
  54.1 0.0 copy-done.2
  54.1 0.5 collective-permute-start
  54.6 2.1 %collective-permute-done.1.other_ref = bf16[1024,512]{1,0:T(8,128)(2,1)S(1)} collective-permute-done((bf16[1024,512]{1,0:T(8,128)(2,1)S(1)}, bf16[1024,512]{1,0:T(8,128)(2,1)S(1)}, u32[]{:S(2)}, u32[]{:S(2)}) %collective-permute-start.1) | collective-permute-done | bytes 1048608 | tf_op jit(solution)/shard_map/ppermute | solution.py:420
  56.7 0.0 collective-permute-done.2.w_other_ref
  56.7 4.5 %branch.1 = (bf16[1024,1024]{1,0:T(8,128)(2,1)S(1)}, f32[8,128]{1,0:T(8,128)S(1)}) custom-call(bf16[1024,512]{1,0:T(8,128)(2,1)S(1)} %get-tuple-element.16.own_ref, bf16[1024,512]{1,0:T(8,128)(2,1)S(1)} %collective-permute-done.1.other_ref, bf16[512,2048]{1,0:T(8,128)(2,1)} %w_own_ref, bf16[512,2048]{1,0:T(8,128)(2,1)S(1)} %collective-permute-done.2.w_other_ref), custom_call_target="tpu_custom_call" | custom-call | flops 2147483648 | bytes 8388608 | tf_op jit(solution)/shard_map/branch/pallas_call | solution.py:246
  61.2 0.0 copy-done.3
  61.2 0.0 copy-start
  61.3 1.3 %copy-done = bf16[1024,1024]{1,0:T(8,128)(2,1)} copy-done((bf16[1024,1024]{1,0:T(8,128)(2,1)}, bf16[1024,1024]{1,0:T(8,128)(2,1)S(1)}, u32[]{:S(2)}) %copy-start) | copy-done | bytes 2097176
  62.6 0.0 collective-permute-done.w_other_ref
  62.6 22.9 %all-to-all-done.1.kv_ref = bf16[64,64,512]{2,1,0:T(8,128)(2,1)} async-done(((bf16[64,64,512]{2,1,0:T(8,128)(2,1)}), bf16[64,64,512]{2,1,0:T(8,128)(2,1)}, u32[]{:S(2)}, u32[]{:S(2)}) %all-to-all-start.1) | async-done | bytes 4194336 | tf_op jit(solution)/shard_map/all_to_all | solution.py:421
  85.4 0.0 copy-done.4
  85.4 0.0 copy-done.5
  85.5 0.0 copy-start.1
  85.5 4.2 %attend.1 = (bf16[1024,256]{1,0:T(8,128)(2,1)S(1)}, bf16[256,1024]{1,0:T(8,128)(2,1)S(1)}) custom-call(s32[4,8]{1,0:T(4,128)S(1)} %bitcast.4, f32[2]{0:T(128)S(1)} %copy-done.5, bf16[1024,256]{1,0:T(8,128)(2,1)} %copy-done.3, bf16[64,64,512]{2,1,0:T(8,128)(2,1)} %all-to-all-done.1.kv_ref, bf16[256,2048]{1,0:T(8,128)(2,1)} %collective-permute-done.w_other_ref, ...), custom_call_target="tpu_custom_call" | custom-call | flops 1073741824 | bytes 3145728 | tf_op jit(solution)/shard_map/attend/pallas_call | solution.py:335
  89.7 3.1 %collective-permute-start.3 = (bf16[1024,256]{1,0:T(8,128)(2,1)S(1)}, bf16[1024,256]{1,0:T(8,128)(2,1)S(1)}, u32[]{:S(2)}, u32[]{:S(2)}) collective-permute-start(bf16[1024,256]{1,0:T(8,128)(2,1)S(1)} %get-tuple-element.19.own_ref), channel_id=1, source_target_pairs={{0,1},{1,0},{2,3},{3,2},{4,5},{5,4},{6,7},{7,6},{8,9},{9,8},{10,11... | collective-permute-start | bytes 1572872 | tf_op jit(solution)/shard_map/ppermute | solution.py:420
  92.8 0.0 copy-done.1
  92.8 1.1 %own_part.1.sum_ref = f32[1024,1024]{1,0:T(8,128)S(1)} custom-call(bf16[1024,256]{1,0:T(8,128)(2,1)S(1)} %get-tuple-element.19.own_ref, bf16[256,2048]{1,0:T(8,128)(2,1)S(1)} %copy-done.2, bf16[1024,1024]{1,0:T(8,128)(2,1)S(1)} %copy-done.1, bf16[1024,1024]{1,0:T(8,128)(2,1)S(1)} %get-tuple-element.22.gate_ref), custom_call_target="tpu_custom_call" | custom-call | flops 536870912 | bytes 12582912 | tf_op jit(solution)/shard_map/own_part/pallas_call | solution.py:376
  93.9 0.5 collective-permute-done.3.other_ref
  94.3 1.8 %mixed.1 = bf16[1024,1024]{1,0:T(8,128)(2,1)} custom-call(bf16[1024,256]{1,0:T(8,128)(2,1)S(1)} %collective-permute-done.3.other_ref, bf16[256,1024]{1,0:T(8,128)(2,1)S(1)} %get-tuple-element.20.w_ref, f32[1024,1024]{1,0:T(8,128)S(1)} %own_part.1.sum_ref, bf16[1024,1024]{1,0:T(8,128)(2,1)S(1)} %get-tuple-element.22.gate_ref), custom_call_target="tpu_custom_call" | custom-call | flops 536870912 | bytes 12582912 | tf_op jit(solution)/shard_map/mixed/pallas_call | solution.py:404
Async XLA Ops:
  1.4 20.3 %all-to-all-start = ((s32[64,1,128]{2,1,0:T(1,128)}), s32[64,1,128]{2,1,0:T(1,128)S(1)}, u32[]{:S(2)}, u32[]{:S(2)}) async-start(s32[64,1,128]{2,1,0:T(1,128)} %requests.1), calls=%async_computation | async-start | bytes 65536 | tf_op jit(solution)/shard_map/all_to_all | solution.py:421
  24.6 11.5 %copy-start.9 = (bf16[2,256,256]{2,1,0:T(8,128)(2,1)S(1)}, bf16[2,256,256]{2,1,0:T(8,128)(2,1)}, u32[]{:S(2)}) copy-start(bf16[2,256,256]{2,1,0:T(8,128)(2,1)} %mix_ref.1) | copy-start | bytes 786436
  24.7 11.5 %copy-start.10 = (f32[2048]{0:T(1024)S(1)}, f32[2048]{0:T(1024)}, u32[]{:S(2)}) copy-start(f32[2048]{0:T(1024)} %param.15) | copy-start | bytes 24580
  24.7 60.8 %all-to-all-start.1 = ((bf16[64,64,512]{2,1,0:T(8,128)(2,1)}), bf16[64,64,512]{2,1,0:T(8,128)(2,1)}, u32[]{:S(2)}, u32[]{:S(2)}) async-start(bf16[64,64,512]{2,1,0:T(8,128)(2,1)} %place.1), calls=%async_computation.1 | async-start | bytes 8388608 | tf_op jit(solution)/shard_map/all_to_all | solution.py:421
  34.6 22.1 %collective-permute-start.2 = (bf16[512,2048]{1,0:T(8,128)(2,1)}, bf16[512,2048]{1,0:T(8,128)(2,1)S(1)}, u32[]{:S(2)}, u32[]{:S(2)}) collective-permute-start(bf16[512,2048]{1,0:T(8,128)(2,1)} %w_own_ref), channel_id=1, source_target_pairs={{0,1},{1,0},{2,3},{3,2},{4,5},{5,4},{6,7},{7,6},{8,9},{9,8},{10,11... | collective-permute-start | bytes 6291464 | tf_op jit(solution)/shard_map/ppermute | solution.py:420
  36.2 2.2 %copy-start.6 = (bf16[1024,2048]{1,0:T(8,128)(2,1)S(1)}, bf16[1024,2048]{1,0:T(8,128)(2,1)}, u32[]{:S(2)}) copy-start(bf16[1024,2048]{1,0:T(8,128)(2,1)} %hidden_ref.1) | copy-start | bytes 12582916
  38.4 1.6 %copy-start.7 = (bf16[2048,512]{1,0:T(8,128)(2,1)S(1)}, bf16[2048,512]{1,0:T(8,128)(2,1)}, u32[]{:S(2)}) copy-start(bf16[2048,512]{1,0:T(8,128)(2,1)} %pool_ref.1) | copy-start | bytes 6291460
  39.9 1.2 %copy-start.8 = (bf16[2048,256]{1,0:T(8,128)(2,1)S(1)}, bf16[2048,256]{1,0:T(8,128)(2,1)}, u32[]{:S(2)}) copy-start(bf16[2048,256]{1,0:T(8,128)(2,1)} %query_ref.1) | copy-start | bytes 3145732
  41.2 12.9 %copy-start.2 = (bf16[256,2048]{1,0:T(8,128)(2,1)S(1)}, bf16[256,2048]{1,0:T(8,128)(2,1)}, u32[]{:S(2)}) copy-start(bf16[256,2048]{1,0:T(8,128)(2,1)} %w_ref) | copy-start | bytes 3145732
  53.9 7.3 %copy-start.3 = (bf16[1024,256]{1,0:T(8,128)(2,1)}, bf16[1024,256]{1,0:T(8,128)(2,1)S(1)}, u32[]{:S(2)}) copy-start(bf16[1024,256]{1,0:T(8,128)(2,1)S(1)} %get-tuple-element.14.query_hbm) | copy-start | bytes 1572868
  53.9 31.5 %copy-start.4 = (s32[8,4]{0,1:T(4,128)S(1)}, s32[8,4]{0,1:T(4,128)}, u32[]{:S(2)}) copy-start(s32[8,4]{0,1:T(4,128)} %param.18) | copy-start | bytes 388
  54.0 31.5 %copy-start.5 = (f32[2]{0:T(128)S(1)}, f32[2]{0:T(128)}, u32[]{:S(2)}) copy-start(f32[2]{0:T(128)} %sharp_ref.1) | copy-start | bytes 28
  54.0 2.7 %collective-permute-start.1 = (bf16[1024,512]{1,0:T(8,128)(2,1)S(1)}, bf16[1024,512]{1,0:T(8,128)(2,1)S(1)}, u32[]{:S(2)}, u32[]{:S(2)}) collective-permute-start(bf16[1024,512]{1,0:T(8,128)(2,1)S(1)} %get-tuple-element.16.own_ref), channel_id=1, source_target_pairs={{0,1},{1,0},{2,3},{3,2},{4,5},{5,4},{6,7},{7,6},{8,9},{9,8},{10,11... | collective-permute-start | bytes 3145736 | tf_op jit(solution)/shard_map/ppermute | solution.py:420
  54.1 8.5 %collective-permute-start = (bf16[256,2048]{1,0:T(8,128)(2,1)S(1)}, bf16[256,2048]{1,0:T(8,128)(2,1)}, u32[]{:S(2)}, u32[]{:S(2)}) collective-permute-start(bf16[256,2048]{1,0:T(8,128)(2,1)S(1)} %copy-done.2), channel_id=1, source_target_pairs={{0,1},{1,0},{2,3},{3,2},{4,5},{5,4},{6,7},{7,6},{8,9},{9,8},{10,11... | collective-permute-start | bytes 3145736 | tf_op jit(solution)/shard_map/ppermute | solution.py:420
  61.2 1.3 %copy-start = (bf16[1024,1024]{1,0:T(8,128)(2,1)}, bf16[1024,1024]{1,0:T(8,128)(2,1)S(1)}, u32[]{:S(2)}) copy-start(bf16[1024,1024]{1,0:T(8,128)(2,1)S(1)} %get-tuple-element.21.pool_ref) | copy-start | bytes 6291460
  85.5 7.3 %copy-start.1 = (bf16[1024,1024]{1,0:T(8,128)(2,1)S(1)}, bf16[1024,1024]{1,0:T(8,128)(2,1)}, u32[]{:S(2)}) copy-start(bf16[1024,1024]{1,0:T(8,128)(2,1)} %copy-done) | copy-start | bytes 6291460
  89.7 4.7 %collective-permute-start.3 = (bf16[1024,256]{1,0:T(8,128)(2,1)S(1)}, bf16[1024,256]{1,0:T(8,128)(2,1)S(1)}, u32[]{:S(2)}, u32[]{:S(2)}) collective-permute-start(bf16[1024,256]{1,0:T(8,128)(2,1)S(1)} %get-tuple-element.19.own_ref), channel_id=1, source_target_pairs={{0,1},{1,0},{2,3},{3,2},{4,5},{5,4},{6,7},{7,6},{8,9},{9,8},{10,11... | collective-permute-start | bytes 1572872 | tf_op jit(solution)/shard_map/ppermute | solution.py:420
